TPU v7x, 128 devices: a whole 4x4x4 slice. The times are simulated.
128 devices in a mesh: sp: 32 (over z, y, core), tp: 4 (over x).
Axes of the slice: x: 4, y: 4, z: 4, core: 2. Of those that a mesh axis runs over, the one named last changes fastest.
Arguments:
- middle_stream: bfloat16 [6144, 2048], P('sp', 'tp'), may hold values from -6 to 6
- output_gradient: bfloat16 [6144, 2048], P('sp', 'tp'), may hold values from -6 to 6
- routes: int32 [6144, 2], P('sp'), may hold values from 0 to 31, all different within a row; in each aligned block of 192 rows (0 to 191, 192 to 383, ...) at most 18 rows name the same one
- chosen_expert_weight: float32 [6144, 2], P('sp'), may hold values from 0.2 to 1
- expert_gate_weight: bfloat16 [32, 2048, 3584], P('sp', None, 'tp'), may hold values from -0.125 to 0.125
- expert_up_weight: bfloat16 [32, 2048, 3584], P('sp', None, 'tp'), may hold values from -0.125 to 0.125
- expert_down_weight: bfloat16 [32, 3584, 2048], P('sp', 'tp'), may hold values from -0.09375 to 0.09375
- recurrent_output_weight: bfloat16 [2048, 1024], P(None, 'tp'), may hold values from -0.1875 to 0.1875
- recurrence_input: bfloat16 [6144, 1024], P('sp', 'tp'), may hold values from -8 to 8
- output_gate_logits: bfloat16 [6144, 1024], P('sp', 'tp'), may hold values from -6 to 6
- recurrence_gate_weight: bfloat16 [8, 128, 128], replicated, may hold values from -0.5 to 0.5
- input_gate_weight: bfloat16 [8, 128, 128], replicated, may hold values from -0.5 to 0.5
- channel_decay_param: float32 [1024], P('tp'), may hold values from 4 to 13
- extra_log_decay: float32 [6144, 1024], P('sp', 'tp'), may hold values from -0.7 to 0
Outputs:
- grad_gate: bfloat16 [32, 2048, 3584], P('sp', None, 'tp')
- grad_up: bfloat16 [32, 2048, 3584], P('sp', None, 'tp')
- grad_down: bfloat16 [32, 3584, 2048], P('sp', 'tp')
- grad_out_proj: float32 [2048, 1024], P('sp', 'tp')
- grad_input: float32 [6144, 1024], P('sp', 'tp')
- grad_gate_pre: float32 [6144, 1024], P('sp', 'tp')
Inputs may be any that keep to these rules, and one draw needn't show every extreme that they name: `routes`: in the rows of one index of sp no expert is named more than 18 times, a bound that some block reaches in some of them; the entries of a row differ.
All inputs are finite; a program needn't handle non-finite values.
Results may differ from a plain program's by a relative error of at most 0.017.
Values may be sent and summed in bfloat16 or wider, within the bound.
No kernel may reach another device: no remote copies, remote signals or barrier semaphores. Data moves between devices by JAX's collectives and lax.ppermute only.
A program may use at most 128 MiB of HBM per device.

v0:
```python
import jax
import jax.numpy as jnp
from jax import lax
from jax.experimental import pallas as pl
from jax.experimental.pallas import tpu as pltpu
from jax.sharding import PartitionSpec as P

BF = jnp.bfloat16
F32 = jnp.float32
ROWS = 192
PEERS = 32
TPN = 4
LANE = 128
CH = 256
HID = 896
WIDTH = 2048
VMEM = pl.BlockSpec(memory_space=pltpu.VMEM)
SMEM = pl.BlockSpec(memory_space=pltpu.SMEM)


def mm(a, b, ca=1, cb=0):
    return lax.dot_general(a, b, (((ca,), (cb,)), ((), ())), preferred_element_type=F32)


def iota(shape, dim):
    return lax.broadcasted_iota(jnp.int32, shape, dim)


def call(body, out, n_in, flops, moved, smem=()):
    return pl.pallas_call(
        body,
        out_shape=out,
        in_specs=[SMEM if k in smem else VMEM for k in range(n_in)],
        out_specs=jax.tree.map(lambda _: VMEM, out),
        cost_estimate=pl.CostEstimate(flops=flops, bytes_accessed=moved, transcendentals=0),
        compiler_params=pltpu.CompilerParams(vmem_limit_bytes=56 * 1024 * 1024),
    )


def pack_main(block, out, base, pieces):
    rows = block.reshape(PEERS, 8, pieces * LANE)
    for pair in range(pieces // 2):
        lo = rows[:, :, 2 * pair * LANE : (2 * pair + 1) * LANE]
        hi = rows[:, :, (2 * pair + 1) * LANE : (2 * pair + 2) * LANE]
        at = base + pair * 16
        out[:, at : at + 16, :] = jnp.concatenate([lo, hi], axis=1).astype(BF)


def unpack_main(block, pair):
    got = block[:, pair * 16 : pair * 16 + 16, :].astype(F32)
    lo = got[:, :8, :].reshape(PEERS * 8, LANE).astype(BF)
    hi = got[:, 8:, :].reshape(PEERS * 8, LANE).astype(BF)
    return lo, hi


def tail_order(pieces):
    n = PEERS * pieces * 2
    r, c = iota((n, n), 0), iota((n, n), 1)
    peer, piece, slot = r // (pieces * 2), (r // 2) % pieces, r % 2
    return (piece * (PEERS * 2) + peer * 2 + slot == c).astype(F32).astype(BF)


def tail_order_back(pieces):
    n = PEERS * pieces * 2
    r, c = iota((n, n), 0), iota((n, n), 1)
    peer, piece, slot = c // (pieces * 2), (c // 2) % pieces, c % 2
    return (piece * (PEERS * 2) + peer * 2 + slot == r).astype(F32).astype(BF)


def pack_body(routes, weights, x, g, out_a, out_b, out_idx):
    experts = iota((PEERS, ROWS), 0)
    before = (iota((ROWS, ROWS), 0) < iota((ROWS, ROWS), 1)).astype(F32).astype(BF)
    same = iota((ROWS, ROWS), 0) == iota((ROWS, ROWS), 1)
    r0, r1 = routes[0:1, :], routes[1:2, :]
    o0 = (experts == r0).astype(F32)
    o1 = (experts == r1).astype(F32)
    c0 = mm(o0.astype(BF), before)
    c1 = mm(o1.astype(BF), before) + jnp.sum(o0, axis=1, keepdims=True)
    k0 = jnp.sum(o0 * c0, axis=0, keepdims=True).astype(jnp.int32)
    k1 = jnp.sum(o1 * c1, axis=0, keepdims=True).astype(jnp.int32)
    idx = []
    for low, high in ((0, 8), (8, 16), (16, 18)):
        for r, k in ((r0, k0), (r1, k1)):
            here = (k >= low) & (k < high)
            idx.append(jnp.where(here, r * (high - low) + k - low, -1))
    none = jnp.full((1, ROWS), -1, jnp.int32)
    out_idx[...] = jnp.concatenate(idx + [none, none], axis=0)
    xv = x[...]
    gf = g[...].astype(F32)
    cots = []
    for k in range(2):
        w = jnp.sum(jnp.where(same, weights[k : k + 1, :], 0.0), axis=1, keepdims=True)
        cots.append((w * gf).astype(BF))
    both = jnp.concatenate(cots, axis=0)

    def chosen(first, n):
        r = iota((n, ROWS), 0)
        p0 = (r == idx[first]).astype(F32)
        p1 = (r == idx[first + 1]).astype(F32)
        return (
            mm((p0 + p1).astype(BF), xv),
            mm(jnp.concatenate([p0, p1], axis=1).astype(BF), both),
        )

    for first, out in ((0, out_a), (2, out_b)):
        xm, cm = chosen(first, PEERS * 8)
        pack_main(xm, out, 0, 4)
        pack_main(cm, out, 32, 4)
    xt, ct = chosen(4, PEERS * 2)
    pieces = [v[:, q * LANE : (q + 1) * LANE] for v in (xt, ct) for q in range(4)]
    tail = mm(tail_order(8), jnp.concatenate(pieces, axis=0).astype(BF))
    out_a[:, 64:80, :] = tail.astype(BF).reshape(PEERS, 16, LANE)


def chain_body(tail, tp_ref, own, left, right, far1, far2, wg, wu, wd, x, c, hid, dg, du, out):
    main = PEERS * 8
    tp = tp_ref[0]

    def at(off):
        return pl.multiple_of(((tp + off) % TPN) * 512, 512)

    if tail:
        order = tail_order_back(8)
    for off, parts in ((0, (own,)), (3, (left,)), (1, (right,)), (2, (far1, far2))):
        value = jnp.concatenate([p[...] for p in parts], axis=0) if len(parts) > 1 else parts[0][...]
        for q2 in range(4):
            lo, hi = unpack_main(value, q2)
            dest = x if q2 < 2 else c
            col = at(off) + (q2 % 2) * 256
            dest[0:main, pl.ds(col, 256)] = jnp.concatenate([lo, hi], axis=1)
        if tail:
            rows = mm(order, value[:, 64:80, :].reshape(PEERS * 16, LANE)).astype(BF)
            for q in range(8):
                dest = x if q < 4 else c
                dest[main : main + 64, pl.ds(at(off) + (q % 4) * LANE, LANE)] = rows[
                    q * 64 : (q + 1) * 64
                ]
    xv, cv = x[...], c[...]
    gate = mm(xv, wg[...])
    up = mm(xv, wu[...])
    dh = mm(cv, wd[...], 1, 1)
    sig = 1.0 / (1.0 + jnp.exp(-gate))
    silu = gate * sig
    hid[...] = (silu * up).astype(BF)
    dg[...] = (dh * up * sig * (1.0 + gate * (1.0 - sig))).astype(BF)
    du[...] = (dh * silu).astype(BF)
    dgv, duv = dg[...], du[...]
    size = 40 if tail else 32
    tails = []
    for t in range(TPN):
        part = mm(dgv, wg[t * 512 : (t + 1) * 512, :], 1, 1)
        part = part + mm(duv, wu[t * 512 : (t + 1) * 512, :], 1, 1)
        pack_main(part[:main], out, t * size, 4)
        if tail:
            pieces = [part[main:, q * LANE : (q + 1) * LANE] for q in range(4)]
            tails.append(jnp.concatenate(pieces, axis=0).astype(BF))
    if tail:
        put = mm(tail_order(4), jnp.concatenate(tails, axis=1))
        for t in range(TPN):
            out[:, t * size + 32 : t * size + 40, :] = (
                put[:, t * LANE : (t + 1) * LANE].reshape(PEERS, 8, LANE).astype(BF)
            )


def combine_body(got_a, got_b, idx, g, out):
    n = PEERS * TPN
    col = [idx[:, k : k + 1] for k in range(6)]

    def mask(code, first):
        return ((code == col[first]) | (code == col[first + 1])).astype(F32)

    m = iota((1, n * 16), 1)
    code = (m // 64) * 8 + m % 8
    half = (m // 8) % 2
    acc = [None] * 4
    for first, got in ((0, got_a), (2, got_b)):
        both = mask(code, first)
        values = [got[:, 16 * p : 16 * p + 16, :].reshape(n * 16, LANE) for p in range(2)]
        value = jnp.concatenate(values, axis=1)
        for q2 in range(2):
            r = mm(jnp.where(half == q2, both, 0.0).astype(BF), value)
            for p in range(2):
                q = 2 * p + q2
                piece = r[:, p * LANE : (p + 1) * LANE]
                acc[q] = piece if acc[q] is None else acc[q] + piece
    m = iota((1, n * 8), 1)
    both = mask((m // 32) * 2 + m % 2, 4)
    value = got_a[:, 32:40, :].reshape(n * 8, LANE)
    for q in range(4):
        acc[q] = acc[q] + mm(jnp.where((m // 2) % 4 == q, both, 0.0).astype(BF), value)
    res = (g[...].astype(F32) + jnp.concatenate(acc, axis=1)).astype(BF)
    for t in range(TPN):
        out[t] = res


def scan_body(a_ref, b_ref, cum, loc, gain, ends):
    a = a_ref[...]
    row = iota((ROWS, CH), 0)
    ca, cb = a, b_ref[...]
    step = 1
    while step < ROWS:
        ok = row >= step
        pa, pb = pltpu.roll(ca, step, 0), pltpu.roll(cb, step, 0)
        cb = jnp.where(ok, ca * pb + cb, cb)
        ca = jnp.where(ok, ca * pa, ca)
        step *= 2
    cum[...] = ca
    loc[...] = cb
    ends[0:1, :] = ca[ROWS - 1 : ROWS]
    ends[1:2, :] = cb[ROWS - 1 : ROWS]
    gn = jnp.where(row < ROWS - 1, pltpu.roll(a, ROWS - 1, 0), 1.0)
    step = 1
    while step < ROWS:
        ok = row < ROWS - step
        gn = jnp.where(ok, gn * pltpu.roll(gn, ROWS - step, 0), gn)
        step *= 2
    gain[...] = gn


def states_body(sp_ref, gains, terms, a, cum, loc, logits, q, rr, s1, gv, lru, r_out, coef):
    sp = sp_ref[0]
    row = iota((PEERS, CH), 0)
    gn = gains[...]
    fwd = jnp.where(row < sp, gn, 1.0)
    fwd = jnp.where(row < PEERS - 1, pltpu.roll(fwd, PEERS - 1, 0), 1.0)
    rev = jnp.where(row > sp, gn, 1.0)
    rev = jnp.where(row > 0, pltpu.roll(rev, 1, 0), 1.0)
    step = 1
    while step < PEERS:
        fwd = jnp.where(row < PEERS - step, fwd * pltpu.roll(fwd, PEERS - step, 0), fwd)
        rev = jnp.where(row >= step, rev * pltpu.roll(rev, step, 0), rev)
        step *= 2
    carry = jnp.sum(jnp.where(row < sp, terms[...] * fwd, 0.0), axis=0, keepdims=True)
    coef[...] = jnp.where(row > sp, rev, 0.0)
    st = loc[...] + cum[...] * carry
    wide = iota((ROWS, CH), 0)
    prev = jnp.where(wide > 0, pltpu.roll(st, 1, 0), carry)
    z = logits[...].astype(F32)
    k = 0.7978845608028654
    t = jnp.tanh(k * (z + 0.044715 * z * z * z))
    val = 0.5 * z * (1.0 + t)
    der = 0.5 * (1.0 + t) + 0.5 * z * (1.0 - t * t) * k * (1.0 + 3.0 * 0.044715 * z * z)
    s1[...] = st * der
    gv[...] = val
    lru[...] = (st * val).astype(BF)
    r_out[...] = rr[...] * (prev * a[...] - q[...])


def reverse_body(full, wout, gv, s1, lru, a_ref, gate_pre, tail_sum, send):
    mixer = mm(full[0], wout[0:512, :])
    for t in range(1, TPN):
        mixer = mixer + mm(full[t], wout[t * 512 : (t + 1) * 512, :])
    gate_pre[...] = mixer * s1[...]
    row = iota((ROWS, CH), 0)
    a = a_ref[...]
    gn = jnp.where(row < ROWS - 1, pltpu.roll(a, ROWS - 1, 0), 1.0)
    s = mixer * gv[...]
    step = 1
    while step < ROWS:
        ok = row < ROWS - step
        s = jnp.where(ok, s + gn * pltpu.roll(s, ROWS - step, 0), s)
        gn = jnp.where(ok, gn * pltpu.roll(gn, ROWS - step, 0), gn)
        step *= 2
    tail_sum[...] = s
    term = a[0:1] * s[0:1]
    hi = term.astype(BF)
    rest = term - hi.astype(F32)
    mid = rest.astype(BF)
    low = (rest - mid.astype(F32)).astype(BF)
    which = iota((8, CH), 0)
    extra = jnp.where(which == 0, hi.astype(F32), 0.0)
    extra = jnp.where(which == 1, mid.astype(F32), extra)
    extra = jnp.where(which == 2, low.astype(F32), extra).astype(BF)
    send[:, 64:72, :] = jnp.broadcast_to(extra[None], (PEERS, 8, CH))
    lv = lru[...]
    for t in range(TPN):
        part = mm(full[t], lv, 0, 0).astype(BF)
        send[8 * t : 8 * t + 8, 0:64, :] = part.reshape(8, 64, CH)


def final_body(got, coef, tail_sum, gain, rr, ad, scaled, wr, wi, out_proj, grad_in):
    acc = got[0, 0:64, :].astype(F32)
    for s in range(1, PEERS):
        acc = acc + got[s, 0:64, :].astype(F32)
    out_proj[...] = acc
    terms = jnp.sum(got[:, 64:72, :].astype(F32), axis=1)
    carry = jnp.sum(terms * coef[...], axis=0, keepdims=True)
    sg = tail_sum[...] + gain[...] * carry
    d_recall = (sg * rr[...]).astype(BF)
    d_admit = (sg * ad[...]).astype(BF)
    base = sg * scaled[...]
    for n in range(2):
        cols = slice(n * LANE, (n + 1) * LANE)
        back = mm(d_recall[:, cols], wr[n], 1, 1) + mm(d_admit[:, cols], wi[n], 1, 1)
        grad_in[:, cols] = base[:, cols] + back


RING = [(i, (i + 1) % TPN) for i in range(TPN)]
BACK = [(i, (i - 1) % TPN) for i in range(TPN)]


def ring_parts(own):
    left = lax.ppermute(own, "tp", RING)
    right = lax.ppermute(own, "tp", BACK)
    half = PEERS // 2
    far1 = lax.ppermute(left[:half], "tp", RING)
    far2 = lax.ppermute(right[half:], "tp", BACK)
    return own, left, right, far1, far2


def shape(*dims, dtype=BF):
    return jax.ShapeDtypeStruct(dims, dtype)


def expert_chain(tail, tp, parts, weights):
    rows = PEERS * (10 if tail else 8)
    size = 40 if tail else 32
    out = [shape(rows, WIDTH), shape(rows, WIDTH)] + [shape(rows, HID)] * 3
    out.append(shape(PEERS, TPN * size, LANE))

    def body(*refs):
        chain_body(tail, *refs)

    flops = 10 * rows * WIDTH * HID
    *saved, partial_value = call(body, out, 9, flops, 12 << 20, smem=(0,))(tp, *parts, *weights)
    return saved, partial_value.reshape(PEERS * TPN, size, LANE)


def per_device(
    middle_stream,
    output_gradient,
    routes,
    chosen_expert_weight,
    expert_gate_weight,
    expert_up_weight,
    expert_down_weight,
    recurrent_output_weight,
    recurrence_input,
    output_gate_logits,
    recurrence_gate_weight,
    input_gate_weight,
    channel_decay_param,
    extra_log_decay,
):
    tp = lax.axis_index("tp").reshape(1).astype(jnp.int32)
    sp = lax.axis_index("sp").reshape(1).astype(jnp.int32)
    weights = (expert_gate_weight[0], expert_up_weight[0], expert_down_weight[0])

    send_a, send_b, idx = call(
        pack_body,
        [shape(PEERS, 80, LANE), shape(PEERS, 64, LANE), shape(8, ROWS, dtype=jnp.int32)],
        4,
        1 << 30,
        3 << 20,
    )(routes.T, chosen_expert_weight.T, middle_stream, output_gradient)
    own_a = lax.all_to_all(send_a, "sp", 0, 0, tiled=True)
    own_a, send_b = lax.optimization_barrier((own_a, send_b))
    own_b = lax.all_to_all(send_b, "sp", 0, 0, tiled=True)
    parts_a = ring_parts(own_a)
    parts_b = ring_parts(own_b)

    first = lax.axis_index("tp") * 2
    recall_weight = lax.dynamic_slice_in_dim(recurrence_gate_weight, first, 2, 0)
    admit_weight = lax.dynamic_slice_in_dim(input_gate_weight, first, 2, 0)
    u_blocks = recurrence_input.reshape(ROWS, 2, LANE)

    def gate(weight):
        return jax.nn.sigmoid(
            jnp.einsum("tnb,nbc->tnc", u_blocks, weight, preferred_element_type=F32).reshape(
                ROWS, CH
            )
        )

    recall, admit = gate(recall_weight), gate(admit_weight)
    rate = -8.0 * jax.nn.softplus(-channel_decay_param)[None, :]
    log_decay = rate * recall + extra_log_decay
    decay = jnp.exp(log_decay)
    scale = jnp.sqrt(-jnp.expm1(2.0 * log_decay))
    u = recurrence_input.astype(F32)
    scaled = admit * scale
    driven = u * scaled
    minus = u * admit * decay * decay / scale
    of_recall = rate * recall * (1.0 - recall)
    of_admit = driven * (1.0 - admit)
    tile = shape(ROWS, CH, dtype=F32)
    cum, loc, gain, ends = call(
        scan_body, [tile, tile, tile, shape(2, CH, dtype=F32)], 2, 1 << 28, 1 << 20
    )(decay, driven)
    ends, own_b2 = lax.optimization_barrier((ends, own_b))
    all_ends = lax.all_to_all(
        jnp.broadcast_to(ends[None], (PEERS, 2, CH)), "sp", 0, 0, tiled=True
    )
    s1, gelu_val, lru, of_log, coef = call(
        states_body,
        [tile, tile, shape(ROWS, CH), tile, shape(PEERS, CH, dtype=F32)],
        9,
        1 << 28,
        2 << 20,
        smem=(0,),
    )(sp, all_ends[:, 0], all_ends[:, 1], decay, cum, loc, output_gate_logits, minus, of_recall)

    saved_a, part_a = expert_chain(True, tp, parts_a, weights)
    got_a = lax.all_to_all(part_a, ("sp", "tp"), 0, 0, tiled=True)
    saved_b, part_b = expert_chain(False, tp, parts_b, weights)
    got_b = lax.all_to_all(part_b, ("sp", "tp"), 0, 0, tiled=True)

    x, cot, hid, dg, du = (jnp.concatenate([a, b], axis=0) for a, b in zip(saved_a, saved_b))
    grad_gate = mm(x, dg, 0, 0).astype(BF)
    grad_up = mm(x, du, 0, 0).astype(BF)
    grad_down = mm(hid, cot, 0, 0).astype(BF)

    spread = call(combine_body, shape(TPN, ROWS, 512), 4, 1 << 31, 4 << 20)(
        got_a, got_b, idx.T, output_gradient
    )
    full = lax.all_to_all(spread, "tp", 0, 0, tiled=True)
    grad_gate_pre, tail_sum, send = call(
        reverse_body, [tile, tile, shape(PEERS, 72, CH)], 6, 1 << 30, 4 << 20
    )(full, recurrent_output_weight, gelu_val, s1, lru, decay)
    got = lax.all_to_all(send, "sp", 0, 0, tiled=True)
    grad_out_proj, grad_input = call(
        final_body, [shape(64, CH, dtype=F32), tile], 9, 1 << 28, 3 << 20
    )(got, coef, tail_sum, gain, of_log, of_admit, scaled, recall_weight, admit_weight)
    return (
        grad_gate[None],
        grad_up[None],
        grad_down[None],
        grad_out_proj,
        grad_input,
        grad_gate_pre,
    )


def solution(mesh):
    placed = (
        P("sp", "tp"),
        P("sp", "tp"),
        P("sp", None),
        P("sp", None),
        P("sp", None, "tp"),
        P("sp", None, "tp"),
        P("sp", "tp", None),
        P(None, "tp"),
        P("sp", "tp"),
        P("sp", "tp"),
        P(),
        P(),
        P("tp"),
        P("sp", "tp"),
    )
    return jax.shard_map(
        per_device,
        mesh=mesh,
        in_specs=placed,
        out_specs=(
            P("sp", None, "tp"),
            P("sp", None, "tp"),
            P("sp", "tp", None),
            P("sp", "tp"),
            P("sp", "tp"),
            P("sp", "tp"),
        ),
        check_vma=False,
    )
```

profile of v0, /device:TPU:1, one launch (start us, length us, event | category | flops | bytes accessed | tf_op | source)
XLA Modules:
  0.0 211.4 jit_solution(2239981720550943274)
XLA Ops:
  0.6 3.1 %shard_map.181 = (bf16[32,80,128]{2,1,0:T(8,128)(2,1)}, bf16[32,64,128]{2,1,0:T(8,128)(2,1)}, s32[8,192]{1,0:T(8,128)}) custom-call(s32[2,192]{1,0:T(2,128)} %bitcast.72, f32[2,192]{1,0:T(2,128)} %bitcast.73, bf16[192,512]{1,0:T(8,128)(2,1)} %x.1, bf16[192,512]{1,0:T(8,128)(2,1)} %g.3), custom_call_target="tpu_custom_call" | custom-call | flops 1073741824 | bytes 3145728 | tf_op jit(solution)/shard_map/pallas_call | solution.py:349
  3.8 22.6 %all_to_all.35.refs_1_ = bf16[32,80,128]{2,1,0:T(8,128)(2,1)S(1)} all-to-all(bf16[32,80,128]{2,1,0:T(8,128)(2,1)} %get-tuple-element.38), channel_id=1, replica_groups=mesh['sp'=32,'tp'=4] {'sp'}, dimensions={0} | all-to-all | bytes 1310720 | tf_op jit(solution)/shard_map/all_to_all | solution.py:356
  26.3 2.5 %collective-permute-start.1 = (bf16[32,80,128]{2,1,0:T(8,128)(2,1)S(1)}, bf16[32,80,128]{2,1,0:T(8,128)(2,1)S(1)}, u32[]{:S(2)}, u32[]{:S(2)}) collective-permute-start(bf16[32,80,128]{2,1,0:T(8,128)(2,1)S(1)} %all_to_all.35.refs_1_), channel_id=1, source_target_pairs={{0,3},{1,0},{2,1},{3,2},{4,7},{5,4},{6,5},{7,6},{8,11},{9,8},{10,9... | collective-permute-start | bytes 1966088 | tf_op jit(solution)/shard_map/ppermute | solution.py:304
  30.1 4.3 %all-to-all-start.1 = ((bf16[32,64,128]{2,1,0:T(8,128)(2,1)}), bf16[32,64,128]{2,1,0:T(8,128)(2,1)S(1)}, u32[]{:S(2)}, u32[]{:S(2)}) async-start(bf16[32,64,128]{2,1,0:T(8,128)(2,1)} %get-tuple-element.42), calls=%async_computation.1 | async-start | bytes 1048576 | tf_op jit(solution)/shard_map/all_to_all | solution.py:358
  34.5 7.9 %collective-permute-done.1.refs_3_ = bf16[32,80,128]{2,1,0:T(8,128)(2,1)S(1)} collective-permute-done((bf16[32,80,128]{2,1,0:T(8,128)(2,1)S(1)}, bf16[32,80,128]{2,1,0:T(8,128)(2,1)S(1)}, u32[]{:S(2)}, u32[]{:S(2)}) %collective-permute-start.1) | collective-permute-done | bytes 655392 | tf_op jit(solution)/shard_map/ppermute | solution.py:304
  42.4 3.5 %collective-permute-start.3 = (bf16[16,80,128]{2,1,0:T(8,128)(2,1)S(1)}, bf16[16,80,128]{2,1,0:T(8,128)(2,1)}, u32[]{:S(2)}, u32[]{:S(2)}) collective-permute-start(bf16[16,80,128]{2,1,0:T(8,128)(2,1)S(1)} %slice.25), channel_id=1, source_target_pairs={{0,3},{1,0},{2,1},{3,2},{4,7},{5,4},{6,5},{7,6},{8,11},{9,8},{10,9... | collective-permute-start | bytes 983048 | tf_op jit(solution)/shard_map/ppermute | solution.py:307
  48.9 2.1 shard_map.185
  51.0 1.4 broadcast_in_dim.19
  52.4 5.3 %all-to-all-start.5 = ((f32[32,2,256]{2,1,0:T(2,128)}), f32[32,2,256]{2,1,0:T(2,128)S(1)}, u32[]{:S(2)}, u32[]{:S(2)}) async-start(f32[32,2,256]{2,1,0:T(2,128)} %broadcast_in_dim.19), calls=%async_computation.5 | async-start | bytes 131072 | tf_op jit(solution)/shard_map/all_to_all | solution.py:390
  57.7 14.2 %shard_map.182 = (bf16[320,2048]{1,0:T(8,128)(2,1)}, bf16[320,2048]{1,0:T(8,128)(2,1)}, bf16[320,896]{1,0:T(8,128)(2,1)}, bf16[320,896]{1,0:T(8,128)(2,1)}, bf16...) custom-call(s32[1]{0:T(128)} %bitcast.refs_0_, bf16[32,80,128]{2,1,0:T(8,128)(2,1)} %copy-done.7, ...), custom_call_target="tpu_custom_call" | custom-call | flops 5872025600 | bytes 12582912 | tf_op jit(solution)/shard_map/pallas_call | solution.py:325
  71.9 9.4 %all-to-all-start.2 = ((bf16[128,40,128]{2,1,0:T(8,128)(2,1)}), bf16[128,40,128]{2,1,0:T(8,128)(2,1)S(1)}, u32[]{:S(2)}, u32[]{:S(2)}) async-start(bf16[128,40,128]{2,1,0:T(8,128)(2,1)} %bitcast.61), calls=%async_computation.2 | async-start | bytes 2621440 | tf_op jit(solution)/shard_map/all_to_all | solution.py:403
  81.4 2.6 %collective-permute-start.5 = (bf16[32,64,128]{2,1,0:T(8,128)(2,1)S(1)}, bf16[32,64,128]{2,1,0:T(8,128)(2,1)S(1)}, u32[]{:S(2)}, u32[]{:S(2)}) collective-permute-start(bf16[32,64,128]{2,1,0:T(8,128)(2,1)S(1)} %all-to-all-done.1.refs_1_), channel_id=1, source_target_pairs={{0,3},{1,0},{2,1},{3,2},{4,7},{5,4},{6,5},{7,6},{8,11},{9,8},{10,9... | collective-permute-start | bytes 1572872 | tf_op jit(solution)/shard_map/ppermute | solution.py:304
  84.0 24.0 %collective-permute-done.5.refs_3_ = bf16[32,64,128]{2,1,0:T(8,128)(2,1)S(1)} collective-permute-done((bf16[32,64,128]{2,1,0:T(8,128)(2,1)S(1)}, bf16[32,64,128]{2,1,0:T(8,128)(2,1)S(1)}, u32[]{:S(2)}, u32[]{:S(2)}) %collective-permute-start.5) | collective-permute-done | bytes 524320 | tf_op jit(solution)/shard_map/ppermute | solution.py:304
  109.7 5.3 %collective-permute-done.7.refs_5_ = bf16[16,64,128]{2,1,0:T(8,128)(2,1)S(1)} collective-permute-done((bf16[16,64,128]{2,1,0:T(8,128)(2,1)S(1)}, bf16[16,64,128]{2,1,0:T(8,128)(2,1)S(1)}, u32[]{:S(2)}, u32[]{:S(2)}) %collective-permute-start.7) | collective-permute-done | bytes 262176 | tf_op jit(solution)/shard_map/ppermute | solution.py:307
  115.0 2.0 collective-permute-done.6.refs_4_
  117.7 11.8 %shard_map.183 = (bf16[256,2048]{1,0:T(8,128)(2,1)}, bf16[256,2048]{1,0:T(8,128)(2,1)}, bf16[256,896]{1,0:T(8,128)(2,1)}, bf16[256,896]{1,0:T(8,128)(2,1)}, bf16...) custom-call(s32[1]{0:T(128)} %bitcast.refs_0_, bf16[32,64,128]{2,1,0:T(8,128)(2,1)} %copy-done.8, ...), custom_call_target="tpu_custom_call" | custom-call | flops 4697620480 | bytes 12582912 | tf_op jit(solution)/shard_map/pallas_call | solution.py:325
  129.5 9.8 %all-to-all-start.3 = ((bf16[128,32,128]{2,1,0:T(8,128)(2,1)}), bf16[128,32,128]{2,1,0:T(8,128)(2,1)S(1)}, u32[]{:S(2)}, u32[]{:S(2)}) async-start(bf16[128,32,128]{2,1,0:T(8,128)(2,1)} %bitcast.62), calls=%async_computation.3 | async-start | bytes 2097152 | tf_op jit(solution)/shard_map/all_to_all | solution.py:405
  141.3 2.3 %shard_map.186 = (f32[192,256]{1,0:T(8,128)}, f32[192,256]{1,0:T(8,128)}, bf16[192,256]{1,0:T(8,128)(2,1)}, f32[192,256]{1,0:T(8,128)}, f32[32,256]{1,0:T(8,128)}) custom-call(s32[1]{0:T(128)} %bitcast.12.sp_ref, f32[32,256]{1,0:T(8,128)} %bitcast.64, f32[32,256]{1,0:T(8,128)} %bitcast.63, f32[192,256]{1,0:T(8,128)} %get-tuple-element.76.a_ref.a, ...), custom_call_target="tpu_custom_call" | custom-call | flops 268435456 | bytes 2097152 | tf_op jit(solution)/shard_map/pallas_call | solution.py:393
  143.6 15.2 %all-to-all-done.3.got_b = bf16[128,32,128]{2,1,0:T(8,128)(2,1)S(1)} async-done(((bf16[128,32,128]{2,1,0:T(8,128)(2,1)}), bf16[128,32,128]{2,1,0:T(8,128)(2,1)S(1)}, u32[]{:S(2)}, u32[]{:S(2)}) %all-to-all-start.3) | async-done | bytes 1048608 | tf_op jit(solution)/shard_map/all_to_all | solution.py:405
  159.8 4.0 %shard_map.184 = bf16[4,192,512]{2,1,0:T(8,128)(2,1)} custom-call(bf16[128,40,128]{2,1,0:T(8,128)(2,1)} %copy-done.2, bf16[128,32,128]{2,1,0:T(8,128)(2,1)} %copy-done.4, s32[192,8]{1,0:T(8,128)} %bitcast.65, bf16[192,512]{1,0:T(8,128)(2,1)} %g.3), custom_call_target="tpu_custom_call" | custom-call | flops 2147483648 | bytes 4194304 | tf_op jit(solution)/shard_map/pallas_call | solution.py:412
  163.8 3.6 %all-to-all-start.4 = ((bf16[4,192,512]{2,1,0:T(8,128)(2,1)}), bf16[4,192,512]{2,1,0:T(8,128)(2,1)S(1)}, u32[]{:S(2)}, u32[]{:S(2)}) async-start(bf16[4,192,512]{2,1,0:T(8,128)(2,1)} %shard_map.184), calls=%async_computation.4 | async-start | bytes 1572864 | tf_op jit(solution)/shard_map/all_to_all | solution.py:415
  167.5 1.1 constant_dynamic-update-slice_fusion.1
  169.4 5.6 %convert_bitcast_fusion = bf16[1,896,2048]{2,1,0:T(8,128)(2,1)} fusion(bf16[256,2048]{1,0:T(8,128)(2,1)S(1)} %copy-done.20, bf16[320,2048]{1,0:T(8,128)(2,1)S(1)} %copy-done.24, bf16[256,896]{1,0:T(8,128)(2,1)S(1)} %copy-done.23, bf16[320,896]{1,0:T(8,128)(2,1)} %get-tuple-element.48), kind=kOutput, calls=%fused_computation | convolution fusion | flops 2122547200 | bytes 7061504 | tf_op jit(solution)/shard_map/dot_general | solution.py:22
  174.9 4.5 %all-to-all-done.4.full = bf16[4,192,512]{2,1,0:T(8,128)(2,1)S(1)} async-done(((bf16[4,192,512]{2,1,0:T(8,128)(2,1)}), bf16[4,192,512]{2,1,0:T(8,128)(2,1)S(1)}, u32[]{:S(2)}, u32[]{:S(2)}) %all-to-all-start.4) | async-done | bytes 786464 | tf_op jit(solution)/shard_map/all_to_all | solution.py:415
  180.3 3.6 %shard_map.187 = (f32[192,256]{1,0:T(8,128)}, f32[192,256]{1,0:T(8,128)}, bf16[32,72,256]{2,1,0:T(8,128)(2,1)}) custom-call(bf16[4,192,512]{2,1,0:T(8,128)(2,1)} %copy-done.5, bf16[2048,256]{1,0:T(8,128)(2,1)} %wout.1, f32[192,256]{1,0:T(8,128)} %get-tuple-element.59.gv, f32[192,256]{1,0:T(8,128)} %get-tuple-element.60.s1, ...), custom_call_target="tpu_custom_call" | custom-call | flops 1073741824 | bytes 4194304 | tf_op jit(solution)/shard_map/pallas_call | solution.py:416
  183.9 5.2 %all-to-all-start.6 = ((bf16[32,72,256]{2,1,0:T(8,128)(2,1)}), bf16[32,72,256]{2,1,0:T(8,128)(2,1)S(1)}, u32[]{:S(2)}, u32[]{:S(2)}) async-start(bf16[32,72,256]{2,1,0:T(8,128)(2,1)} %get-tuple-element.62), calls=%async_computation.6 | async-start | bytes 2359296 | tf_op jit(solution)/shard_map/all_to_all | solution.py:419
  189.1 1.0 constant_dynamic-update-slice_fusion
  190.1 7.0 %convert_bitcast_fusion.1 = bf16[1,2048,896]{2,1,0:T(8,128)(2,1)} fusion(bf16[576,2048]{1,0:T(8,128)(2,1)} %constant_dynamic-update-slice_fusion, bf16[256,896]{1,0:T(8,128)(2,1)S(1)} %copy-done.22, bf16[320,896]{1,0:T(8,128)(2,1)S(1)} %copy-done.26), kind=kOutput, calls=%fused_computation.1 | convolution fusion | flops 2117828608 | bytes 7061504 | tf_op jit(solution)/shard_map/dot_general | solution.py:22
  197.2 4.8 %convert_bitcast_fusion.2 = bf16[1,2048,896]{2,1,0:T(8,128)(2,1)} fusion(bf16[576,2048]{1,0:T(8,128)(2,1)S(1)} %copy-done.6, bf16[256,896]{1,0:T(8,128)(2,1)S(1)} %copy-done.21, bf16[320,896]{1,0:T(8,128)(2,1)S(1)} %copy-done.25), kind=kOutput, calls=%fused_computation.2 | convolution fusion | flops 2117828608 | bytes 7061504 | tf_op jit(solution)/shard_map/dot_general | solution.py:22
  202.0 5.7 %all-to-all-done.6.got = bf16[32,72,256]{2,1,0:T(8,128)(2,1)S(1)} async-done(((bf16[32,72,256]{2,1,0:T(8,128)(2,1)}), bf16[32,72,256]{2,1,0:T(8,128)(2,1)S(1)}, u32[]{:S(2)}, u32[]{:S(2)}) %all-to-all-start.6) | async-done | bytes 1179680 | tf_op jit(solution)/shard_map/all_to_all | solution.py:419
  207.7 1.1 copy-done
  208.8 2.6 %shard_map.188 = (f32[64,256]{1,0:T(8,128)}, f32[192,256]{1,0:T(8,128)}) custom-call(bf16[32,72,256]{2,1,0:T(8,128)(2,1)} %copy-done, f32[32,256]{1,0:T(8,128)} %get-tuple-element.63.coef, f32[192,256]{1,0:T(8,128)} %get-tuple-element.64.tail_sum, f32[192,256]{1,0:T(8,128)} %get-tuple-element.65.gain, f32[192,256]{1,0:T(8,128)} %get-tuple-element.66.rr, ...), custom_call_target="tpu_custom_call" | custom-call | flops 268435456 | bytes 3145728 | tf_op jit(solution)/shard_map/pallas_call | solution.py:420
  (79 shorter events, 11.4 us)
Async XLA Ops:
  0.6 29.1 %copy-start.9 = (bf16[192,256]{1,0:T(8,128)(2,1)S(1)}, bf16[192,256]{1,0:T(8,128)(2,1)}, u32[]{:S(2)}) copy-start(bf16[192,256]{1,0:T(8,128)(2,1)} %param.22) | copy-start | bytes 294916
  3.7 26.4 %copy-start.17 = (f32[256]{0:T(256)S(1)}, f32[256]{0:T(256)}, u32[]{:S(2)}) copy-start(f32[256]{0:T(256)} %param.26) | copy-start | bytes 3076
  26.3 21.7 %copy-start.7 = (bf16[32,80,128]{2,1,0:T(8,128)(2,1)}, bf16[32,80,128]{2,1,0:T(8,128)(2,1)S(1)}, u32[]{:S(2)}) copy-start(bf16[32,80,128]{2,1,0:T(8,128)(2,1)S(1)} %all_to_all.35.refs_1_) | copy-start | bytes 1966084
  26.3 20.7 %copy-start.12 = (f32[192,256]{1,0:T(8,128)S(1)}, f32[192,256]{1,0:T(8,128)}, u32[]{:S(2)}) copy-start(f32[192,256]{1,0:T(8,128)} %param.27) | copy-start | bytes 589828
  26.3 16.1 %collective-permute-start.1 = (bf16[32,80,128]{2,1,0:T(8,128)(2,1)S(1)}, bf16[32,80,128]{2,1,0:T(8,128)(2,1)S(1)}, u32[]{:S(2)}, u32[]{:S(2)}) collective-permute-start(bf16[32,80,128]{2,1,0:T(8,128)(2,1)S(1)} %all_to_all.35.refs_1_), channel_id=1, source_target_pairs={{0,3},{1,0},{2,1},{3,2},{4,7},{5,4},{6,5},{7,6},{8,11},{9,8},{10,9... | collective-permute-start | bytes 1966088 | tf_op jit(solution)/shard_map/ppermute | solution.py:304
  28.8 17.1 %collective-permute-start = (bf16[32,80,128]{2,1,0:T(8,128)(2,1)S(1)}, bf16[32,80,128]{2,1,0:T(8,128)(2,1)}, u32[]{:S(2)}, u32[]{:S(2)}) collective-permute-start(bf16[32,80,128]{2,1,0:T(8,128)(2,1)S(1)} %all_to_all.35.refs_1_), channel_id=1, source_target_pairs={{0,1},{1,2},{2,3},{3,0},{4,5},{5,6},{6,7},{7,4},{8,9},{9,10},{10,1... | collective-permute-start | bytes 1966088 | tf_op jit(solution)/shard_map/ppermute | solution.py:303
  29.7 18.4 %copy-start.10 = (bf16[2,128,128]{2,1,0:T(8,128)(2,1)}, bf16[2,128,128]{2,1,0:T(8,128)(2,1)S(1)}, u32[]{:S(2)}) copy-start(bf16[2,128,128]{2,1,0:T(8,128)(2,1)S(1)} %get-tuple-element.79.wi) | copy-start | bytes 196612
  29.7 18.4 %copy-start.11 = (bf16[2,128,128]{2,1,0:T(8,128)(2,1)}, bf16[2,128,128]{2,1,0:T(8,128)(2,1)S(1)}, u32[]{:S(2)}) copy-start(bf16[2,128,128]{2,1,0:T(8,128)(2,1)S(1)} %get-tuple-element.80.wr) | copy-start | bytes 196612
  30.1 20.9 %all-to-all-start.1 = ((bf16[32,64,128]{2,1,0:T(8,128)(2,1)}), bf16[32,64,128]{2,1,0:T(8,128)(2,1)S(1)}, u32[]{:S(2)}, u32[]{:S(2)}) async-start(bf16[32,64,128]{2,1,0:T(8,128)(2,1)} %get-tuple-element.42), calls=%async_computation.1 | async-start | bytes 1048576 | tf_op jit(solution)/shard_map/all_to_all | solution.py:358
  42.4 8.6 %copy-start.13 = (bf16[32,80,128]{2,1,0:T(8,128)(2,1)}, bf16[32,80,128]{2,1,0:T(8,128)(2,1)S(1)}, u32[]{:S(2)}) copy-start(bf16[32,80,128]{2,1,0:T(8,128)(2,1)S(1)} %collective-permute-done.1.refs_3_) | copy-start | bytes 1966084
  42.4 15.3 %collective-permute-start.3 = (bf16[16,80,128]{2,1,0:T(8,128)(2,1)S(1)}, bf16[16,80,128]{2,1,0:T(8,128)(2,1)}, u32[]{:S(2)}, u32[]{:S(2)}) collective-permute-start(bf16[16,80,128]{2,1,0:T(8,128)(2,1)S(1)} %slice.25), channel_id=1, source_target_pairs={{0,3},{1,0},{2,1},{3,2},{4,7},{5,4},{6,5},{7,6},{8,11},{9,8},{10,9... | collective-permute-start | bytes 983048 | tf_op jit(solution)/shard_map/ppermute | solution.py:307
  46.9 10.8 %collective-permute-start.2 = (bf16[16,80,128]{2,1,0:T(8,128)(2,1)S(1)}, bf16[16,80,128]{2,1,0:T(8,128)(2,1)}, u32[]{:S(2)}, u32[]{:S(2)}) collective-permute-start(bf16[16,80,128]{2,1,0:T(8,128)(2,1)S(1)} %slice.24), channel_id=1, source_target_pairs={{0,1},{1,2},{2,3},{3,0},{4,5},{5,6},{6,7},{7,4},{8,9},{9,10},{10,1... | collective-permute-start | bytes 983048 | tf_op jit(solution)/shard_map/ppermute | solution.py:306
  51.0 33.0 %copy-start.8 = (bf16[32,64,128]{2,1,0:T(8,128)(2,1)}, bf16[32,64,128]{2,1,0:T(8,128)(2,1)S(1)}, u32[]{:S(2)}) copy-start(bf16[32,64,128]{2,1,0:T(8,128)(2,1)S(1)} %all-to-all-done.1.refs_1_) | copy-start | bytes 1572868
  52.4 19.5 %all-to-all-start.5 = ((f32[32,2,256]{2,1,0:T(2,128)}), f32[32,2,256]{2,1,0:T(2,128)S(1)}, u32[]{:S(2)}, u32[]{:S(2)}) async-start(f32[32,2,256]{2,1,0:T(2,128)} %broadcast_in_dim.19), calls=%async_computation.5 | async-start | bytes 131072 | tf_op jit(solution)/shard_map/all_to_all | solution.py:390
  71.9 57.5 %all-to-all-start.2 = ((bf16[128,40,128]{2,1,0:T(8,128)(2,1)}), bf16[128,40,128]{2,1,0:T(8,128)(2,1)S(1)}, u32[]{:S(2)}, u32[]{:S(2)}) async-start(bf16[128,40,128]{2,1,0:T(8,128)(2,1)} %bitcast.61), calls=%async_computation.2 | async-start | bytes 2621440 | tf_op jit(solution)/shard_map/all_to_all | solution.py:403
  81.4 26.6 %collective-permute-start.5 = (bf16[32,64,128]{2,1,0:T(8,128)(2,1)S(1)}, bf16[32,64,128]{2,1,0:T(8,128)(2,1)S(1)}, u32[]{:S(2)}, u32[]{:S(2)}) collective-permute-start(bf16[32,64,128]{2,1,0:T(8,128)(2,1)S(1)} %all-to-all-done.1.refs_1_), channel_id=1, source_target_pairs={{0,3},{1,0},{2,1},{3,2},{4,7},{5,4},{6,5},{7,6},{8,11},{9,8},{10,9... | collective-permute-start | bytes 1572872 | tf_op jit(solution)/shard_map/ppermute | solution.py:304
  84.0 25.2 %collective-permute-start.4 = (bf16[32,64,128]{2,1,0:T(8,128)(2,1)S(1)}, bf16[32,64,128]{2,1,0:T(8,128)(2,1)S(1)}, u32[]{:S(2)}, u32[]{:S(2)}) collective-permute-start(bf16[32,64,128]{2,1,0:T(8,128)(2,1)S(1)} %all-to-all-done.1.refs_1_), channel_id=1, source_target_pairs={{0,1},{1,2},{2,3},{3,0},{4,5},{5,6},{6,7},{7,4},{8,9},{9,10},{10,1... | collective-permute-start | bytes 1572872 | tf_op jit(solution)/shard_map/ppermute | solution.py:303
  108.0 9.0 %copy-start.14 = (bf16[32,64,128]{2,1,0:T(8,128)(2,1)}, bf16[32,64,128]{2,1,0:T(8,128)(2,1)S(1)}, u32[]{:S(2)}) copy-start(bf16[32,64,128]{2,1,0:T(8,128)(2,1)S(1)} %collective-permute-done.5.refs_3_) | copy-start | bytes 1572868
  108.0 7.0 %collective-permute-start.7 = (bf16[16,64,128]{2,1,0:T(8,128)(2,1)S(1)}, bf16[16,64,128]{2,1,0:T(8,128)(2,1)S(1)}, u32[]{:S(2)}, u32[]{:S(2)}) collective-permute-start(bf16[16,64,128]{2,1,0:T(8,128)(2,1)S(1)} %slice.27), channel_id=1, source_target_pairs={{0,3},{1,0},{2,1},{3,2},{4,7},{5,4},{6,5},{7,6},{8,11},{9,8},{10,9... | collective-permute-start | bytes 786440 | tf_op jit(solution)/shard_map/ppermute | solution.py:307
  109.2 7.7 %copy-start.15 = (bf16[32,64,128]{2,1,0:T(8,128)(2,1)}, bf16[32,64,128]{2,1,0:T(8,128)(2,1)S(1)}, u32[]{:S(2)}) copy-start(bf16[32,64,128]{2,1,0:T(8,128)(2,1)S(1)} %collective-permute-done.4.refs_2_) | copy-start | bytes 1572868
  109.3 30.0 %copy-start.16 = (s32[8,192]{1,0:T(8,128)S(1)}, s32[8,192]{1,0:T(8,128)}, u32[]{:S(2)}) copy-start(s32[8,192]{1,0:T(8,128)} %get-tuple-element.54) | copy-start | bytes 18436
  109.3 7.7 %collective-permute-start.6 = (bf16[16,64,128]{2,1,0:T(8,128)(2,1)S(1)}, bf16[16,64,128]{2,1,0:T(8,128)(2,1)S(1)}, u32[]{:S(2)}, u32[]{:S(2)}) collective-permute-start(bf16[16,64,128]{2,1,0:T(8,128)(2,1)S(1)} %slice.26), channel_id=1, source_target_pairs={{0,1},{1,2},{2,3},{3,0},{4,5},{5,6},{6,7},{7,4},{8,9},{9,10},{10,1... | collective-permute-start | bytes 786440 | tf_op jit(solution)/shard_map/ppermute | solution.py:306
  129.5 29.3 %copy-start.2 = (bf16[128,40,128]{2,1,0:T(8,128)(2,1)}, bf16[128,40,128]{2,1,0:T(8,128)(2,1)S(1)}, u32[]{:S(2)}) copy-start(bf16[128,40,128]{2,1,0:T(8,128)(2,1)S(1)} %all-to-all-done.2.got_a) | copy-start | bytes 3932164
  129.5 29.3 %all-to-all-start.3 = ((bf16[128,32,128]{2,1,0:T(8,128)(2,1)}), bf16[128,32,128]{2,1,0:T(8,128)(2,1)S(1)}, u32[]{:S(2)}, u32[]{:S(2)}) async-start(bf16[128,32,128]{2,1,0:T(8,128)(2,1)} %bitcast.62), calls=%async_computation.3 | async-start | bytes 2097152 | tf_op jit(solution)/shard_map/all_to_all | solution.py:405
  163.8 15.6 %all-to-all-start.4 = ((bf16[4,192,512]{2,1,0:T(8,128)(2,1)}), bf16[4,192,512]{2,1,0:T(8,128)(2,1)S(1)}, u32[]{:S(2)}, u32[]{:S(2)}) async-start(bf16[4,192,512]{2,1,0:T(8,128)(2,1)} %shard_map.184), calls=%async_computation.4 | async-start | bytes 1572864 | tf_op jit(solution)/shard_map/all_to_all | solution.py:415
  180.3 8.8 %copy-start.3 = (bf16[256,2048]{1,0:T(8,128)(2,1)S(1)}, bf16[256,2048]{1,0:T(8,128)(2,1)}, u32[]{:S(2)}) copy-start(bf16[256,2048]{1,0:T(8,128)(2,1)} %get-tuple-element.43) | copy-start | bytes 3145732
  183.9 6.2 %copy-start.22 = (bf16[256,896]{1,0:T(8,128)(2,1)S(1)}, bf16[256,896]{1,0:T(8,128)(2,1)}, u32[]{:S(2)}) copy-start(bf16[256,896]{1,0:T(8,128)(2,1)} %get-tuple-element.47) | copy-start | bytes 1376260
  183.9 6.2 %copy-start.26 = (bf16[320,896]{1,0:T(8,128)(2,1)S(1)}, bf16[320,896]{1,0:T(8,128)(2,1)}, u32[]{:S(2)}) copy-start(bf16[320,896]{1,0:T(8,128)(2,1)} %get-tuple-element.46) | copy-start | bytes 1720324
  183.9 23.8 %all-to-all-start.6 = ((bf16[32,72,256]{2,1,0:T(8,128)(2,1)}), bf16[32,72,256]{2,1,0:T(8,128)(2,1)S(1)}, u32[]{:S(2)}, u32[]{:S(2)}) async-start(bf16[32,72,256]{2,1,0:T(8,128)(2,1)} %get-tuple-element.62), calls=%async_computation.6 | async-start | bytes 2359296 | tf_op jit(solution)/shard_map/all_to_all | solution.py:419
  190.1 7.0 %copy-start.6 = (bf16[576,2048]{1,0:T(8,128)(2,1)S(1)}, bf16[576,2048]{1,0:T(8,128)(2,1)}, u32[]{:S(2)}) copy-start(bf16[576,2048]{1,0:T(8,128)(2,1)} %constant_dynamic-update-slice_fusion) | copy-start | bytes 7077892
  190.1 7.0 %copy-start.21 = (bf16[256,896]{1,0:T(8,128)(2,1)S(1)}, bf16[256,896]{1,0:T(8,128)(2,1)}, u32[]{:S(2)}) copy-start(bf16[256,896]{1,0:T(8,128)(2,1)} %get-tuple-element.45) | copy-start | bytes 1376260
  190.1 7.0 %copy-start.25 = (bf16[320,896]{1,0:T(8,128)(2,1)S(1)}, bf16[320,896]{1,0:T(8,128)(2,1)}, u32[]{:S(2)}) copy-start(bf16[320,896]{1,0:T(8,128)(2,1)} %get-tuple-element.44) | copy-start | bytes 1720324
  (9 other events, 17.2 us)
where the time goes:
time: 212 us; the launch traced here: 211 us
  waiting for transfers between devices  65 us (31%)
  starting transfers between devices  47.5 us (22%)
  Pallas kernels  43.7 us (21%)
  blocking collectives  22.6 us (11%)
  matrix products  17.8 us (8%)
  local copies, waits for them, and re-layouts  12 us (6%)
    ppermute x2, waiting for transfers between devices, ring_parts(): right = lax.ppermute(own, 'tp', BACK)  31.9 us
    pallas_call x2, Pallas kernels, expert_chain(): call(body, out, 9, flops, 12 << 20, smem=(0,))(tp, *parts, *weights)  26 us
    all_to_all x1, blocking collectives, per_device(): own_a = lax.all_to_all(send_a, 'sp', 0, 0, tiled=True)  22.6 us
    dot_general x3, matrix products, mm(): lax.dot_general(a, b, (((ca,), (cb,)), ((), ())), preferred_element_type=...  17.4 us
    all_to_all x1, waiting for transfers between devices, per_device(): got_b = lax.all_to_all(part_b, ('sp', 'tp'), 0, 0, tiled=True)  15.2 us
    all_to_all x1, starting transfers between devices, per_device(): got_b = lax.all_to_all(part_b, ('sp', 'tp'), 0, 0, tiled=True)  9.78 us
    all_to_all x1, starting transfers between devices, per_device(): got_a = lax.all_to_all(part_a, ('sp', 'tp'), 0, 0, tiled=True)  9.44 us
    unnamed x57, local copies, waits for them, and re-layouts  6.83 us
  transfers between devices with their start and end apart: 14, of which 8 were waited for; matrix products, arithmetic and copies ran while one was open for 13% of the time, Pallas kernels for 14%

commit v1 on v0

--- a/solution.py
+++ b/solution.py
@@ -16,6 +16,7 @@
 WIDTH = 2048
 VMEM = pl.BlockSpec(memory_space=pltpu.VMEM)
 SMEM = pl.BlockSpec(memory_space=pltpu.SMEM)
+HBM = pl.BlockSpec(memory_space=pltpu.HBM)
 
 
 def mm(a, b, ca=1, cb=0):
@@ -26,15 +27,21 @@
     return lax.broadcasted_iota(jnp.int32, shape, dim)
 
 
-def call(body, out, n_in, flops, moved, smem=()):
+def call(body, out, n_in, flops, moved, mib=56, smem=(), far=(), far_out=(), scratch=()):
+    kinds = {**dict.fromkeys(smem, SMEM), **dict.fromkeys(far, HBM)}
     return pl.pallas_call(
         body,
         out_shape=out,
-        in_specs=[SMEM if k in smem else VMEM for k in range(n_in)],
-        out_specs=jax.tree.map(lambda _: VMEM, out),
+        in_specs=[kinds.get(k, VMEM) for k in range(n_in)],
+        out_specs=[HBM if k in far_out else VMEM for k in range(len(out))],
+        scratch_shapes=list(scratch),
         cost_estimate=pl.CostEstimate(flops=flops, bytes_accessed=moved, transcendentals=0),
-        compiler_params=pltpu.CompilerParams(vmem_limit_bytes=56 * 1024 * 1024),
+        compiler_params=pltpu.CompilerParams(vmem_limit_bytes=mib * 1024 * 1024),
     )
+
+
+def dma(count):
+    return pltpu.SemaphoreType.DMA((count,))
 
 
 def pack_main(block, out, base, pieces):
@@ -112,8 +119,34 @@
     out_a[:, 64:80, :] = tail.astype(BF).reshape(PEERS, 16, LANE)
 
 
-def chain_body(tail, tp_ref, own, left, right, far1, far2, wg, wu, wd, x, c, hid, dg, du, out):
+def chain_body(tail, tp_ref, *refs):
+    parts, weights, outs, rest = refs[:7], refs[7:10], refs[10:16], refs[16:]
+    values, x, c, hid, dg, du, out, wg, wu, wd, sem_in, sem_w, sem_out = rest
     main = PEERS * 8
+    half = PEERS // 2
+    depth = 80 if tail else 64
+    size = 40 if tail else 32
+    places = [values.at[0]] + [values.at[s, pl.ds(h * half, half)] for s in (1, 2, 3) for h in (0, 1)]
+    fetch = [
+        pltpu.make_async_copy(p.at[:, 0:depth] if k == 0 else p, place, sem_in.at[k])
+        for k, (p, place) in enumerate(zip(parts, places))
+    ]
+    loads = [
+        pltpu.make_async_copy(w, v, sem_w.at[k])
+        for k, (w, v) in enumerate(zip(weights, (wg, wu, wd)))
+    ]
+    for copy in fetch + loads:
+        copy.start()
+    saves = [
+        pltpu.make_async_copy(v, o, sem_out.at[k])
+        for k, (v, o) in enumerate(zip((x, c, hid, dg, du), outs))
+    ]
+    saves += [
+        pltpu.make_async_copy(
+            out.at[:, t * size : (t + 1) * size], outs[5].at[:, t * size : (t + 1) * size], sem_out.at[5 + t]
+        )
+        for t in range(TPN)
+    ]
     tp = tp_ref[0]
 
     def at(off):
@@ -121,8 +154,10 @@
 
     if tail:
         order = tail_order_back(8)
-    for off, parts in ((0, (own,)), (3, (left,)), (1, (right,)), (2, (far1, far2))):
-        value = jnp.concatenate([p[...] for p in parts], axis=0) if len(parts) > 1 else parts[0][...]
+    for source, (off, arriving) in enumerate(((0, (0,)), (3, (1, 2)), (1, (3, 4)), (2, (5, 6)))):
+        for k in arriving:
+            fetch[k].wait()
+        value = values[source]
         for q2 in range(4):
             lo, hi = unpack_main(value, q2)
             dest = x if q2 < 2 else c
@@ -135,65 +170,84 @@
                 dest[main : main + 64, pl.ds(at(off) + (q % 4) * LANE, LANE)] = rows[
                     q * 64 : (q + 1) * 64
                 ]
+    saves[0].start()
+    saves[1].start()
     xv, cv = x[...], c[...]
+    loads[0].wait()
     gate = mm(xv, wg[...])
+    loads[1].wait()
     up = mm(xv, wu[...])
+    loads[2].wait()
     dh = mm(cv, wd[...], 1, 1)
     sig = 1.0 / (1.0 + jnp.exp(-gate))
     silu = gate * sig
     hid[...] = (silu * up).astype(BF)
     dg[...] = (dh * up * sig * (1.0 + gate * (1.0 - sig))).astype(BF)
     du[...] = (dh * silu).astype(BF)
+    for k in (2, 3, 4):
+        saves[k].start()
     dgv, duv = dg[...], du[...]
-    size = 40 if tail else 32
-    tails = []
+    if tail:
+        order = tail_order(4)
     for t in range(TPN):
         part = mm(dgv, wg[t * 512 : (t + 1) * 512, :], 1, 1)
         part = part + mm(duv, wu[t * 512 : (t + 1) * 512, :], 1, 1)
         pack_main(part[:main], out, t * size, 4)
         if tail:
             pieces = [part[main:, q * LANE : (q + 1) * LANE] for q in range(4)]
-            tails.append(jnp.concatenate(pieces, axis=0).astype(BF))
-    if tail:
-        put = mm(tail_order(4), jnp.concatenate(tails, axis=1))
-        for t in range(TPN):
-            out[:, t * size + 32 : t * size + 40, :] = (
-                put[:, t * LANE : (t + 1) * LANE].reshape(PEERS, 8, LANE).astype(BF)
-            )
-
-
-def combine_body(got_a, got_b, idx, g, out):
+            put = mm(order, jnp.concatenate(pieces, axis=0).astype(BF))
+            out[:, t * size + 32 : t * size + 40, :] = put.reshape(PEERS, 8, LANE).astype(BF)
+        saves[5 + t].start()
+    for save in saves:
+        save.wait()
+
+
+def slot_mask(idx, code, first):
+    at0, at1 = idx[:, first : first + 1], idx[:, first + 1 : first + 2]
+    return ((code == at0) | (code == at1)).astype(F32)
+
+
+def add_main(got, idx, first):
     n = PEERS * TPN
-    col = [idx[:, k : k + 1] for k in range(6)]
-
-    def mask(code, first):
-        return ((code == col[first]) | (code == col[first + 1])).astype(F32)
-
     m = iota((1, n * 16), 1)
-    code = (m // 64) * 8 + m % 8
+    both = slot_mask(idx, (m // 64) * 8 + m % 8, first)
     half = (m // 8) % 2
-    acc = [None] * 4
-    for first, got in ((0, got_a), (2, got_b)):
-        both = mask(code, first)
-        values = [got[:, 16 * p : 16 * p + 16, :].reshape(n * 16, LANE) for p in range(2)]
-        value = jnp.concatenate(values, axis=1)
-        for q2 in range(2):
-            r = mm(jnp.where(half == q2, both, 0.0).astype(BF), value)
-            for p in range(2):
-                q = 2 * p + q2
-                piece = r[:, p * LANE : (p + 1) * LANE]
-                acc[q] = piece if acc[q] is None else acc[q] + piece
+    values = [got[:, 16 * p : 16 * p + 16, :].reshape(n * 16, LANE) for p in range(2)]
+    value = jnp.concatenate(values, axis=1)
+    even, odd = [mm(jnp.where(half == k, both, 0.0).astype(BF), value) for k in range(2)]
+    return [even[:, :LANE], odd[:, :LANE], even[:, LANE:], odd[:, LANE:]]
+
+
+def combine_a_body(got, idx, g, out):
+    n = PEERS * TPN
+    acc = add_main(got, idx, 0)
     m = iota((1, n * 8), 1)
-    both = mask((m // 32) * 2 + m % 2, 4)
-    value = got_a[:, 32:40, :].reshape(n * 8, LANE)
+    both = slot_mask(idx, (m // 32) * 2 + m % 2, 4)
+    value = got[:, 32:40, :].reshape(n * 8, LANE)
     for q in range(4):
         acc[q] = acc[q] + mm(jnp.where((m // 2) % 4 == q, both, 0.0).astype(BF), value)
-    res = (g[...].astype(F32) + jnp.concatenate(acc, axis=1)).astype(BF)
-    for t in range(TPN):
-        out[t] = res
-
-
-def scan_body(a_ref, b_ref, cum, loc, gain, ends):
+    out[...] = g[...].astype(F32) + jnp.concatenate(acc, axis=1)
+
+
+def combine_b_body(got, idx, so_far, out, res, sem):
+    acc = add_main(got, idx, 2)
+    res[...] = (so_far[...] + jnp.concatenate(acc, axis=1)).astype(BF)
+    copies = [pltpu.make_async_copy(res, out.at[t], sem.at[t]) for t in range(TPN)]
+    for copy in copies:
+        copy.start()
+    for copy in copies:
+        copy.wait()
+
+
+def in_three(v):
+    hi = v.astype(BF)
+    rest = v - hi.astype(F32)
+    mid = rest.astype(BF)
+    low = (rest - mid.astype(F32)).astype(BF)
+    return [p.astype(F32) for p in (hi, mid, low)]
+
+
+def scan_body(a_ref, b_ref, rows_b, cum, loc, gain, send):
     a = a_ref[...]
     row = iota((ROWS, CH), 0)
     ca, cb = a, b_ref[...]
@@ -206,8 +260,15 @@
         step *= 2
     cum[...] = ca
     loc[...] = cb
-    ends[0:1, :] = ca[ROWS - 1 : ROWS]
-    ends[1:2, :] = cb[ROWS - 1 : ROWS]
+    lines = []
+    for v in (ca[ROWS - 1 : ROWS], cb[ROWS - 1 : ROWS]):
+        pieces = in_three(v)
+        for h in range(2):
+            lines += [p[:, h * LANE : (h + 1) * LANE] for p in pieces]
+    lines.append(jnp.zeros((4, LANE), F32))
+    extra = jnp.concatenate(lines, axis=0).astype(BF)
+    send[:, 0:64, :] = rows_b[...]
+    send[:, 64:80, :] = jnp.broadcast_to(extra[None], (PEERS, 16, LANE))
     gn = jnp.where(row < ROWS - 1, pltpu.roll(a, ROWS - 1, 0), 1.0)
     step = 1
     while step < ROWS:
@@ -217,10 +278,14 @@
     gain[...] = gn
 
 
-def states_body(sp_ref, gains, terms, a, cum, loc, logits, q, rr, s1, gv, lru, r_out, coef):
+def states_body(sp_ref, got, a, cum, loc, logits, q, rr, s1, gv, lru, r_out, coef):
     sp = sp_ref[0]
     row = iota((PEERS, CH), 0)
-    gn = gains[...]
+    ends = got[:, 64:80, :].astype(F32)
+    line = iota((PEERS, 16, LANE), 1)
+    halves = [jnp.sum(jnp.where(line // 3 == k, ends, 0.0), axis=1) for k in range(4)]
+    gn = jnp.concatenate(halves[:2], axis=1)
+    terms = jnp.concatenate(halves[2:], axis=1)
     fwd = jnp.where(row < sp, gn, 1.0)
     fwd = jnp.where(row < PEERS - 1, pltpu.roll(fwd, PEERS - 1, 0), 1.0)
     rev = jnp.where(row > sp, gn, 1.0)
@@ -230,7 +295,7 @@
         fwd = jnp.where(row < PEERS - step, fwd * pltpu.roll(fwd, PEERS - step, 0), fwd)
         rev = jnp.where(row >= step, rev * pltpu.roll(rev, step, 0), rev)
         step *= 2
-    carry = jnp.sum(jnp.where(row < sp, terms[...] * fwd, 0.0), axis=0, keepdims=True)
+    carry = jnp.sum(jnp.where(row < sp, terms * fwd, 0.0), axis=0, keepdims=True)
     coef[...] = jnp.where(row > sp, rev, 0.0)
     st = loc[...] + cum[...] * carry
     wide = iota((ROWS, CH), 0)
@@ -246,7 +311,7 @@
     r_out[...] = rr[...] * (prev * a[...] - q[...])
 
 
-def reverse_body(full, wout, gv, s1, lru, a_ref, gate_pre, tail_sum, send):
+def reverse_body(full, wout, gv, s1, lru, a_ref, gate_pre, tail_sum, out, send, sem):
     mixer = mm(full[0], wout[0:512, :])
     for t in range(1, TPN):
         mixer = mixer + mm(full[t], wout[t * 512 : (t + 1) * 512, :])
@@ -263,19 +328,18 @@
         step *= 2
     tail_sum[...] = s
     term = a[0:1] * s[0:1]
-    hi = term.astype(BF)
-    rest = term - hi.astype(F32)
-    mid = rest.astype(BF)
-    low = (rest - mid.astype(F32)).astype(BF)
-    which = iota((8, CH), 0)
-    extra = jnp.where(which == 0, hi.astype(F32), 0.0)
-    extra = jnp.where(which == 1, mid.astype(F32), extra)
-    extra = jnp.where(which == 2, low.astype(F32), extra).astype(BF)
-    send[:, 64:72, :] = jnp.broadcast_to(extra[None], (PEERS, 8, CH))
+    pieces = jnp.concatenate(in_three(term) + [jnp.zeros((5, CH), F32)], axis=0).astype(BF)
+    send[:, 64:72, :] = jnp.broadcast_to(pieces[None], (PEERS, 8, CH))
     lv = lru[...]
+    copies = []
     for t in range(TPN):
         part = mm(full[t], lv, 0, 0).astype(BF)
         send[8 * t : 8 * t + 8, 0:64, :] = part.reshape(8, 64, CH)
+        rows = pl.ds(8 * t, 8)
+        copies.append(pltpu.make_async_copy(send.at[rows], out.at[rows], sem.at[t]))
+        copies[t].start()
+    for copy in copies:
+        copy.wait()
 
 
 def final_body(got, coef, tail_sum, gain, rr, ad, scaled, wr, wi, out_proj, grad_in):
@@ -299,13 +363,21 @@
 BACK = [(i, (i - 1) % TPN) for i in range(TPN)]
 
 
-def ring_parts(own):
-    left = lax.ppermute(own, "tp", RING)
-    right = lax.ppermute(own, "tp", BACK)
+def ring_parts(own, name):
     half = PEERS // 2
-    far1 = lax.ppermute(left[:half], "tp", RING)
-    far2 = lax.ppermute(right[half:], "tp", BACK)
-    return own, left, right, far1, far2
+    depth = own.shape[1] if name == "a" else 64
+    low, high = own[:half, :depth], own[half:, :depth]
+
+    def move(value, where):
+        return lax.ppermute(value, "tp", where)
+
+    left1 = move(low, RING)
+    right2 = move(high, BACK)
+    left2 = move(high, RING)
+    right1 = move(low, BACK)
+    far1 = move(left1, RING)
+    far2 = move(right2, BACK)
+    return own, left1, left2, right1, right2, far1, far2
 
 
 def shape(*dims, dtype=BF):
@@ -322,7 +394,20 @@
         chain_body(tail, *refs)
 
     flops = 10 * rows * WIDTH * HID
-    *saved, partial_value = call(body, out, 9, flops, 12 << 20, smem=(0,))(tp, *parts, *weights)
+    held = [(TPN, PEERS, 80 if tail else 64, LANE)] + [o.shape for o in out]
+    held += [(WIDTH, HID), (WIDTH, HID), (HID, WIDTH)]
+    scratch = [pltpu.VMEM(dims, BF) for dims in held] + [dma(7), dma(3), dma(9)]
+    *saved, partial_value = call(
+        body,
+        out,
+        11,
+        flops,
+        12 << 20,
+        smem=(0,),
+        far=range(1, 11),
+        far_out=range(6),
+        scratch=scratch,
+    )(tp, *parts, *weights)
     return saved, partial_value.reshape(PEERS * TPN, size, LANE)
 
 
@@ -354,11 +439,6 @@
         3 << 20,
     )(routes.T, chosen_expert_weight.T, middle_stream, output_gradient)
     own_a = lax.all_to_all(send_a, "sp", 0, 0, tiled=True)
-    own_a, send_b = lax.optimization_barrier((own_a, send_b))
-    own_b = lax.all_to_all(send_b, "sp", 0, 0, tiled=True)
-    parts_a = ring_parts(own_a)
-    parts_b = ring_parts(own_b)
-
     first = lax.axis_index("tp") * 2
     recall_weight = lax.dynamic_slice_in_dim(recurrence_gate_weight, first, 2, 0)
     admit_weight = lax.dynamic_slice_in_dim(input_gate_weight, first, 2, 0)
@@ -383,21 +463,21 @@
     of_recall = rate * recall * (1.0 - recall)
     of_admit = driven * (1.0 - admit)
     tile = shape(ROWS, CH, dtype=F32)
-    cum, loc, gain, ends = call(
-        scan_body, [tile, tile, tile, shape(2, CH, dtype=F32)], 2, 1 << 28, 1 << 20
-    )(decay, driven)
-    ends, own_b2 = lax.optimization_barrier((ends, own_b))
-    all_ends = lax.all_to_all(
-        jnp.broadcast_to(ends[None], (PEERS, 2, CH)), "sp", 0, 0, tiled=True
-    )
+    cum, loc, gain, send_b = call(
+        scan_body, [tile, tile, tile, shape(PEERS, 80, LANE)], 3, 1 << 28, 2 << 20
+    )(decay, driven, send_b)
+    own_a, send_b = lax.optimization_barrier((own_a, send_b))
+    own_b = lax.all_to_all(send_b, "sp", 0, 0, tiled=True)
+    parts_a = ring_parts(own_a, "a")
+    parts_b = ring_parts(own_b, "b")
     s1, gelu_val, lru, of_log, coef = call(
         states_body,
         [tile, tile, shape(ROWS, CH), tile, shape(PEERS, CH, dtype=F32)],
-        9,
+        8,
         1 << 28,
         2 << 20,
         smem=(0,),
-    )(sp, all_ends[:, 0], all_ends[:, 1], decay, cum, loc, output_gate_logits, minus, of_recall)
+    )(sp, own_b, decay, cum, loc, output_gate_logits, minus, of_recall)
 
     saved_a, part_a = expert_chain(True, tp, parts_a, weights)
     got_a = lax.all_to_all(part_a, ("sp", "tp"), 0, 0, tiled=True)
@@ -409,16 +489,34 @@
     grad_up = mm(x, du, 0, 0).astype(BF)
     grad_down = mm(hid, cot, 0, 0).astype(BF)
 
-    spread = call(combine_body, shape(TPN, ROWS, 512), 4, 1 << 31, 4 << 20)(
-        got_a, got_b, idx.T, output_gradient
+    columns = idx.T
+    (so_far,) = call(combine_a_body, [shape(ROWS, 512, dtype=F32)], 3, 1 << 30, 2 << 20, 12)(
+        got_a, columns, output_gradient
     )
+    (spread,) = call(
+        combine_b_body,
+        [shape(TPN, ROWS, 512)],
+        3,
+        1 << 30,
+        3 << 20,
+        12,
+        far_out=(0,),
+        scratch=[pltpu.VMEM((ROWS, 512), BF), dma(TPN)],
+    )(got_b, columns, so_far)
     full = lax.all_to_all(spread, "tp", 0, 0, tiled=True)
     grad_gate_pre, tail_sum, send = call(
-        reverse_body, [tile, tile, shape(PEERS, 72, CH)], 6, 1 << 30, 4 << 20
+        reverse_body,
+        [tile, tile, shape(PEERS, 72, CH)],
+        6,
+        1 << 30,
+        4 << 20,
+        12,
+        far_out=(2,),
+        scratch=[pltpu.VMEM((PEERS, 72, CH), BF), dma(TPN)],
     )(full, recurrent_output_weight, gelu_val, s1, lru, decay)
     got = lax.all_to_all(send, "sp", 0, 0, tiled=True)
     grad_out_proj, grad_input = call(
-        final_body, [shape(64, CH, dtype=F32), tile], 9, 1 << 28, 3 << 20
+        final_body, [shape(64, CH, dtype=F32), tile], 9, 1 << 28, 3 << 20, 8
     )(got, coef, tail_sum, gain, of_log, of_admit, scaled, recall_weight, admit_weight)
     return (
         grad_gate[None],
@@ -447,6 +545,7 @@
         P("tp"),
         P("sp", "tp"),
     )
+
     return jax.shard_map(
         per_device,
         mesh=mesh,

time: 212 us -> 193 us (0.910)
  blocking collectives: 22.6 us -> 0 us
  starting transfers between devices: 47.5 us -> 54 us
  waiting for transfers between devices: 65 us -> 71 us
  Pallas kernels: 43.7 us -> 39 us
  local copies, waits for them, and re-layouts: 12 us -> 8.61 us
    all_to_all x1 -> x0, blocking collectives: 22.6 us -> none  [per_device(): own_a = lax.all_to_all(send_a, 'sp', 0, 0, tiled=True)]
    all_to_all x1, waiting for transfers between devices: 0.01 us -> 7.13 us  [per_device(): own_a = lax.all_to_all(send_a, 'sp', 0, 0, tiled=True)]
    pallas_call x6 -> x7, Pallas kernels: 38.3 us -> 33.3 us  [the longest x2 24.6 us: expert_chain(): call(body, out, 11, flops, 12 << 20, smem=(0,), far=range(1, 11), far_out...]
    ppermute x8 -> x12, starting transfers between devices: 9.92 us -> 14.9 us  [move(): return lax.ppermute(value, 'tp', where)]
    all_to_all x1, starting transfers between devices: 5.27 us -> 9.72 us  [per_device(): own_a = lax.all_to_all(send_a, 'sp', 0, 0, tiled=True)]
    all_to_all x1, starting transfers between devices: 9.44 us -> 5.07 us  [per_device(): got_a = lax.all_to_all(part_a, ('sp', 'tp'), 0, 0, tiled=True)]
    ppermute x8 -> x12, waiting for transfers between devices: 39.6 us -> 38.6 us  [move(): return lax.ppermute(value, 'tp', where)]
    unnamed x57 -> x71, local copies, waits for them, and re-layouts: 6.83 us -> 6.48 us
  transfers between devices with their start and end apart: 14 -> 18, of which waited for: 8 -> 13; matrix products, arithmetic and copies ran while one was open for 13% -> 12% of each run, Pallas kernels for 14% -> 16%
where the time goes in v1:
time: 193 us; the launch traced here: 192 us
  waiting for transfers between devices  71 us (37%)
  starting transfers between devices  54 us (28%)
  Pallas kernels  39 us (20%)
  matrix products  16.9 us (9%)
  local copies, waits for them, and re-layouts  8.61 us (4%)
    ppermute x12, waiting for transfers between devices, move(): return lax.ppermute(value, 'tp', where)  38.6 us
    pallas_call x2, Pallas kernels, expert_chain(): call(body, out, 11, flops, 12 << 20, smem=(0,), far=range(1, 11), far_out...  24.6 us
    dot_general x3, matrix products, mm(): lax.dot_general(a, b, (((ca,), (cb,)), ((), ())), preferred_element_type=...  16.5 us
    all_to_all x1, waiting for transfers between devices, per_device(): got_b = lax.all_to_all(part_b, ('sp', 'tp'), 0, 0, tiled=True)  14.9 us
    ppermute x12, starting transfers between devices, move(): return lax.ppermute(value, 'tp', where)  14.9 us
    all_to_all x1, starting transfers between devices, per_device(): own_a = lax.all_to_all(send_a, 'sp', 0, 0, tiled=True)  9.72 us
    all_to_all x1, starting transfers between devices, per_device(): got_b = lax.all_to_all(part_b, ('sp', 'tp'), 0, 0, tiled=True)  9.62 us
    all_to_all x1, waiting for transfers between devices, per_device(): own_a = lax.all_to_all(send_a, 'sp', 0, 0, tiled=True)  7.13 us
  transfers between devices with their start and end apart: 18, of which 13 were waited for; matrix products, arithmetic and copies ran while one was open for 12% of the time, Pallas kernels for 16%

profile of v1, /device:TPU:1, one launch (start us, length us, event | category | flops | bytes accessed | tf_op | source)
XLA Modules:
  0.0 192.4 jit_solution(10428376440439665852)
XLA Ops:
  0.7 3.1 %shard_map.181 = (bf16[32,80,128]{2,1,0:T(8,128)(2,1)}, bf16[32,64,128]{2,1,0:T(8,128)(2,1)}, s32[8,192]{1,0:T(8,128)}) custom-call(s32[2,192]{1,0:T(2,128)} %bitcast.65, f32[2,192]{1,0:T(2,128)} %bitcast.66, bf16[192,512]{1,0:T(8,128)(2,1)} %x.1, bf16[192,512]{1,0:T(8,128)(2,1)} %g.3), custom_call_target="tpu_custom_call" | custom-call | flops 1073741824 | bytes 3145728 | tf_op jit(solution)/shard_map/pallas_call | solution.py:434
  3.8 9.7 %all-to-all-start = ((bf16[32,80,128]{2,1,0:T(8,128)(2,1)}), bf16[32,80,128]{2,1,0:T(8,128)(2,1)S(1)}, u32[]{:S(2)}, u32[]{:S(2)}) async-start(bf16[32,80,128]{2,1,0:T(8,128)(2,1)} %get-tuple-element.37), calls=%async_computation | async-start | bytes 1310720 | tf_op jit(solution)/shard_map/all_to_all | solution.py:441
  16.7 2.5 %shard_map.182 = (f32[192,256]{1,0:T(8,128)}, f32[192,256]{1,0:T(8,128)}, f32[192,256]{1,0:T(8,128)}, bf16[32,80,128]{2,1,0:T(8,128)(2,1)}) custom-call(f32[192,256]{1,0:T(8,128)} %get-tuple-element.78.a_ref.a, f32[192,256]{1,0:T(8,128)} %get-tuple-element.69.b_ref, bf16[32,64,128]{2,1,0:T(8,128)(2,1)} %get-tuple-element.38.rows_b), custom_call_target="tpu_custom_call" | custom-call | flops 268435456 | bytes 2097152 | tf_op jit(solution)/shard_map/pallas_call | solution.py:466
  19.2 7.1 %all-to-all-done.refs_1_ = bf16[32,80,128]{2,1,0:T(8,128)(2,1)S(1)} async-done(((bf16[32,80,128]{2,1,0:T(8,128)(2,1)}), bf16[32,80,128]{2,1,0:T(8,128)(2,1)S(1)}, u32[]{:S(2)}, u32[]{:S(2)}) %all-to-all-start) | async-done | bytes 655392 | tf_op jit(solution)/shard_map/all_to_all | solution.py:441
  26.4 2.5 %collective-permute-start.3 = (bf16[16,80,128]{2,1,0:T(8,128)(2,1)S(1)}, bf16[16,80,128]{2,1,0:T(8,128)(2,1)S(1)}, u32[]{:S(2)}, u32[]{:S(2)}) collective-permute-start(bf16[16,80,128]{2,1,0:T(8,128)(2,1)S(1)} %get-tuple-element.74), channel_id=1, source_target_pairs={{0,3},{1,0},{2,1},{3,2},{4,7},{5,4},{6,5},{7,6},{8,11},{9,8},{10,9... | collective-permute-start | bytes 983048 | tf_op jit(solution)/shard_map/ppermute | solution.py:372
  29.1 2.5 %collective-permute-start.2 = (bf16[16,80,128]{2,1,0:T(8,128)(2,1)S(1)}, bf16[16,80,128]{2,1,0:T(8,128)(2,1)}, u32[]{:S(2)}, u32[]{:S(2)}) collective-permute-start(bf16[16,80,128]{2,1,0:T(8,128)(2,1)S(1)} %get-tuple-element.75), channel_id=1, source_target_pairs={{0,3},{1,0},{2,1},{3,2},{4,7},{5,4},{6,5},{7,6},{8,11},{9,8},{10,9... | collective-permute-start | bytes 983048 | tf_op jit(solution)/shard_map/ppermute | solution.py:372
  31.6 3.9 %collective-permute-done.3.refs_5_ = bf16[16,80,128]{2,1,0:T(8,128)(2,1)S(1)} collective-permute-done((bf16[16,80,128]{2,1,0:T(8,128)(2,1)S(1)}, bf16[16,80,128]{2,1,0:T(8,128)(2,1)S(1)}, u32[]{:S(2)}, u32[]{:S(2)}) %collective-permute-start.3) | collective-permute-done | bytes 327712 | tf_op jit(solution)/shard_map/ppermute | solution.py:372
  35.5 3.4 %collective-permute-start.5 = (bf16[16,80,128]{2,1,0:T(8,128)(2,1)S(1)}, bf16[16,80,128]{2,1,0:T(8,128)(2,1)}, u32[]{:S(2)}, u32[]{:S(2)}) collective-permute-start(bf16[16,80,128]{2,1,0:T(8,128)(2,1)S(1)} %collective-permute-done.3.refs_5_), channel_id=1, source_target_pairs={{0,3},{1,0},{2,1},{3,2},{4,7},{5,4},{6,5},{7,6},{8,11},{9,8},{10,9... | collective-permute-start | bytes 983048 | tf_op jit(solution)/shard_map/ppermute | solution.py:372
  38.9 6.1 %all-to-all-start.1 = ((bf16[32,80,128]{2,1,0:T(8,128)(2,1)}), bf16[32,80,128]{2,1,0:T(8,128)(2,1)S(1)}, u32[]{:S(2)}, u32[]{:S(2)}) async-start(bf16[32,80,128]{2,1,0:T(8,128)(2,1)} %get-tuple-element.42), calls=%async_computation.1 | async-start | bytes 1310720 | tf_op jit(solution)/shard_map/all_to_all | solution.py:470
  45.7 3.9 %collective-permute-done.5.refs_7_ = bf16[16,80,128]{2,1,0:T(8,128)(2,1)} collective-permute-done((bf16[16,80,128]{2,1,0:T(8,128)(2,1)S(1)}, bf16[16,80,128]{2,1,0:T(8,128)(2,1)}, u32[]{:S(2)}, u32[]{:S(2)}) %collective-permute-start.5) | collective-permute-done | bytes 327712 | tf_op jit(solution)/shard_map/ppermute | solution.py:372
  49.5 3.2 %collective-permute-done.4.refs_6_ = bf16[16,80,128]{2,1,0:T(8,128)(2,1)} collective-permute-done((bf16[16,80,128]{2,1,0:T(8,128)(2,1)S(1)}, bf16[16,80,128]{2,1,0:T(8,128)(2,1)}, u32[]{:S(2)}, u32[]{:S(2)}) %collective-permute-start.4) | collective-permute-done | bytes 327712 | tf_op jit(solution)/shard_map/ppermute | solution.py:372
  52.8 13.6 %shard_map.183 = (bf16[320,2048]{1,0:T(8,128)(2,1)}, bf16[320,2048]{1,0:T(8,128)(2,1)}, bf16[320,896]{1,0:T(8,128)(2,1)}, bf16[320,896]{1,0:T(8,128)(2,1)}, bf16...) custom-call(s32[1]{0:T(128)} %bitcast.refs_0_, bf16[32,80,128]{2,1,0:T(8,128)(2,1)} %copy-done.12, ...), custom_call_target="tpu_custom_call" | custom-call | flops 5872025600 | bytes 12582912 | tf_op jit(solution)/shard_map/pallas_call | solution.py:400
  66.5 5.1 %all-to-all-start.3 = ((bf16[128,40,128]{2,1,0:T(8,128)(2,1)}), bf16[128,40,128]{2,1,0:T(8,128)(2,1)S(1)}, u32[]{:S(2)}, u32[]{:S(2)}) async-start(bf16[128,40,128]{2,1,0:T(8,128)(2,1)} %bitcast.57), calls=%async_computation.3 | async-start | bytes 2621440 | tf_op jit(solution)/shard_map/all_to_all | solution.py:483
  71.6 2.7 %collective-permute-start.9 = (bf16[16,64,128]{2,1,0:T(8,128)(2,1)S(1)}, bf16[16,64,128]{2,1,0:T(8,128)(2,1)S(1)}, u32[]{:S(2)}, u32[]{:S(2)}) collective-permute-start(bf16[16,64,128]{2,1,0:T(8,128)(2,1)S(1)} %get-tuple-element.72), channel_id=1, source_target_pairs={{0,3},{1,0},{2,1},{3,2},{4,7},{5,4},{6,5},{7,6},{8,11},{9,8},{10,9... | collective-permute-start | bytes 786440 | tf_op jit(solution)/shard_map/ppermute | solution.py:372
  74.5 2.5 %collective-permute-start.8 = (bf16[16,64,128]{2,1,0:T(8,128)(2,1)S(1)}, bf16[16,64,128]{2,1,0:T(8,128)(2,1)S(1)}, u32[]{:S(2)}, u32[]{:S(2)}) collective-permute-start(bf16[16,64,128]{2,1,0:T(8,128)(2,1)S(1)} %get-tuple-element.73), channel_id=1, source_target_pairs={{0,3},{1,0},{2,1},{3,2},{4,7},{5,4},{6,5},{7,6},{8,11},{9,8},{10,9... | collective-permute-start | bytes 786440 | tf_op jit(solution)/shard_map/ppermute | solution.py:372
  77.0 15.6 %collective-permute-done.9.refs_5_ = bf16[16,64,128]{2,1,0:T(8,128)(2,1)S(1)} collective-permute-done((bf16[16,64,128]{2,1,0:T(8,128)(2,1)S(1)}, bf16[16,64,128]{2,1,0:T(8,128)(2,1)S(1)}, u32[]{:S(2)}, u32[]{:S(2)}) %collective-permute-start.9) | collective-permute-done | bytes 262176 | tf_op jit(solution)/shard_map/ppermute | solution.py:372
  94.1 5.4 %collective-permute-done.7.refs_3_ = bf16[16,64,128]{2,1,0:T(8,128)(2,1)S(1)} collective-permute-done((bf16[16,64,128]{2,1,0:T(8,128)(2,1)S(1)}, bf16[16,64,128]{2,1,0:T(8,128)(2,1)S(1)}, u32[]{:S(2)}, u32[]{:S(2)}) %collective-permute-start.7) | collective-permute-done | bytes 262176 | tf_op jit(solution)/shard_map/ppermute | solution.py:372
  99.5 4.4 %collective-permute-done.11.refs_7_ = bf16[16,64,128]{2,1,0:T(8,128)(2,1)S(1)} collective-permute-done((bf16[16,64,128]{2,1,0:T(8,128)(2,1)S(1)}, bf16[16,64,128]{2,1,0:T(8,128)(2,1)S(1)}, u32[]{:S(2)}, u32[]{:S(2)}) %collective-permute-start.11) | collective-permute-done | bytes 262176 | tf_op jit(solution)/shard_map/ppermute | solution.py:372
  105.6 11.0 %shard_map.184 = (bf16[256,2048]{1,0:T(8,128)(2,1)}, bf16[256,2048]{1,0:T(8,128)(2,1)}, bf16[256,896]{1,0:T(8,128)(2,1)}, bf16[256,896]{1,0:T(8,128)(2,1)}, bf16...) custom-call(s32[1]{0:T(128)} %bitcast.refs_0_, bf16[32,80,128]{2,1,0:T(8,128)(2,1)} %copy-done.11, ...), custom_call_target="tpu_custom_call" | custom-call | flops 4697620480 | bytes 12582912 | tf_op jit(solution)/shard_map/pallas_call | solution.py:400
  116.6 9.6 %all-to-all-start.2 = ((bf16[128,32,128]{2,1,0:T(8,128)(2,1)}), bf16[128,32,128]{2,1,0:T(8,128)(2,1)S(1)}, u32[]{:S(2)}, u32[]{:S(2)}) async-start(bf16[128,32,128]{2,1,0:T(8,128)(2,1)} %bitcast.58), calls=%async_computation.2 | async-start | bytes 2097152 | tf_op jit(solution)/shard_map/all_to_all | solution.py:485
  126.4 2.6 %shard_map.187 = (f32[192,256]{1,0:T(8,128)}, f32[192,256]{1,0:T(8,128)}, bf16[192,256]{1,0:T(8,128)(2,1)}, f32[192,256]{1,0:T(8,128)}, f32[32,256]{1,0:T(8,128)}) custom-call(s32[1]{0:T(128)} %bitcast.14.sp_ref, bf16[32,80,128]{2,1,0:T(8,128)(2,1)} %copy-done.11, f32[192,256]{1,0:T(8,128)} %get-tuple-element.78.a_ref.a, f32[192,256]{1,0:T(8,128)} %get-tuple-element.55.cum, ...), custom_call_target="tpu_custom_call" | custom-call | flops 268435456 | bytes 2097152 | tf_op jit(solution)/shard_map/pallas_call | solution.py:473
  130.8 14.9 %all-to-all-done.2.got = bf16[128,32,128]{2,1,0:T(8,128)(2,1)S(1)} async-done(((bf16[128,32,128]{2,1,0:T(8,128)(2,1)}), bf16[128,32,128]{2,1,0:T(8,128)(2,1)S(1)}, u32[]{:S(2)}, u32[]{:S(2)}) %all-to-all-start.2) | async-done | bytes 1048608 | tf_op jit(solution)/shard_map/all_to_all | solution.py:485
  146.8 1.6 shard_map.186
  148.3 3.6 %all-to-all-start.4 = ((bf16[4,192,512]{2,1,0:T(8,128)(2,1)}), bf16[4,192,512]{2,1,0:T(8,128)(2,1)S(1)}, u32[]{:S(2)}, u32[]{:S(2)}) async-start(bf16[4,192,512]{2,1,0:T(8,128)(2,1)} %shard_map.186), calls=%async_computation.4 | async-start | bytes 1572864 | tf_op jit(solution)/shard_map/all_to_all | solution.py:506
  152.0 2.7 %constant_dynamic-update-slice_fusion.1 = bf16[576,2048]{1,0:T(8,128)(2,1)} fusion(bf16[320,2048]{1,0:T(8,128)(2,1)} %get-tuple-element.41), kind=kLoop, calls=%fused_computation.42 | loop fusion | bytes 2621440
  154.8 4.5 %convert_bitcast_fusion = bf16[1,896,2048]{2,1,0:T(8,128)(2,1)} fusion(bf16[256,2048]{1,0:T(8,128)(2,1)S(1)} %copy-done.28, bf16[320,2048]{1,0:T(8,128)(2,1)S(1)} %copy-done.32, bf16[256,896]{1,0:T(8,128)(2,1)S(1)} %copy-done.31, bf16[320,896]{1,0:T(8,128)(2,1)S(1)} %copy-done.34), kind=kOutput, calls=%fused_computation | convolution fusion | flops 2122547200 | bytes 7061504 | tf_op jit(solution)/shard_map/dot_general | solution.py:23
  159.3 4.7 %all-to-all-done.4.full = bf16[4,192,512]{2,1,0:T(8,128)(2,1)S(1)} async-done(((bf16[4,192,512]{2,1,0:T(8,128)(2,1)}), bf16[4,192,512]{2,1,0:T(8,128)(2,1)S(1)}, u32[]{:S(2)}, u32[]{:S(2)}) %all-to-all-start.4) | async-done | bytes 786464 | tf_op jit(solution)/shard_map/all_to_all | solution.py:506
  165.2 2.5 %shard_map.188 = (f32[192,256]{1,0:T(8,128)}, f32[192,256]{1,0:T(8,128)S(1)}, bf16[32,72,256]{2,1,0:T(8,128)(2,1)}) custom-call(bf16[4,192,512]{2,1,0:T(8,128)(2,1)S(1)} %all-to-all-done.4.full, bf16[2048,256]{1,0:T(8,128)(2,1)S(1)} %copy-done.4, f32[192,256]{1,0:T(8,128)S(1)} %copy-done.7, f32[192,256]{1,0:T(8,128)S(1)} %copy-done.6, ...), custom_call_target="tpu_custom_call" | custom-call | flops 1073741824 | bytes 4194304 | tf_op jit(solution)/shard_map/pallas_call | solution.py:507
  167.8 5.0 %all-to-all-start.5 = ((bf16[32,72,256]{2,1,0:T(8,128)(2,1)}), bf16[32,72,256]{2,1,0:T(8,128)(2,1)S(1)}, u32[]{:S(2)}, u32[]{:S(2)}) async-start(bf16[32,72,256]{2,1,0:T(8,128)(2,1)} %get-tuple-element.60), calls=%async_computation.5 | async-start | bytes 2359296 | tf_op jit(solution)/shard_map/all_to_all | solution.py:517
  173.8 7.1 %convert_bitcast_fusion.1 = bf16[1,2048,896]{2,1,0:T(8,128)(2,1)} fusion(bf16[576,2048]{1,0:T(8,128)(2,1)} %constant_dynamic-update-slice_fusion, bf16[256,896]{1,0:T(8,128)(2,1)S(1)} %copy-done.30, bf16[320,896]{1,0:T(8,128)(2,1)} %get-tuple-element.46), kind=kOutput, calls=%fused_computation.1 | convolution fusion | flops 2117828608 | bytes 7061504 | tf_op jit(solution)/shard_map/dot_general | solution.py:23
  181.0 4.8 %convert_bitcast_fusion.2 = bf16[1,2048,896]{2,1,0:T(8,128)(2,1)} fusion(bf16[576,2048]{1,0:T(8,128)(2,1)S(1)} %copy-done.14, bf16[256,896]{1,0:T(8,128)(2,1)S(1)} %copy-done.29, bf16[320,896]{1,0:T(8,128)(2,1)S(1)} %copy-done.33), kind=kOutput, calls=%fused_computation.2 | convolution fusion | flops 2117828608 | bytes 7061504 | tf_op jit(solution)/shard_map/dot_general | solution.py:23
  185.8 5.6 %all-to-all-done.5.got = bf16[32,72,256]{2,1,0:T(8,128)(2,1)S(1)} async-done(((bf16[32,72,256]{2,1,0:T(8,128)(2,1)}), bf16[32,72,256]{2,1,0:T(8,128)(2,1)S(1)}, u32[]{:S(2)}, u32[]{:S(2)}) %all-to-all-start.5) | async-done | bytes 1179680 | tf_op jit(solution)/shard_map/all_to_all | solution.py:517
  (97 shorter events, 13.8 us)
Async XLA Ops:
  0.6 12.9 %copy-start.18 = (f32[256]{0:T(256)S(1)}, f32[256]{0:T(256)}, u32[]{:S(2)}) copy-start(f32[256]{0:T(256)} %param.26) | copy-start | bytes 3076
  0.6 13.8 %copy-start.15 = (bf16[192,256]{1,0:T(8,128)(2,1)S(1)}, bf16[192,256]{1,0:T(8,128)(2,1)}, u32[]{:S(2)}) copy-start(bf16[192,256]{1,0:T(8,128)(2,1)} %param.22) | copy-start | bytes 294916
  3.8 11.1 %copy-start.16 = (f32[192,256]{1,0:T(8,128)S(1)}, f32[192,256]{1,0:T(8,128)}, u32[]{:S(2)}) copy-start(f32[192,256]{1,0:T(8,128)} %param.27) | copy-start | bytes 589828
  3.8 22.6 %all-to-all-start = ((bf16[32,80,128]{2,1,0:T(8,128)(2,1)}), bf16[32,80,128]{2,1,0:T(8,128)(2,1)S(1)}, u32[]{:S(2)}, u32[]{:S(2)}) async-start(bf16[32,80,128]{2,1,0:T(8,128)(2,1)} %get-tuple-element.37), calls=%async_computation | async-start | bytes 1310720 | tf_op jit(solution)/shard_map/all_to_all | solution.py:441
  26.3 26.5 %copy-start.12 = (bf16[32,80,128]{2,1,0:T(8,128)(2,1)}, bf16[32,80,128]{2,1,0:T(8,128)(2,1)S(1)}, u32[]{:S(2)}) copy-start(bf16[32,80,128]{2,1,0:T(8,128)(2,1)S(1)} %all-to-all-done.refs_1_) | copy-start | bytes 1966084
  26.4 9.1 %collective-permute-start.3 = (bf16[16,80,128]{2,1,0:T(8,128)(2,1)S(1)}, bf16[16,80,128]{2,1,0:T(8,128)(2,1)S(1)}, u32[]{:S(2)}, u32[]{:S(2)}) collective-permute-start(bf16[16,80,128]{2,1,0:T(8,128)(2,1)S(1)} %get-tuple-element.74), channel_id=1, source_target_pairs={{0,3},{1,0},{2,1},{3,2},{4,7},{5,4},{6,5},{7,6},{8,11},{9,8},{10,9... | collective-permute-start | bytes 983048 | tf_op jit(solution)/shard_map/ppermute | solution.py:372
  28.9 10.0 %collective-permute-start = (bf16[16,80,128]{2,1,0:T(8,128)(2,1)S(1)}, bf16[16,80,128]{2,1,0:T(8,128)(2,1)S(1)}, u32[]{:S(2)}, u32[]{:S(2)}) collective-permute-start(bf16[16,80,128]{2,1,0:T(8,128)(2,1)S(1)} %get-tuple-element.75), channel_id=1, source_target_pairs={{0,1},{1,2},{2,3},{3,0},{4,5},{5,6},{6,7},{7,4},{8,9},{9,10},{10,1... | collective-permute-start | bytes 983048 | tf_op jit(solution)/shard_map/ppermute | solution.py:372
  28.9 16.7 %collective-permute-start.1 = (bf16[16,80,128]{2,1,0:T(8,128)(2,1)S(1)}, bf16[16,80,128]{2,1,0:T(8,128)(2,1)S(1)}, u32[]{:S(2)}, u32[]{:S(2)}) collective-permute-start(bf16[16,80,128]{2,1,0:T(8,128)(2,1)S(1)} %get-tuple-element.74), channel_id=1, source_target_pairs={{0,1},{1,2},{2,3},{3,0},{4,5},{5,6},{6,7},{7,4},{8,9},{9,10},{10,1... | collective-permute-start | bytes 983048 | tf_op jit(solution)/shard_map/ppermute | solution.py:372
  29.1 16.5 %collective-permute-start.2 = (bf16[16,80,128]{2,1,0:T(8,128)(2,1)S(1)}, bf16[16,80,128]{2,1,0:T(8,128)(2,1)}, u32[]{:S(2)}, u32[]{:S(2)}) collective-permute-start(bf16[16,80,128]{2,1,0:T(8,128)(2,1)S(1)} %get-tuple-element.75), channel_id=1, source_target_pairs={{0,3},{1,0},{2,1},{3,2},{4,7},{5,4},{6,5},{7,6},{8,11},{9,8},{10,9... | collective-permute-start | bytes 983048 | tf_op jit(solution)/shard_map/ppermute | solution.py:372
  35.5 17.3 %copy-start.19 = (bf16[16,80,128]{2,1,0:T(8,128)(2,1)}, bf16[16,80,128]{2,1,0:T(8,128)(2,1)S(1)}, u32[]{:S(2)}) copy-start(bf16[16,80,128]{2,1,0:T(8,128)(2,1)S(1)} %collective-permute-done.3.refs_5_) | copy-start | bytes 983044
  35.5 14.0 %collective-permute-start.5 = (bf16[16,80,128]{2,1,0:T(8,128)(2,1)S(1)}, bf16[16,80,128]{2,1,0:T(8,128)(2,1)}, u32[]{:S(2)}, u32[]{:S(2)}) collective-permute-start(bf16[16,80,128]{2,1,0:T(8,128)(2,1)S(1)} %collective-permute-done.3.refs_5_), channel_id=1, source_target_pairs={{0,3},{1,0},{2,1},{3,2},{4,7},{5,4},{6,5},{7,6},{8,11},{9,8},{10,9... | collective-permute-start | bytes 983048 | tf_op jit(solution)/shard_map/ppermute | solution.py:372
  38.9 13.9 %copy-start.20 = (bf16[16,80,128]{2,1,0:T(8,128)(2,1)}, bf16[16,80,128]{2,1,0:T(8,128)(2,1)S(1)}, u32[]{:S(2)}) copy-start(bf16[16,80,128]{2,1,0:T(8,128)(2,1)S(1)} %collective-permute-done.refs_2_) | copy-start | bytes 983044
  38.9 13.9 %collective-permute-start.4 = (bf16[16,80,128]{2,1,0:T(8,128)(2,1)S(1)}, bf16[16,80,128]{2,1,0:T(8,128)(2,1)}, u32[]{:S(2)}, u32[]{:S(2)}) collective-permute-start(bf16[16,80,128]{2,1,0:T(8,128)(2,1)S(1)} %collective-permute-done.refs_2_), channel_id=1, source_target_pairs={{0,1},{1,2},{2,3},{3,0},{4,5},{5,6},{6,7},{7,4},{8,9},{9,10},{10,1... | collective-permute-start | bytes 983048 | tf_op jit(solution)/shard_map/ppermute | solution.py:372
  38.9 27.5 %all-to-all-start.1 = ((bf16[32,80,128]{2,1,0:T(8,128)(2,1)}), bf16[32,80,128]{2,1,0:T(8,128)(2,1)S(1)}, u32[]{:S(2)}, u32[]{:S(2)}) async-start(bf16[32,80,128]{2,1,0:T(8,128)(2,1)} %get-tuple-element.42), calls=%async_computation.1 | async-start | bytes 1310720 | tf_op jit(solution)/shard_map/all_to_all | solution.py:470
  66.4 38.4 %copy-start.11 = (bf16[32,80,128]{2,1,0:T(8,128)(2,1)}, bf16[32,80,128]{2,1,0:T(8,128)(2,1)S(1)}, u32[]{:S(2)}) copy-start(bf16[32,80,128]{2,1,0:T(8,128)(2,1)S(1)} %all-to-all-done.1.refs_1_.got) | copy-start | bytes 1966084
  66.5 50.2 %all-to-all-start.3 = ((bf16[128,40,128]{2,1,0:T(8,128)(2,1)}), bf16[128,40,128]{2,1,0:T(8,128)(2,1)S(1)}, u32[]{:S(2)}, u32[]{:S(2)}) async-start(bf16[128,40,128]{2,1,0:T(8,128)(2,1)} %bitcast.57), calls=%async_computation.3 | async-start | bytes 2621440 | tf_op jit(solution)/shard_map/all_to_all | solution.py:483
  71.6 21.0 %collective-permute-start.9 = (bf16[16,64,128]{2,1,0:T(8,128)(2,1)S(1)}, bf16[16,64,128]{2,1,0:T(8,128)(2,1)S(1)}, u32[]{:S(2)}, u32[]{:S(2)}) collective-permute-start(bf16[16,64,128]{2,1,0:T(8,128)(2,1)S(1)} %get-tuple-element.72), channel_id=1, source_target_pairs={{0,3},{1,0},{2,1},{3,2},{4,7},{5,4},{6,5},{7,6},{8,11},{9,8},{10,9... | collective-permute-start | bytes 786440 | tf_op jit(solution)/shard_map/ppermute | solution.py:372
  74.3 52.0 %copy-start.17 = (s32[8,192]{1,0:T(8,128)S(1)}, s32[8,192]{1,0:T(8,128)}, u32[]{:S(2)}) copy-start(s32[8,192]{1,0:T(8,128)} %get-tuple-element.53) | copy-start | bytes 18436
  74.3 19.5 %collective-permute-start.6 = (bf16[16,64,128]{2,1,0:T(8,128)(2,1)S(1)}, bf16[16,64,128]{2,1,0:T(8,128)(2,1)S(1)}, u32[]{:S(2)}, u32[]{:S(2)}) collective-permute-start(bf16[16,64,128]{2,1,0:T(8,128)(2,1)S(1)} %get-tuple-element.73), channel_id=1, source_target_pairs={{0,1},{1,2},{2,3},{3,0},{4,5},{5,6},{6,7},{7,4},{8,9},{9,10},{10,1... | collective-permute-start | bytes 786440 | tf_op jit(solution)/shard_map/ppermute | solution.py:372
  74.3 25.2 %collective-permute-start.7 = (bf16[16,64,128]{2,1,0:T(8,128)(2,1)S(1)}, bf16[16,64,128]{2,1,0:T(8,128)(2,1)S(1)}, u32[]{:S(2)}, u32[]{:S(2)}) collective-permute-start(bf16[16,64,128]{2,1,0:T(8,128)(2,1)S(1)} %get-tuple-element.72), channel_id=1, source_target_pairs={{0,1},{1,2},{2,3},{3,0},{4,5},{5,6},{6,7},{7,4},{8,9},{9,10},{10,1... | collective-permute-start | bytes 786440 | tf_op jit(solution)/shard_map/ppermute | solution.py:372
  74.5 24.9 %collective-permute-start.8 = (bf16[16,64,128]{2,1,0:T(8,128)(2,1)S(1)}, bf16[16,64,128]{2,1,0:T(8,128)(2,1)S(1)}, u32[]{:S(2)}, u32[]{:S(2)}) collective-permute-start(bf16[16,64,128]{2,1,0:T(8,128)(2,1)S(1)} %get-tuple-element.73), channel_id=1, source_target_pairs={{0,3},{1,0},{2,1},{3,2},{4,7},{5,4},{6,5},{7,6},{8,11},{9,8},{10,9... | collective-permute-start | bytes 786440 | tf_op jit(solution)/shard_map/ppermute | solution.py:372
  92.6 12.3 %copy-start.22 = (bf16[16,64,128]{2,1,0:T(8,128)(2,1)}, bf16[16,64,128]{2,1,0:T(8,128)(2,1)S(1)}, u32[]{:S(2)}) copy-start(bf16[16,64,128]{2,1,0:T(8,128)(2,1)S(1)} %collective-permute-done.9.refs_5_) | copy-start | bytes 786436
  92.6 11.2 %collective-permute-start.11 = (bf16[16,64,128]{2,1,0:T(8,128)(2,1)S(1)}, bf16[16,64,128]{2,1,0:T(8,128)(2,1)S(1)}, u32[]{:S(2)}, u32[]{:S(2)}) collective-permute-start(bf16[16,64,128]{2,1,0:T(8,128)(2,1)S(1)} %collective-permute-done.9.refs_5_), channel_id=1, source_target_pairs={{0,3},{1,0},{2,1},{3,2},{4,7},{5,4},{6,5},{7,6},{8,11},{9,8},{10,9... | collective-permute-start | bytes 786440 | tf_op jit(solution)/shard_map/ppermute | solution.py:372
  93.8 11.0 %copy-start.23 = (bf16[16,64,128]{2,1,0:T(8,128)(2,1)}, bf16[16,64,128]{2,1,0:T(8,128)(2,1)S(1)}, u32[]{:S(2)}) copy-start(bf16[16,64,128]{2,1,0:T(8,128)(2,1)S(1)} %collective-permute-done.6.refs_2_) | copy-start | bytes 786436
  93.8 11.0 %collective-permute-start.10 = (bf16[16,64,128]{2,1,0:T(8,128)(2,1)S(1)}, bf16[16,64,128]{2,1,0:T(8,128)(2,1)S(1)}, u32[]{:S(2)}, u32[]{:S(2)}) collective-permute-start(bf16[16,64,128]{2,1,0:T(8,128)(2,1)S(1)} %collective-permute-done.6.refs_2_), channel_id=1, source_target_pairs={{0,1},{1,2},{2,3},{3,0},{4,5},{5,6},{6,7},{7,4},{8,9},{9,10},{10,1... | collective-permute-start | bytes 786440 | tf_op jit(solution)/shard_map/ppermute | solution.py:372
  116.6 12.4 %copy-start.5 = (bf16[192,512]{1,0:T(8,128)(2,1)S(1)}, bf16[192,512]{1,0:T(8,128)(2,1)}, u32[]{:S(2)}) copy-start(bf16[192,512]{1,0:T(8,128)(2,1)} %g.3) | copy-start | bytes 589828
  116.6 29.2 %all-to-all-start.2 = ((bf16[128,32,128]{2,1,0:T(8,128)(2,1)}), bf16[128,32,128]{2,1,0:T(8,128)(2,1)S(1)}, u32[]{:S(2)}, u32[]{:S(2)}) async-start(bf16[128,32,128]{2,1,0:T(8,128)(2,1)} %bitcast.58), calls=%async_computation.2 | async-start | bytes 2097152 | tf_op jit(solution)/shard_map/all_to_all | solution.py:485
  148.3 15.6 %all-to-all-start.4 = ((bf16[4,192,512]{2,1,0:T(8,128)(2,1)}), bf16[4,192,512]{2,1,0:T(8,128)(2,1)S(1)}, u32[]{:S(2)}, u32[]{:S(2)}) async-start(bf16[4,192,512]{2,1,0:T(8,128)(2,1)} %shard_map.186), calls=%async_computation.4 | async-start | bytes 1572864 | tf_op jit(solution)/shard_map/all_to_all | solution.py:506
  167.8 23.6 %all-to-all-start.5 = ((bf16[32,72,256]{2,1,0:T(8,128)(2,1)}), bf16[32,72,256]{2,1,0:T(8,128)(2,1)S(1)}, u32[]{:S(2)}, u32[]{:S(2)}) async-start(bf16[32,72,256]{2,1,0:T(8,128)(2,1)} %get-tuple-element.60), calls=%async_computation.5 | async-start | bytes 2359296 | tf_op jit(solution)/shard_map/all_to_all | solution.py:517
  180.9 10.4 %copy-start.1 = (f32[192,256]{1,0:T(8,128)S(1)}, f32[192,256]{1,0:T(8,128)}, u32[]{:S(2)}) copy-start(f32[192,256]{1,0:T(8,128)} %get-tuple-element.63.gain) | copy-start | bytes 589828
  181.0 10.4 %copy-start.2 = (f32[192,256]{1,0:T(8,128)S(1)}, f32[192,256]{1,0:T(8,128)}, u32[]{:S(2)}) copy-start(f32[192,256]{1,0:T(8,128)} %get-tuple-element.64.rr) | copy-start | bytes 589828
  181.0 10.4 %copy-start.3 = (f32[32,256]{1,0:T(8,128)S(1)}, f32[32,256]{1,0:T(8,128)}, u32[]{:S(2)}) copy-start(f32[32,256]{1,0:T(8,128)} %get-tuple-element.61.coef) | copy-start | bytes 98308
  (21 other events, 109.2 us)

commit v2 on v1

--- a/solution.py
+++ b/solution.py
@@ -74,10 +74,28 @@
     return (piece * (PEERS * 2) + peer * 2 + slot == r).astype(F32).astype(BF)
 
 
-def pack_body(routes, weights, x, g, out_a, out_b, out_idx):
+def weighted(weights, g):
+    same = iota((ROWS, ROWS), 0) == iota((ROWS, ROWS), 1)
+    gf = g[...].astype(F32)
+    cots = []
+    for k in range(2):
+        w = jnp.sum(jnp.where(same, weights[k : k + 1, :], 0.0), axis=1, keepdims=True)
+        cots.append((w * gf).astype(BF))
+    return jnp.concatenate(cots, axis=0)
+
+
+def chosen(at0, at1, n, x, both):
+    r = iota((n, ROWS), 0)
+    p0, p1 = (r == at0).astype(F32), (r == at1).astype(F32)
+    return (
+        mm((p0 + p1).astype(BF), x),
+        mm(jnp.concatenate([p0, p1], axis=1).astype(BF), both),
+    )
+
+
+def pack_body(routes, weights, x, g, out_a, out_idx):
     experts = iota((PEERS, ROWS), 0)
     before = (iota((ROWS, ROWS), 0) < iota((ROWS, ROWS), 1)).astype(F32).astype(BF)
-    same = iota((ROWS, ROWS), 0) == iota((ROWS, ROWS), 1)
     r0, r1 = routes[0:1, :], routes[1:2, :]
     o0 = (experts == r0).astype(F32)
     o1 = (experts == r1).astype(F32)
@@ -92,50 +110,40 @@
             idx.append(jnp.where(here, r * (high - low) + k - low, -1))
     none = jnp.full((1, ROWS), -1, jnp.int32)
     out_idx[...] = jnp.concatenate(idx + [none, none], axis=0)
+    both = weighted(weights, g)
     xv = x[...]
-    gf = g[...].astype(F32)
-    cots = []
-    for k in range(2):
-        w = jnp.sum(jnp.where(same, weights[k : k + 1, :], 0.0), axis=1, keepdims=True)
-        cots.append((w * gf).astype(BF))
-    both = jnp.concatenate(cots, axis=0)
-
-    def chosen(first, n):
-        r = iota((n, ROWS), 0)
-        p0 = (r == idx[first]).astype(F32)
-        p1 = (r == idx[first + 1]).astype(F32)
-        return (
-            mm((p0 + p1).astype(BF), xv),
-            mm(jnp.concatenate([p0, p1], axis=1).astype(BF), both),
-        )
-
-    for first, out in ((0, out_a), (2, out_b)):
-        xm, cm = chosen(first, PEERS * 8)
-        pack_main(xm, out, 0, 4)
-        pack_main(cm, out, 32, 4)
-    xt, ct = chosen(4, PEERS * 2)
-    pieces = [v[:, q * LANE : (q + 1) * LANE] for v in (xt, ct) for q in range(4)]
-    tail = mm(tail_order(8), jnp.concatenate(pieces, axis=0).astype(BF))
-    out_a[:, 64:80, :] = tail.astype(BF).reshape(PEERS, 16, LANE)
+    xm, cm = chosen(idx[0], idx[1], PEERS * 8, xv, both)
+    pack_main(xm, out_a, 0, 4)
+    pack_main(cm, out_a, 32, 4)
 
 
 def chain_body(tail, tp_ref, *refs):
-    parts, weights, outs, rest = refs[:7], refs[7:10], refs[10:16], refs[16:]
+    n = 5 if tail else 7
+    parts, weights, outs, rest = refs[:n], refs[n : n + 3], refs[n + 3 : n + 9], refs[n + 9 :]
     values, x, c, hid, dg, du, out, wg, wu, wd, sem_in, sem_w, sem_out = rest
     main = PEERS * 8
     half = PEERS // 2
     depth = 80 if tail else 64
     size = 40 if tail else 32
-    places = [values.at[0]] + [values.at[s, pl.ds(h * half, half)] for s in (1, 2, 3) for h in (0, 1)]
+    if tail:
+        places = [values.at[0], values.at[1], values.at[2]]
+        arrivals = ((0,), (1,), (2,), (3, 4))
+    else:
+        places = [values.at[0]] + [values.at[s, pl.ds(h * half, half)] for s in (1, 2) for h in (0, 1)]
+        arrivals = ((0,), (1, 2), (3, 4), (5, 6))
+    places += [values.at[3, pl.ds(h * half, half)] for h in (0, 1)]
     fetch = [
         pltpu.make_async_copy(p.at[:, 0:depth] if k == 0 else p, place, sem_in.at[k])
         for k, (p, place) in enumerate(zip(parts, places))
     ]
-    loads = [
-        pltpu.make_async_copy(w, v, sem_w.at[k])
-        for k, (w, v) in enumerate(zip(weights, (wg, wu, wd)))
-    ]
-    for copy in fetch + loads:
+    loads = []
+    for k, (w, v) in enumerate(zip(weights, (wg, wu, wd))):
+        n = w.shape[0] // 2
+        loads += [
+            pltpu.make_async_copy(w.at[pl.ds(h * n, n)], v.at[pl.ds(h * n, n)], sem_w.at[2 * k + h])
+            for h in range(2)
+        ]
+    for copy in fetch + loads[:2]:
         copy.start()
     saves = [
         pltpu.make_async_copy(v, o, sem_out.at[k])
@@ -154,31 +162,40 @@
 
     if tail:
         order = tail_order_back(8)
-    for source, (off, arriving) in enumerate(((0, (0,)), (3, (1, 2)), (1, (3, 4)), (2, (5, 6)))):
+    for source, (off, arriving) in enumerate(zip((0, 3, 1, 2), arrivals)):
         for k in arriving:
             fetch[k].wait()
+        if source == 3:
+            for load in loads[2:]:
+                load.start()
         value = values[source]
         for q2 in range(4):
             lo, hi = unpack_main(value, q2)
             dest = x if q2 < 2 else c
             col = at(off) + (q2 % 2) * 256
             dest[0:main, pl.ds(col, 256)] = jnp.concatenate([lo, hi], axis=1)
-        if tail:
-            rows = mm(order, value[:, 64:80, :].reshape(PEERS * 16, LANE)).astype(BF)
+    if tail:
+        lines = [values[source, :, 64:80, :].reshape(PEERS * 16, LANE) for source in range(TPN)]
+        rows = mm(order, jnp.concatenate(lines, axis=1)).astype(BF)
+        for source, off in enumerate((0, 3, 1, 2)):
+            cols = slice(source * LANE, (source + 1) * LANE)
             for q in range(8):
                 dest = x if q < 4 else c
                 dest[main : main + 64, pl.ds(at(off) + (q % 4) * LANE, LANE)] = rows[
-                    q * 64 : (q + 1) * 64
+                    q * 64 : (q + 1) * 64, cols
                 ]
+    xv, cv = x[...], c[...]
+    for load in loads[0:2]:
+        load.wait()
+    gate = mm(xv, wg[...])
+    for load in loads[2:4]:
+        load.wait()
+    up = mm(xv, wu[...])
+    for load in loads[4:6]:
+        load.wait()
+    dh = mm(cv, wd[...], 1, 1)
     saves[0].start()
     saves[1].start()
-    xv, cv = x[...], c[...]
-    loads[0].wait()
-    gate = mm(xv, wg[...])
-    loads[1].wait()
-    up = mm(xv, wu[...])
-    loads[2].wait()
-    dh = mm(cv, wd[...], 1, 1)
     sig = 1.0 / (1.0 + jnp.exp(-gate))
     silu = gate * sig
     hid[...] = (silu * up).astype(BF)
@@ -219,18 +236,26 @@
 
 
 def combine_a_body(got, idx, g, out):
+    out[...] = g[...].astype(F32) + jnp.concatenate(add_main(got, idx, 0), axis=1)
+
+
+def bring(pairs, sem):
+    copies = [pltpu.make_async_copy(src, dst, sem.at[k]) for k, (src, dst) in enumerate(pairs)]
+    for copy in copies:
+        copy.start()
+    return copies
+
+
+def combine_b_body(got, idx, so_far_far, out, res, so_far, sem_in, sem):
+    (early,) = bring([(so_far_far, so_far)], sem_in)
     n = PEERS * TPN
-    acc = add_main(got, idx, 0)
+    acc = add_main(got, idx, 2)
     m = iota((1, n * 8), 1)
     both = slot_mask(idx, (m // 32) * 2 + m % 2, 4)
     value = got[:, 32:40, :].reshape(n * 8, LANE)
     for q in range(4):
         acc[q] = acc[q] + mm(jnp.where((m // 2) % 4 == q, both, 0.0).astype(BF), value)
-    out[...] = g[...].astype(F32) + jnp.concatenate(acc, axis=1)
-
-
-def combine_b_body(got, idx, so_far, out, res, sem):
-    acc = add_main(got, idx, 2)
+    early.wait()
     res[...] = (so_far[...] + jnp.concatenate(acc, axis=1)).astype(BF)
     copies = [pltpu.make_async_copy(res, out.at[t], sem.at[t]) for t in range(TPN)]
     for copy in copies:
@@ -247,7 +272,16 @@
     return [p.astype(F32) for p in (hi, mid, low)]
 
 
-def scan_body(a_ref, b_ref, rows_b, cum, loc, gain, send):
+def scan_body(a_ref, b_ref, idx, weights, x, g, cum, loc, gain, send):
+    both = weighted(weights, g)
+    xv = x[...]
+    xm, cm = chosen(idx[2:3, :], idx[3:4, :], PEERS * 8, xv, both)
+    pack_main(xm, send, 0, 4)
+    pack_main(cm, send, 32, 4)
+    xt, ct = chosen(idx[4:5, :], idx[5:6, :], PEERS * 2, xv, both)
+    pieces = [v[:, q * LANE : (q + 1) * LANE] for v in (xt, ct) for q in range(4)]
+    tail = mm(tail_order(8), jnp.concatenate(pieces, axis=0).astype(BF))
+    send[:, 64:80, :] = tail.astype(BF).reshape(PEERS, 16, LANE)
     a = a_ref[...]
     row = iota((ROWS, CH), 0)
     ca, cb = a, b_ref[...]
@@ -267,8 +301,7 @@
             lines += [p[:, h * LANE : (h + 1) * LANE] for p in pieces]
     lines.append(jnp.zeros((4, LANE), F32))
     extra = jnp.concatenate(lines, axis=0).astype(BF)
-    send[:, 0:64, :] = rows_b[...]
-    send[:, 64:80, :] = jnp.broadcast_to(extra[None], (PEERS, 16, LANE))
+    send[:, 80:96, :] = jnp.broadcast_to(extra[None], (PEERS, 16, LANE))
     gn = jnp.where(row < ROWS - 1, pltpu.roll(a, ROWS - 1, 0), 1.0)
     step = 1
     while step < ROWS:
@@ -281,7 +314,7 @@
 def states_body(sp_ref, got, a, cum, loc, logits, q, rr, s1, gv, lru, r_out, coef):
     sp = sp_ref[0]
     row = iota((PEERS, CH), 0)
-    ends = got[:, 64:80, :].astype(F32)
+    ends = got[:, 80:96, :].astype(F32)
     line = iota((PEERS, 16, LANE), 1)
     halves = [jnp.sum(jnp.where(line // 3 == k, ends, 0.0), axis=1) for k in range(4)]
     gn = jnp.concatenate(halves[:2], axis=1)
@@ -311,11 +344,25 @@
     r_out[...] = rr[...] * (prev * a[...] - q[...])
 
 
-def reverse_body(full, wout, gv, s1, lru, a_ref, gate_pre, tail_sum, out, send, sem):
+def reverse_body(full, *refs):
+    far, (gate_pre, tail_sum, out, send), rest = refs[:5], refs[5:9], refs[9:]
+    (lru, wout, gv, a_ref, s1), (sem_in, sem) = rest[:5], rest[5:]
+    arrivals = bring(list(zip(far, (lru, wout, gv, a_ref, s1))), sem_in)
+    arrivals[0].wait()
+    lv = lru[...]
+    copies = []
+    for t in range(TPN):
+        part = mm(full[t], lv, 0, 0).astype(BF)
+        send[8 * t : 8 * t + 8, 0:64, :] = part.reshape(8, 64, CH)
+        rows = pl.ds(8 * t, 8), pl.ds(0, 64)
+        copies.append(pltpu.make_async_copy(send.at[rows], out.at[rows], sem.at[t]))
+        copies[t].start()
+    arrivals[1].wait()
     mixer = mm(full[0], wout[0:512, :])
     for t in range(1, TPN):
         mixer = mixer + mm(full[t], wout[t * 512 : (t + 1) * 512, :])
-    gate_pre[...] = mixer * s1[...]
+    arrivals[2].wait()
+    arrivals[3].wait()
     row = iota((ROWS, CH), 0)
     a = a_ref[...]
     gn = jnp.where(row < ROWS - 1, pltpu.roll(a, ROWS - 1, 0), 1.0)
@@ -326,18 +373,15 @@
         s = jnp.where(ok, s + gn * pltpu.roll(s, ROWS - step, 0), s)
         gn = jnp.where(ok, gn * pltpu.roll(gn, ROWS - step, 0), gn)
         step *= 2
-    tail_sum[...] = s
     term = a[0:1] * s[0:1]
     pieces = jnp.concatenate(in_three(term) + [jnp.zeros((5, CH), F32)], axis=0).astype(BF)
     send[:, 64:72, :] = jnp.broadcast_to(pieces[None], (PEERS, 8, CH))
-    lv = lru[...]
-    copies = []
-    for t in range(TPN):
-        part = mm(full[t], lv, 0, 0).astype(BF)
-        send[8 * t : 8 * t + 8, 0:64, :] = part.reshape(8, 64, CH)
-        rows = pl.ds(8 * t, 8)
-        copies.append(pltpu.make_async_copy(send.at[rows], out.at[rows], sem.at[t]))
-        copies[t].start()
+    rows = pl.ds(0, PEERS), pl.ds(64, 8)
+    copies.append(pltpu.make_async_copy(send.at[rows], out.at[rows], sem.at[TPN]))
+    copies[TPN].start()
+    tail_sum[...] = s
+    arrivals[4].wait()
+    gate_pre[...] = mixer * s1[...]
     for copy in copies:
         copy.wait()
 
@@ -363,14 +407,13 @@
 BACK = [(i, (i - 1) % TPN) for i in range(TPN)]
 
 
-def ring_parts(own, name):
+def move(value, where):
+    return lax.ppermute(value, "tp", where)
+
+
+def ring_parts_a(own):
     half = PEERS // 2
-    depth = own.shape[1] if name == "a" else 64
-    low, high = own[:half, :depth], own[half:, :depth]
-
-    def move(value, where):
-        return lax.ppermute(value, "tp", where)
-
+    low, high = own[:half], own[half:]
     left1 = move(low, RING)
     right2 = move(high, BACK)
     left2 = move(high, RING)
@@ -380,6 +423,16 @@
     return own, left1, left2, right1, right2, far1, far2
 
 
+def ring_parts_b(own):
+    half = PEERS // 2
+    rows = own[:, :80]
+    left = move(rows, RING)
+    right = move(rows, BACK)
+    far1 = move(left[:half], RING)
+    far2 = move(right[half:], BACK)
+    return own, left, right, far1, far2
+
+
 def shape(*dims, dtype=BF):
     return jax.ShapeDtypeStruct(dims, dtype)
 
@@ -396,15 +449,15 @@
     flops = 10 * rows * WIDTH * HID
     held = [(TPN, PEERS, 80 if tail else 64, LANE)] + [o.shape for o in out]
     held += [(WIDTH, HID), (WIDTH, HID), (HID, WIDTH)]
-    scratch = [pltpu.VMEM(dims, BF) for dims in held] + [dma(7), dma(3), dma(9)]
+    scratch = [pltpu.VMEM(dims, BF) for dims in held] + [dma(7), dma(6), dma(9)]
     *saved, partial_value = call(
         body,
         out,
-        11,
+        len(parts) + 4,
         flops,
         12 << 20,
         smem=(0,),
-        far=range(1, 11),
+        far=range(1, len(parts) + 4),
         far_out=range(6),
         scratch=scratch,
     )(tp, *parts, *weights)
@@ -431,13 +484,14 @@
     sp = lax.axis_index("sp").reshape(1).astype(jnp.int32)
     weights = (expert_gate_weight[0], expert_up_weight[0], expert_down_weight[0])
 
-    send_a, send_b, idx = call(
+    tokens = (chosen_expert_weight.T, middle_stream, output_gradient)
+    send_a, idx = call(
         pack_body,
-        [shape(PEERS, 80, LANE), shape(PEERS, 64, LANE), shape(8, ROWS, dtype=jnp.int32)],
+        [shape(PEERS, 64, LANE), shape(8, ROWS, dtype=jnp.int32)],
         4,
         1 << 30,
         3 << 20,
-    )(routes.T, chosen_expert_weight.T, middle_stream, output_gradient)
+    )(routes.T, *tokens)
     own_a = lax.all_to_all(send_a, "sp", 0, 0, tiled=True)
     first = lax.axis_index("tp") * 2
     recall_weight = lax.dynamic_slice_in_dim(recurrence_gate_weight, first, 2, 0)
@@ -464,12 +518,12 @@
     of_admit = driven * (1.0 - admit)
     tile = shape(ROWS, CH, dtype=F32)
     cum, loc, gain, send_b = call(
-        scan_body, [tile, tile, tile, shape(PEERS, 80, LANE)], 3, 1 << 28, 2 << 20
-    )(decay, driven, send_b)
+        scan_body, [tile, tile, tile, shape(PEERS, 96, LANE)], 6, 1 << 28, 2 << 20
+    )(decay, driven, idx, *tokens)
     own_a, send_b = lax.optimization_barrier((own_a, send_b))
     own_b = lax.all_to_all(send_b, "sp", 0, 0, tiled=True)
-    parts_a = ring_parts(own_a, "a")
-    parts_b = ring_parts(own_b, "b")
+    parts_a = ring_parts_a(own_a)
+    parts_b = ring_parts_b(own_b)
     s1, gelu_val, lru, of_log, coef = call(
         states_body,
         [tile, tile, shape(ROWS, CH), tile, shape(PEERS, CH, dtype=F32)],
@@ -479,15 +533,15 @@
         smem=(0,),
     )(sp, own_b, decay, cum, loc, output_gate_logits, minus, of_recall)
 
-    saved_a, part_a = expert_chain(True, tp, parts_a, weights)
+    saved_a, part_a = expert_chain(False, tp, parts_a, weights)
     got_a = lax.all_to_all(part_a, ("sp", "tp"), 0, 0, tiled=True)
-    saved_b, part_b = expert_chain(False, tp, parts_b, weights)
+    saved_b, part_b = expert_chain(True, tp, parts_b, weights)
     got_b = lax.all_to_all(part_b, ("sp", "tp"), 0, 0, tiled=True)
 
     x, cot, hid, dg, du = (jnp.concatenate([a, b], axis=0) for a, b in zip(saved_a, saved_b))
+    grad_down = mm(hid, cot, 0, 0).astype(BF)
     grad_gate = mm(x, dg, 0, 0).astype(BF)
     grad_up = mm(x, du, 0, 0).astype(BF)
-    grad_down = mm(hid, cot, 0, 0).astype(BF)
 
     columns = idx.T
     (so_far,) = call(combine_a_body, [shape(ROWS, 512, dtype=F32)], 3, 1 << 30, 2 << 20, 12)(
@@ -500,8 +554,9 @@
         1 << 30,
         3 << 20,
         12,
+        far=(2,),
         far_out=(0,),
-        scratch=[pltpu.VMEM((ROWS, 512), BF), dma(TPN)],
+        scratch=[pltpu.VMEM((ROWS, 512), BF), pltpu.VMEM((ROWS, 512), F32), dma(1), dma(TPN)],
     )(got_b, columns, so_far)
     full = lax.all_to_all(spread, "tp", 0, 0, tiled=True)
     grad_gate_pre, tail_sum, send = call(
@@ -511,9 +566,19 @@
         1 << 30,
         4 << 20,
         12,
+        far=range(1, 6),
         far_out=(2,),
-        scratch=[pltpu.VMEM((PEERS, 72, CH), BF), dma(TPN)],
-    )(full, recurrent_output_weight, gelu_val, s1, lru, decay)
+        scratch=[
+            pltpu.VMEM((PEERS, 72, CH), BF),
+            pltpu.VMEM((ROWS, CH), BF),
+            pltpu.VMEM((WIDTH, CH), BF),
+            pltpu.VMEM((ROWS, CH), F32),
+            pltpu.VMEM((ROWS, CH), F32),
+            pltpu.VMEM((ROWS, CH), F32),
+            dma(5),
+            dma(TPN + 1),
+        ],
+    )(full, lru, recurrent_output_weight, gelu_val, decay, s1)
     got = lax.all_to_all(send, "sp", 0, 0, tiled=True)
     grad_out_proj, grad_input = call(
         final_body, [shape(64, CH, dtype=F32), tile], 9, 1 << 28, 3 << 20, 8

time: 193 us -> 184 us (0.953)
  waiting for transfers between devices: 71 us -> 59 us
  local copies, waits for them, and re-layouts: 8.61 us -> 10.6 us
    ppermute x12 -> x10, waiting for transfers between devices: 38.6 us -> 23.5 us  [move(): return lax.ppermute(value, 'tp', where)]
    all_to_all x1, starting transfers between devices: 5.07 us -> 11.3 us  [per_device(): got_a = lax.all_to_all(part_a, ('sp', 'tp'), 0, 0, tiled=True)]
    all_to_all x1, waiting for transfers between devices: 14.9 us -> 20.8 us  [per_device(): got_b = lax.all_to_all(part_b, ('sp', 'tp'), 0, 0, tiled=True)]
    all_to_all x1, waiting for transfers between devices: 0.01 us -> 2.73 us  [per_device(): own_b = lax.all_to_all(send_b, 'sp', 0, 0, tiled=True)]
    all_to_all x1, waiting for transfers between devices: 4.72 us -> 2.03 us  [per_device(): full = lax.all_to_all(spread, 'tp', 0, 0, tiled=True)]
    all_to_all x1, waiting for transfers between devices: 7.13 us -> 4.79 us  [per_device(): own_a = lax.all_to_all(send_a, 'sp', 0, 0, tiled=True)]
    all_to_all x1, starting transfers between devices: 6.14 us -> 3.96 us  [per_device(): own_b = lax.all_to_all(send_b, 'sp', 0, 0, tiled=True)]
    ppermute x12 -> x10, starting transfers between devices: 14.9 us -> 13.7 us  [move(): return lax.ppermute(value, 'tp', where)]
  transfers between devices with their start and end apart: 18 -> 16, of which waited for: 13 -> 8; matrix products, arithmetic and copies ran while one was open for 12% -> 13% of each run, Pallas kernels for 16% -> 16%
where the time goes in v2:
time: 184 us
  waiting for transfers between devices  59 us (32%)
  starting transfers between devices  55.2 us (30%)
  Pallas kernels  39.1 us (21%)
  matrix products  16.7 us (9%)
  local copies, waits for them, and re-layouts  10.6 us (6%)
    ppermute x10, waiting for transfers between devices, move(): return lax.ppermute(value, 'tp', where)  23.5 us
    pallas_call x2, Pallas kernels, expert_chain(): call(body, out, len(parts) + 4, flops, 12 << 20, smem=(0,), far=range(1,...  22.8 us
    all_to_all x1, waiting for transfers between devices, per_device(): got_b = lax.all_to_all(part_b, ('sp', 'tp'), 0, 0, tiled=True)  20.8 us
    dot_general x3, matrix products, mm(): lax.dot_general(a, b, (((ca,), (cb,)), ((), ())), preferred_element_type=...  16.3 us
    ppermute x10, starting transfers between devices, move(): return lax.ppermute(value, 'tp', where)  13.7 us
    all_to_all x1, starting transfers between devices, per_device(): got_a = lax.all_to_all(part_a, ('sp', 'tp'), 0, 0, tiled=True)  11.3 us
    all_to_all x1, starting transfers between devices, per_device(): own_a = lax.all_to_all(send_a, 'sp', 0, 0, tiled=True)  9.72 us
    all_to_all x1, starting transfers between devices, per_device(): got_b = lax.all_to_all(part_b, ('sp', 'tp'), 0, 0, tiled=True)  8.06 us
  transfers between devices with their start and end apart: 16, of which 8 were waited for; matrix products, arithmetic and copies ran while one was open for 13% of the time, Pallas kernels for 16%

profile of v2, /device:TPU:1, one launch (start us, length us, event | category | flops | bytes accessed | tf_op | source)
XLA Modules:
  0.0 183.5 jit_solution(11273919229814286772)
XLA Ops:
  0.6 2.4 %shard_map.181 = (bf16[32,64,128]{2,1,0:T(8,128)(2,1)}, s32[8,192]{1,0:T(8,128)}) custom-call(s32[2,192]{1,0:T(2,128)} %bitcast.65, f32[2,192]{1,0:T(2,128)} %bitcast.66, bf16[192,512]{1,0:T(8,128)(2,1)} %x.3, bf16[192,512]{1,0:T(8,128)(2,1)} %g.5), custom_call_target="tpu_custom_call" | custom-call | flops 1073741824 | bytes 3145728 | tf_op jit(solution)/shard_map/pallas_call | solution.py:488
  3.1 9.7 %all-to-all-start = ((bf16[32,64,128]{2,1,0:T(8,128)(2,1)}), bf16[32,64,128]{2,1,0:T(8,128)(2,1)S(1)}, u32[]{:S(2)}, u32[]{:S(2)}) async-start(bf16[32,64,128]{2,1,0:T(8,128)(2,1)} %get-tuple-element.36), calls=%async_computation | async-start | bytes 1048576 | tf_op jit(solution)/shard_map/all_to_all | solution.py:495
  16.0 3.5 %shard_map.182 = (f32[192,256]{1,0:T(8,128)}, f32[192,256]{1,0:T(8,128)}, f32[192,256]{1,0:T(8,128)}, bf16[32,96,128]{2,1,0:T(8,128)(2,1)}) custom-call(f32[192,256]{1,0:T(8,128)} %get-tuple-element.74.a_ref.a.refs_3_, f32[192,256]{1,0:T(8,128)} %get-tuple-element.67.b_ref, s32[8,192]{1,0:T(8,128)} %get-tuple-element.37.idx, f32[2,192]{1,0:T(2,128)} %bitcast.67, ...), custom_call_target="tpu_custom_call" | custom-call | flops 268435456 | bytes 2097152 | tf_op jit(solution)/shard_map/pallas_call | solution.py:520
  19.5 4.8 %all-to-all-done.refs_1_ = bf16[32,64,128]{2,1,0:T(8,128)(2,1)S(1)} async-done(((bf16[32,64,128]{2,1,0:T(8,128)(2,1)}), bf16[32,64,128]{2,1,0:T(8,128)(2,1)S(1)}, u32[]{:S(2)}, u32[]{:S(2)}) %all-to-all-start) | async-done | bytes 524320 | tf_op jit(solution)/shard_map/all_to_all | solution.py:495
  24.2 4.0 %all-to-all-start.1 = ((bf16[32,96,128]{2,1,0:T(8,128)(2,1)}), bf16[32,96,128]{2,1,0:T(8,128)(2,1)S(1)}, u32[]{:S(2)}, u32[]{:S(2)}) async-start(bf16[32,96,128]{2,1,0:T(8,128)(2,1)} %get-tuple-element.41), calls=%async_computation.1 | async-start | bytes 1572864 | tf_op jit(solution)/shard_map/all_to_all | solution.py:524
  28.3 1.3 collective-permute-start
  29.5 1.5 collective-permute-start.3
  31.0 2.7 %collective-permute-start.2 = (bf16[16,64,128]{2,1,0:T(8,128)(2,1)S(1)}, bf16[16,64,128]{2,1,0:T(8,128)(2,1)}, u32[]{:S(2)}, u32[]{:S(2)}) collective-permute-start(bf16[16,64,128]{2,1,0:T(8,128)(2,1)S(1)} %get-tuple-element.71), channel_id=1, source_target_pairs={{0,3},{1,0},{2,1},{3,2},{4,7},{5,4},{6,5},{7,6},{8,11},{9,8},{10,9... | collective-permute-start | bytes 786440 | tf_op jit(solution)/shard_map/ppermute | solution.py:411
  33.7 3.5 %collective-permute-done.refs_2_ = bf16[16,64,128]{2,1,0:T(8,128)(2,1)} collective-permute-done((bf16[16,64,128]{2,1,0:T(8,128)(2,1)S(1)}, bf16[16,64,128]{2,1,0:T(8,128)(2,1)}, u32[]{:S(2)}, u32[]{:S(2)}) %collective-permute-start) | collective-permute-done | bytes 262176 | tf_op jit(solution)/shard_map/ppermute | solution.py:411
  37.2 2.7 %collective-permute-start.5 = (bf16[16,64,128]{2,1,0:T(8,128)(2,1)}, bf16[16,64,128]{2,1,0:T(8,128)(2,1)}, u32[]{:S(2)}, u32[]{:S(2)}) collective-permute-start(bf16[16,64,128]{2,1,0:T(8,128)(2,1)} %collective-permute-done.3.refs_5_), channel_id=1, source_target_pairs={{0,3},{1,0},{2,1},{3,2},{4,7},{5,4},{6,5},{7,6},{8,11},{9,8},{10,9... | collective-permute-start | bytes 786440 | tf_op jit(solution)/shard_map/ppermute | solution.py:411
  39.8 2.7 %all-to-all-done.1.refs_1_.got = bf16[32,96,128]{2,1,0:T(8,128)(2,1)S(1)} async-done(((bf16[32,96,128]{2,1,0:T(8,128)(2,1)}), bf16[32,96,128]{2,1,0:T(8,128)(2,1)S(1)}, u32[]{:S(2)}, u32[]{:S(2)}) %all-to-all-start.1) | async-done | bytes 786464 | tf_op jit(solution)/shard_map/all_to_all | solution.py:524
  43.9 1.5 collective-permute-start.7
  45.4 3.0 %collective-permute-done.4.refs_6_ = bf16[16,64,128]{2,1,0:T(8,128)(2,1)} collective-permute-done((bf16[16,64,128]{2,1,0:T(8,128)(2,1)}, bf16[16,64,128]{2,1,0:T(8,128)(2,1)}, u32[]{:S(2)}, u32[]{:S(2)}) %collective-permute-start.4) | collective-permute-done | bytes 262176 | tf_op jit(solution)/shard_map/ppermute | solution.py:411
  48.4 10.1 %shard_map.183 = (bf16[256,2048]{1,0:T(8,128)(2,1)}, bf16[256,2048]{1,0:T(8,128)(2,1)}, bf16[256,896]{1,0:T(8,128)(2,1)}, bf16[256,896]{1,0:T(8,128)(2,1)}, bf16...) custom-call(s32[1]{0:T(128)} %bitcast.refs_0_, bf16[32,64,128]{2,1,0:T(8,128)(2,1)} %copy-done.12, ...), custom_call_target="tpu_custom_call" | custom-call | flops 4697620480 | bytes 12582912 | tf_op jit(solution)/shard_map/pallas_call | solution.py:453
  58.5 11.3 %all-to-all-start.3 = ((bf16[128,32,128]{2,1,0:T(8,128)(2,1)}), bf16[128,32,128]{2,1,0:T(8,128)(2,1)S(1)}, u32[]{:S(2)}, u32[]{:S(2)}) async-start(bf16[128,32,128]{2,1,0:T(8,128)(2,1)} %bitcast.58), calls=%async_computation.3 | async-start | bytes 2097152 | tf_op jit(solution)/shard_map/all_to_all | solution.py:537
  70.8 1.4 collective-permute-start.8
  72.3 1.4 collective-permute-start.9
  73.7 17.0 %collective-permute-done.8.refs_4_ = bf16[16,80,128]{2,1,0:T(8,128)(2,1)S(1)} collective-permute-done((bf16[16,80,128]{2,1,0:T(8,128)(2,1)S(1)}, bf16[16,80,128]{2,1,0:T(8,128)(2,1)S(1)}, u32[]{:S(2)}, u32[]{:S(2)}) %collective-permute-start.8) | collective-permute-done | bytes 327712 | tf_op jit(solution)/shard_map/ppermute | solution.py:411
  92.1 12.7 %shard_map.184 = (bf16[320,2048]{1,0:T(8,128)(2,1)}, bf16[320,2048]{1,0:T(8,128)(2,1)}, bf16[320,896]{1,0:T(8,128)(2,1)}, bf16[320,896]{1,0:T(8,128)(2,1)}, bf16...) custom-call(s32[1]{0:T(128)} %bitcast.refs_0_, bf16[32,96,128]{2,1,0:T(8,128)(2,1)} %copy-done.11, ...), custom_call_target="tpu_custom_call" | custom-call | flops 5872025600 | bytes 12582912 | tf_op jit(solution)/shard_map/pallas_call | solution.py:453
  104.8 8.1 %all-to-all-start.2 = ((bf16[128,40,128]{2,1,0:T(8,128)(2,1)}), bf16[128,40,128]{2,1,0:T(8,128)(2,1)S(1)}, u32[]{:S(2)}, u32[]{:S(2)}) async-start(bf16[128,40,128]{2,1,0:T(8,128)(2,1)} %bitcast.57), calls=%async_computation.2 | async-start | bytes 2621440 | tf_op jit(solution)/shard_map/all_to_all | solution.py:539
  114.4 20.8 %all-to-all-done.2.got = bf16[128,40,128]{2,1,0:T(8,128)(2,1)S(1)} async-done(((bf16[128,40,128]{2,1,0:T(8,128)(2,1)}), bf16[128,40,128]{2,1,0:T(8,128)(2,1)S(1)}, u32[]{:S(2)}, u32[]{:S(2)}) %all-to-all-start.2) | async-done | bytes 1310752 | tf_op jit(solution)/shard_map/all_to_all | solution.py:539
  136.2 2.2 %shard_map.186 = bf16[4,192,512]{2,1,0:T(8,128)(2,1)} custom-call(bf16[128,40,128]{2,1,0:T(8,128)(2,1)S(1)} %all-to-all-done.2.got, s32[192,8]{1,0:T(8,128)S(1)} %bitcast.56, f32[192,512]{1,0:T(8,128)S(1)} %copy-done.10), custom_call_target="tpu_custom_call" | custom-call | flops 1073741824 | bytes 3145728 | tf_op jit(solution)/shard_map/pallas_call | solution.py:550
  138.4 3.7 %all-to-all-start.4 = ((bf16[4,192,512]{2,1,0:T(8,128)(2,1)}), bf16[4,192,512]{2,1,0:T(8,128)(2,1)S(1)}, u32[]{:S(2)}, u32[]{:S(2)}) async-start(bf16[4,192,512]{2,1,0:T(8,128)(2,1)} %shard_map.186), calls=%async_computation.4 | async-start | bytes 1572864 | tf_op jit(solution)/shard_map/all_to_all | solution.py:561
  142.2 2.5 %constant_dynamic-update-slice_fusion.1 = bf16[576,2048]{1,0:T(8,128)(2,1)} fusion(bf16[256,2048]{1,0:T(8,128)(2,1)} %get-tuple-element.40), kind=kLoop, calls=%fused_computation.42 | loop fusion | bytes 2097152
  144.6 2.7 %shard_map.187 = (f32[192,256]{1,0:T(8,128)}, f32[192,256]{1,0:T(8,128)}, bf16[192,256]{1,0:T(8,128)(2,1)}, f32[192,256]{1,0:T(8,128)}, f32[32,256]{1,0:T(8,128)}) custom-call(s32[1]{0:T(128)} %bitcast.14.sp_ref, bf16[32,96,128]{2,1,0:T(8,128)(2,1)} %copy-done.11, f32[192,256]{1,0:T(8,128)} %get-tuple-element.74.a_ref.a.refs_3_, ...), custom_call_target="tpu_custom_call" | custom-call | flops 268435456 | bytes 2097152 | tf_op jit(solution)/shard_map/pallas_call | solution.py:527
  147.4 4.5 %convert_bitcast_fusion = bf16[1,896,2048]{2,1,0:T(8,128)(2,1)} fusion(bf16[320,2048]{1,0:T(8,128)(2,1)S(1)} %copy-done.26, bf16[256,2048]{1,0:T(8,128)(2,1)S(1)} %copy-done.22, bf16[320,896]{1,0:T(8,128)(2,1)S(1)} %copy-done.29, bf16[256,896]{1,0:T(8,128)(2,1)S(1)} %copy-done.25), kind=kOutput, calls=%fused_computation | convolution fusion | flops 2122547200 | bytes 7061504 | tf_op jit(solution)/shard_map/dot_general | solution.py:23
  151.9 2.0 %all-to-all-done.4.full = bf16[4,192,512]{2,1,0:T(8,128)(2,1)S(1)} async-done(((bf16[4,192,512]{2,1,0:T(8,128)(2,1)}), bf16[4,192,512]{2,1,0:T(8,128)(2,1)S(1)}, u32[]{:S(2)}, u32[]{:S(2)}) %all-to-all-start.4) | async-done | bytes 786464 | tf_op jit(solution)/shard_map/all_to_all | solution.py:561
  155.2 3.9 %shard_map.188 = (f32[192,256]{1,0:T(8,128)}, f32[192,256]{1,0:T(8,128)S(1)}, bf16[32,72,256]{2,1,0:T(8,128)(2,1)}) custom-call(bf16[4,192,512]{2,1,0:T(8,128)(2,1)S(1)} %all-to-all-done.4.full, bf16[192,256]{1,0:T(8,128)(2,1)S(1)} %copy-done.8, bf16[2048,256]{1,0:T(8,128)(2,1)S(1)} %copy-done.4, f32[192,256]{1,0:T(8,128)S(1)} %copy-done.7, ...), custom_call_target="tpu_custom_call" | custom-call | flops 1073741824 | bytes 4194304 | tf_op jit(solution)/shard_map/pallas_call | solution.py:562
  159.1 4.8 %all-to-all-start.5 = ((bf16[32,72,256]{2,1,0:T(8,128)(2,1)}), bf16[32,72,256]{2,1,0:T(8,128)(2,1)S(1)}, u32[]{:S(2)}, u32[]{:S(2)}) async-start(bf16[32,72,256]{2,1,0:T(8,128)(2,1)} %get-tuple-element.58), calls=%async_computation.5 | async-start | bytes 2359296 | tf_op jit(solution)/shard_map/all_to_all | solution.py:582
  165.5 7.0 %convert_bitcast_fusion.1 = bf16[1,2048,896]{2,1,0:T(8,128)(2,1)} fusion(bf16[576,2048]{1,0:T(8,128)(2,1)} %constant_dynamic-update-slice_fusion, bf16[320,896]{1,0:T(8,128)(2,1)S(1)} %copy-done.28, bf16[256,896]{1,0:T(8,128)(2,1)S(1)} %copy-done.24), kind=kOutput, calls=%fused_computation.1 | convolution fusion | flops 2117828608 | bytes 7061504 | tf_op jit(solution)/shard_map/dot_general | solution.py:23
  172.6 4.8 %convert_bitcast_fusion.2 = bf16[1,2048,896]{2,1,0:T(8,128)(2,1)} fusion(bf16[576,2048]{1,0:T(8,128)(2,1)S(1)} %copy-done.14, bf16[320,896]{1,0:T(8,128)(2,1)S(1)} %copy-done.27, bf16[256,896]{1,0:T(8,128)(2,1)S(1)} %copy-done.23), kind=kOutput, calls=%fused_computation.2 | convolution fusion | flops 2117828608 | bytes 7061504 | tf_op jit(solution)/shard_map/dot_general | solution.py:23
  177.4 5.1 %all-to-all-done.5.got = bf16[32,72,256]{2,1,0:T(8,128)(2,1)S(1)} async-done(((bf16[32,72,256]{2,1,0:T(8,128)(2,1)}), bf16[32,72,256]{2,1,0:T(8,128)(2,1)S(1)}, u32[]{:S(2)}, u32[]{:S(2)}) %all-to-all-start.5) | async-done | bytes 1179680 | tf_op jit(solution)/shard_map/all_to_all | solution.py:582
  (85 shorter events, 13.3 us)
Async XLA Ops:
  0.6 13.1 %copy-start.15 = (bf16[192,256]{1,0:T(8,128)(2,1)S(1)}, bf16[192,256]{1,0:T(8,128)(2,1)}, u32[]{:S(2)}) copy-start(bf16[192,256]{1,0:T(8,128)(2,1)} %param.22) | copy-start | bytes 294916
  3.1 11.1 %copy-start.19 = (f32[256]{0:T(256)S(1)}, f32[256]{0:T(256)}, u32[]{:S(2)}) copy-start(f32[256]{0:T(256)} %param.26) | copy-start | bytes 3076
  3.1 11.1 %copy-start.16 = (f32[192,256]{1,0:T(8,128)S(1)}, f32[192,256]{1,0:T(8,128)}, u32[]{:S(2)}) copy-start(f32[192,256]{1,0:T(8,128)} %param.27) | copy-start | bytes 589828
  3.1 21.2 %all-to-all-start = ((bf16[32,64,128]{2,1,0:T(8,128)(2,1)}), bf16[32,64,128]{2,1,0:T(8,128)(2,1)S(1)}, u32[]{:S(2)}, u32[]{:S(2)}) async-start(bf16[32,64,128]{2,1,0:T(8,128)(2,1)} %get-tuple-element.36), calls=%async_computation | async-start | bytes 1048576 | tf_op jit(solution)/shard_map/all_to_all | solution.py:495
  24.2 24.2 %copy-start.12 = (bf16[32,64,128]{2,1,0:T(8,128)(2,1)}, bf16[32,64,128]{2,1,0:T(8,128)(2,1)S(1)}, u32[]{:S(2)}) copy-start(bf16[32,64,128]{2,1,0:T(8,128)(2,1)S(1)} %all-to-all-done.refs_1_) | copy-start | bytes 1572868
  24.2 18.3 %all-to-all-start.1 = ((bf16[32,96,128]{2,1,0:T(8,128)(2,1)}), bf16[32,96,128]{2,1,0:T(8,128)(2,1)S(1)}, u32[]{:S(2)}, u32[]{:S(2)}) async-start(bf16[32,96,128]{2,1,0:T(8,128)(2,1)} %get-tuple-element.41), calls=%async_computation.1 | async-start | bytes 1572864 | tf_op jit(solution)/shard_map/all_to_all | solution.py:524
  28.3 8.9 %collective-permute-start = (bf16[16,64,128]{2,1,0:T(8,128)(2,1)S(1)}, bf16[16,64,128]{2,1,0:T(8,128)(2,1)}, u32[]{:S(2)}, u32[]{:S(2)}) collective-permute-start(bf16[16,64,128]{2,1,0:T(8,128)(2,1)S(1)} %get-tuple-element.71), channel_id=1, source_target_pairs={{0,1},{1,2},{2,3},{3,0},{4,5},{5,6},{6,7},{7,4},{8,9},{9,10},{10,1... | collective-permute-start | bytes 786440 | tf_op jit(solution)/shard_map/ppermute | solution.py:411
  29.5 7.6 %collective-permute-start.3 = (bf16[16,64,128]{2,1,0:T(8,128)(2,1)S(1)}, bf16[16,64,128]{2,1,0:T(8,128)(2,1)}, u32[]{:S(2)}, u32[]{:S(2)}) collective-permute-start(bf16[16,64,128]{2,1,0:T(8,128)(2,1)S(1)} %get-tuple-element.70), channel_id=1, source_target_pairs={{0,3},{1,0},{2,1},{3,2},{4,7},{5,4},{6,5},{7,6},{8,11},{9,8},{10,9... | collective-permute-start | bytes 786440 | tf_op jit(solution)/shard_map/ppermute | solution.py:411
  31.0 12.9 %collective-permute-start.1 = (bf16[16,64,128]{2,1,0:T(8,128)(2,1)S(1)}, bf16[16,64,128]{2,1,0:T(8,128)(2,1)}, u32[]{:S(2)}, u32[]{:S(2)}) collective-permute-start(bf16[16,64,128]{2,1,0:T(8,128)(2,1)S(1)} %get-tuple-element.70), channel_id=1, source_target_pairs={{0,1},{1,2},{2,3},{3,0},{4,5},{5,6},{6,7},{7,4},{8,9},{9,10},{10,1... | collective-permute-start | bytes 786440 | tf_op jit(solution)/shard_map/ppermute | solution.py:411
  31.0 14.4 %collective-permute-start.2 = (bf16[16,64,128]{2,1,0:T(8,128)(2,1)S(1)}, bf16[16,64,128]{2,1,0:T(8,128)(2,1)}, u32[]{:S(2)}, u32[]{:S(2)}) collective-permute-start(bf16[16,64,128]{2,1,0:T(8,128)(2,1)S(1)} %get-tuple-element.71), channel_id=1, source_target_pairs={{0,3},{1,0},{2,1},{3,2},{4,7},{5,4},{6,5},{7,6},{8,11},{9,8},{10,9... | collective-permute-start | bytes 786440 | tf_op jit(solution)/shard_map/ppermute | solution.py:411
  37.2 11.2 %collective-permute-start.4 = (bf16[16,64,128]{2,1,0:T(8,128)(2,1)}, bf16[16,64,128]{2,1,0:T(8,128)(2,1)}, u32[]{:S(2)}, u32[]{:S(2)}) collective-permute-start(bf16[16,64,128]{2,1,0:T(8,128)(2,1)} %collective-permute-done.refs_2_), channel_id=1, source_target_pairs={{0,1},{1,2},{2,3},{3,0},{4,5},{5,6},{6,7},{7,4},{8,9},{9,10},{10,1... | collective-permute-start | bytes 786440 | tf_op jit(solution)/shard_map/ppermute | solution.py:411
  37.2 11.2 %collective-permute-start.5 = (bf16[16,64,128]{2,1,0:T(8,128)(2,1)}, bf16[16,64,128]{2,1,0:T(8,128)(2,1)}, u32[]{:S(2)}, u32[]{:S(2)}) collective-permute-start(bf16[16,64,128]{2,1,0:T(8,128)(2,1)} %collective-permute-done.3.refs_5_), channel_id=1, source_target_pairs={{0,3},{1,0},{2,1},{3,2},{4,7},{5,4},{6,5},{7,6},{8,11},{9,8},{10,9... | collective-permute-start | bytes 786440 | tf_op jit(solution)/shard_map/ppermute | solution.py:411
  42.6 15.9 %copy-start.11 = (bf16[32,96,128]{2,1,0:T(8,128)(2,1)}, bf16[32,96,128]{2,1,0:T(8,128)(2,1)S(1)}, u32[]{:S(2)}) copy-start(bf16[32,96,128]{2,1,0:T(8,128)(2,1)S(1)} %all-to-all-done.1.refs_1_.got) | copy-start | bytes 2359300
  42.6 27.2 %collective-permute-start.6 = (bf16[32,80,128]{2,1,0:T(8,128)(2,1)S(1)}, bf16[32,80,128]{2,1,0:T(8,128)(2,1)}, u32[]{:S(2)}, u32[]{:S(2)}) collective-permute-start(bf16[32,80,128]{2,1,0:T(8,128)(2,1)S(1)} %slice.20), channel_id=1, source_target_pairs={{0,1},{1,2},{2,3},{3,0},{4,5},{5,6},{6,7},{7,4},{8,9},{9,10},{10,1... | collective-permute-start | bytes 1966088 | tf_op jit(solution)/shard_map/ppermute | solution.py:411
  43.9 28.3 %collective-permute-start.7 = (bf16[32,80,128]{2,1,0:T(8,128)(2,1)S(1)}, bf16[32,80,128]{2,1,0:T(8,128)(2,1)S(1)}, u32[]{:S(2)}, u32[]{:S(2)}) collective-permute-start(bf16[32,80,128]{2,1,0:T(8,128)(2,1)S(1)} %slice.20), channel_id=1, source_target_pairs={{0,3},{1,0},{2,1},{3,2},{4,7},{5,4},{6,5},{7,6},{8,11},{9,8},{10,9... | collective-permute-start | bytes 1966088 | tf_op jit(solution)/shard_map/ppermute | solution.py:411
  58.5 46.3 %all-to-all-start.3 = ((bf16[128,32,128]{2,1,0:T(8,128)(2,1)}), bf16[128,32,128]{2,1,0:T(8,128)(2,1)S(1)}, u32[]{:S(2)}, u32[]{:S(2)}) async-start(bf16[128,32,128]{2,1,0:T(8,128)(2,1)} %bitcast.58), calls=%async_computation.3 | async-start | bytes 2097152 | tf_op jit(solution)/shard_map/all_to_all | solution.py:537
  70.8 19.8 %collective-permute-start.8 = (bf16[16,80,128]{2,1,0:T(8,128)(2,1)S(1)}, bf16[16,80,128]{2,1,0:T(8,128)(2,1)S(1)}, u32[]{:S(2)}, u32[]{:S(2)}) collective-permute-start(bf16[16,80,128]{2,1,0:T(8,128)(2,1)S(1)} %slice.21), channel_id=1, source_target_pairs={{0,1},{1,2},{2,3},{3,0},{4,5},{5,6},{6,7},{7,4},{8,9},{9,10},{10,1... | collective-permute-start | bytes 983048 | tf_op jit(solution)/shard_map/ppermute | solution.py:411
  72.2 18.4 %copy-start.17 = (bf16[32,80,128]{2,1,0:T(8,128)(2,1)}, bf16[32,80,128]{2,1,0:T(8,128)(2,1)S(1)}, u32[]{:S(2)}) copy-start(bf16[32,80,128]{2,1,0:T(8,128)(2,1)S(1)} %collective-permute-done.7.refs_3_) | copy-start | bytes 1966084
  72.3 18.4 %collective-permute-start.9 = (bf16[16,80,128]{2,1,0:T(8,128)(2,1)S(1)}, bf16[16,80,128]{2,1,0:T(8,128)(2,1)S(1)}, u32[]{:S(2)}, u32[]{:S(2)}) collective-permute-start(bf16[16,80,128]{2,1,0:T(8,128)(2,1)S(1)} %slice.22), channel_id=1, source_target_pairs={{0,3},{1,0},{2,1},{3,2},{4,7},{5,4},{6,5},{7,6},{8,11},{9,8},{10,9... | collective-permute-start | bytes 983048 | tf_op jit(solution)/shard_map/ppermute | solution.py:411
  104.8 8.1 %copy-start.18 = (s32[8,192]{1,0:T(8,128)S(1)}, s32[8,192]{1,0:T(8,128)}, u32[]{:S(2)}) copy-start(s32[8,192]{1,0:T(8,128)} %get-tuple-element.37.idx) | copy-start | bytes 18436
  104.8 8.2 %copy-start.5 = (bf16[192,512]{1,0:T(8,128)(2,1)S(1)}, bf16[192,512]{1,0:T(8,128)(2,1)}, u32[]{:S(2)}) copy-start(bf16[192,512]{1,0:T(8,128)(2,1)} %g.5) | copy-start | bytes 589828
  104.8 30.4 %all-to-all-start.2 = ((bf16[128,40,128]{2,1,0:T(8,128)(2,1)}), bf16[128,40,128]{2,1,0:T(8,128)(2,1)S(1)}, u32[]{:S(2)}, u32[]{:S(2)}) async-start(bf16[128,40,128]{2,1,0:T(8,128)(2,1)} %bitcast.57), calls=%async_computation.2 | async-start | bytes 2621440 | tf_op jit(solution)/shard_map/all_to_all | solution.py:539
  138.4 15.5 %all-to-all-start.4 = ((bf16[4,192,512]{2,1,0:T(8,128)(2,1)}), bf16[4,192,512]{2,1,0:T(8,128)(2,1)S(1)}, u32[]{:S(2)}, u32[]{:S(2)}) async-start(bf16[4,192,512]{2,1,0:T(8,128)(2,1)} %shard_map.186), calls=%async_computation.4 | async-start | bytes 1572864 | tf_op jit(solution)/shard_map/all_to_all | solution.py:561
  147.3 6.6 %copy-start = (f32[192,256]{1,0:T(8,128)S(1)}, f32[192,256]{1,0:T(8,128)}, u32[]{:S(2)}) copy-start(f32[192,256]{1,0:T(8,128)} %get-tuple-element.74.a_ref.a.refs_3_) | copy-start | bytes 589828
  155.2 8.7 %copy-start.13 = (bf16[320,2048]{1,0:T(8,128)(2,1)S(1)}, bf16[320,2048]{1,0:T(8,128)(2,1)}, u32[]{:S(2)}) copy-start(bf16[320,2048]{1,0:T(8,128)(2,1)} %get-tuple-element.42) | copy-start | bytes 3932164
  159.1 23.5 %all-to-all-start.5 = ((bf16[32,72,256]{2,1,0:T(8,128)(2,1)}), bf16[32,72,256]{2,1,0:T(8,128)(2,1)S(1)}, u32[]{:S(2)}, u32[]{:S(2)}) async-start(bf16[32,72,256]{2,1,0:T(8,128)(2,1)} %get-tuple-element.58), calls=%async_computation.5 | async-start | bytes 2359296 | tf_op jit(solution)/shard_map/all_to_all | solution.py:582
  165.5 7.0 %copy-start.14 = (bf16[576,2048]{1,0:T(8,128)(2,1)S(1)}, bf16[576,2048]{1,0:T(8,128)(2,1)}, u32[]{:S(2)}) copy-start(bf16[576,2048]{1,0:T(8,128)(2,1)} %constant_dynamic-update-slice_fusion) | copy-start | bytes 7077892
  165.5 7.0 %copy-start.23 = (bf16[256,896]{1,0:T(8,128)(2,1)S(1)}, bf16[256,896]{1,0:T(8,128)(2,1)}, u32[]{:S(2)}) copy-start(bf16[256,896]{1,0:T(8,128)(2,1)} %get-tuple-element.43) | copy-start | bytes 1376260
  165.5 7.0 %copy-start.27 = (bf16[320,896]{1,0:T(8,128)(2,1)S(1)}, bf16[320,896]{1,0:T(8,128)(2,1)}, u32[]{:S(2)}) copy-start(bf16[320,896]{1,0:T(8,128)(2,1)} %get-tuple-element.44) | copy-start | bytes 1720324
  172.5 10.0 %copy-start.1 = (f32[192,256]{1,0:T(8,128)S(1)}, f32[192,256]{1,0:T(8,128)}, u32[]{:S(2)}) copy-start(f32[192,256]{1,0:T(8,128)} %get-tuple-element.61.gain) | copy-start | bytes 589828
  172.5 10.0 %copy-start.2 = (f32[192,256]{1,0:T(8,128)S(1)}, f32[192,256]{1,0:T(8,128)}, u32[]{:S(2)}) copy-start(f32[192,256]{1,0:T(8,128)} %get-tuple-element.62.rr) | copy-start | bytes 589828
  172.6 10.0 %copy-start.3 = (f32[32,256]{1,0:T(8,128)S(1)}, f32[32,256]{1,0:T(8,128)}, u32[]{:S(2)}) copy-start(f32[32,256]{1,0:T(8,128)} %get-tuple-element.59.coef) | copy-start | bytes 98308
  (14 other events, 47.6 us)

commit v3 on v2

--- a/solution.py
+++ b/solution.py
@@ -118,20 +118,14 @@
 
 
 def chain_body(tail, tp_ref, *refs):
-    n = 5 if tail else 7
-    parts, weights, outs, rest = refs[:n], refs[n : n + 3], refs[n + 3 : n + 9], refs[n + 9 :]
+    parts, weights, outs, rest = refs[:7], refs[7:10], refs[10:16], refs[16:]
     values, x, c, hid, dg, du, out, wg, wu, wd, sem_in, sem_w, sem_out = rest
     main = PEERS * 8
     half = PEERS // 2
     depth = 80 if tail else 64
     size = 40 if tail else 32
-    if tail:
-        places = [values.at[0], values.at[1], values.at[2]]
-        arrivals = ((0,), (1,), (2,), (3, 4))
-    else:
-        places = [values.at[0]] + [values.at[s, pl.ds(h * half, half)] for s in (1, 2) for h in (0, 1)]
-        arrivals = ((0,), (1, 2), (3, 4), (5, 6))
-    places += [values.at[3, pl.ds(h * half, half)] for h in (0, 1)]
+    places = [values.at[0]] + [values.at[s, pl.ds(h * half, half)] for s in (1, 2, 3) for h in (0, 1)]
+    arrivals = ((0,), (1, 2), (3, 4), (5, 6))
     fetch = [
         pltpu.make_async_copy(p.at[:, 0:depth] if k == 0 else p, place, sem_in.at[k])
         for k, (p, place) in enumerate(zip(parts, places))
@@ -353,8 +347,10 @@
     copies = []
     for t in range(TPN):
         part = mm(full[t], lv, 0, 0).astype(BF)
-        send[8 * t : 8 * t + 8, 0:64, :] = part.reshape(8, 64, CH)
-        rows = pl.ds(8 * t, 8), pl.ds(0, 64)
+        for h in range(2):
+            piece = part[:, h * LANE : (h + 1) * LANE].reshape(8, 64, LANE)
+            send[8 * t : 8 * t + 8, h * 64 : h * 64 + 64, :] = piece
+        rows = pl.ds(8 * t, 8), pl.ds(0, 128)
         copies.append(pltpu.make_async_copy(send.at[rows], out.at[rows], sem.at[t]))
         copies[t].start()
     arrivals[1].wait()
@@ -374,9 +370,10 @@
         gn = jnp.where(ok, gn * pltpu.roll(gn, ROWS - step, 0), gn)
         step *= 2
     term = a[0:1] * s[0:1]
-    pieces = jnp.concatenate(in_three(term) + [jnp.zeros((5, CH), F32)], axis=0).astype(BF)
-    send[:, 64:72, :] = jnp.broadcast_to(pieces[None], (PEERS, 8, CH))
-    rows = pl.ds(0, PEERS), pl.ds(64, 8)
+    lines = [p[:, h * LANE : (h + 1) * LANE] for h in range(2) for p in in_three(term)]
+    pieces = jnp.concatenate(lines + [jnp.zeros((2, LANE), F32)], axis=0).astype(BF)
+    send[:, 128:136, :] = jnp.broadcast_to(pieces[None], (PEERS, 8, LANE))
+    rows = pl.ds(0, PEERS), pl.ds(128, 8)
     copies.append(pltpu.make_async_copy(send.at[rows], out.at[rows], sem.at[TPN]))
     copies[TPN].start()
     tail_sum[...] = s
@@ -387,11 +384,14 @@
 
 
 def final_body(got, coef, tail_sum, gain, rr, ad, scaled, wr, wi, out_proj, grad_in):
-    acc = got[0, 0:64, :].astype(F32)
+    acc = got[0, 0:128, :].astype(F32)
     for s in range(1, PEERS):
-        acc = acc + got[s, 0:64, :].astype(F32)
-    out_proj[...] = acc
-    terms = jnp.sum(got[:, 64:72, :].astype(F32), axis=1)
+        acc = acc + got[s, 0:128, :].astype(F32)
+    out_proj[...] = jnp.concatenate([acc[0:64], acc[64:128]], axis=1)
+    pieces = got[:, 128:136, :].astype(F32)
+    line = iota((PEERS, 8, LANE), 1)
+    halves = [jnp.sum(jnp.where(line // 3 == h, pieces, 0.0), axis=1) for h in range(2)]
+    terms = jnp.concatenate(halves, axis=1)
     carry = jnp.sum(terms * coef[...], axis=0, keepdims=True)
     sg = tail_sum[...] + gain[...] * carry
     d_recall = (sg * rr[...]).astype(BF)
@@ -411,9 +411,9 @@
     return lax.ppermute(value, "tp", where)
 
 
-def ring_parts_a(own):
+def ring_parts(own, depth):
     half = PEERS // 2
-    low, high = own[:half], own[half:]
+    low, high = own[:half, :depth], own[half:, :depth]
     left1 = move(low, RING)
     right2 = move(high, BACK)
     left2 = move(high, RING)
@@ -421,16 +421,6 @@
     far1 = move(left1, RING)
     far2 = move(right2, BACK)
     return own, left1, left2, right1, right2, far1, far2
-
-
-def ring_parts_b(own):
-    half = PEERS // 2
-    rows = own[:, :80]
-    left = move(rows, RING)
-    right = move(rows, BACK)
-    far1 = move(left[:half], RING)
-    far2 = move(right[half:], BACK)
-    return own, left, right, far1, far2
 
 
 def shape(*dims, dtype=BF):
@@ -522,8 +512,8 @@
     )(decay, driven, idx, *tokens)
     own_a, send_b = lax.optimization_barrier((own_a, send_b))
     own_b = lax.all_to_all(send_b, "sp", 0, 0, tiled=True)
-    parts_a = ring_parts_a(own_a)
-    parts_b = ring_parts_b(own_b)
+    parts_a = ring_parts(own_a, 64)
+    parts_b = ring_parts(own_b, 80)
     s1, gelu_val, lru, of_log, coef = call(
         states_body,
         [tile, tile, shape(ROWS, CH), tile, shape(PEERS, CH, dtype=F32)],
@@ -561,7 +551,7 @@
     full = lax.all_to_all(spread, "tp", 0, 0, tiled=True)
     grad_gate_pre, tail_sum, send = call(
         reverse_body,
-        [tile, tile, shape(PEERS, 72, CH)],
+        [tile, tile, shape(PEERS, 136, LANE)],
         6,
         1 << 30,
         4 << 20,
@@ -569,7 +559,7 @@
         far=range(1, 6),
         far_out=(2,),
         scratch=[
-            pltpu.VMEM((PEERS, 72, CH), BF),
+            pltpu.VMEM((PEERS, 136, LANE), BF),
             pltpu.VMEM((ROWS, CH), BF),
             pltpu.VMEM((WIDTH, CH), BF),
             pltpu.VMEM((ROWS, CH), F32),

time: 184 us -> 191 us (1.038)
  waiting for transfers between devices: 59 us -> 63.6 us
  starting transfers between devices: 55.2 us -> 57.8 us
    ppermute x10 -> x12, waiting for transfers between devices: 23.5 us -> 28.9 us  [move(): return lax.ppermute(value, 'tp', where)]
    ppermute x10 -> x12, starting transfers between devices: 13.7 us -> 16.3 us  [move(): return lax.ppermute(value, 'tp', where)]
    unnamed x61 -> x65, local copies, waits for them, and re-layouts: 7.41 us -> 7.41 us
  transfers between devices with their start and end apart: 16 -> 18, of which waited for: 8 -> 9; matrix products, arithmetic and copies ran while one was open for 13% -> 12% of each run, Pallas kernels for 16% -> 16%
where the time goes in v3:
time: 191 us; the launch traced here: 190 us
  waiting for transfers between devices  63.6 us (33%)
  starting transfers between devices  57.8 us (30%)
  Pallas kernels  39 us (20%)
  matrix products  16.7 us (9%)
  local copies, waits for them, and re-layouts  9.63 us (5%)
    ppermute x12, waiting for transfers between devices, move(): return lax.ppermute(value, 'tp', where)  28.9 us
    pallas_call x2, Pallas kernels, expert_chain(): call(body, out, len(parts) + 4, flops, 12 << 20, smem=(0,), far=range(1,...  22.8 us
    all_to_all x1, waiting for transfers between devices, per_device(): got_b = lax.all_to_all(part_b, ('sp', 'tp'), 0, 0, tiled=True)  20.8 us
    dot_general x3, matrix products, mm(): lax.dot_general(a, b, (((ca,), (cb,)), ((), ())), preferred_element_type=...  16.3 us
    ppermute x12, starting transfers between devices, move(): return lax.ppermute(value, 'tp', where)  16.3 us
    all_to_all x1, starting transfers between devices, per_device(): got_a = lax.all_to_all(part_a, ('sp', 'tp'), 0, 0, tiled=True)  11.3 us
    all_to_all x1, starting transfers between devices, per_device(): own_a = lax.all_to_all(send_a, 'sp', 0, 0, tiled=True)  9.72 us
    all_to_all x1, starting transfers between devices, per_device(): got_b = lax.all_to_all(part_b, ('sp', 'tp'), 0, 0, tiled=True)  8.05 us
  transfers between devices with their start and end apart: 18, of which 9 were waited for; matrix products, arithmetic and copies ran while one was open for 12% of the time, Pallas kernels for 16%

profile of v3, /device:TPU:1, one launch (start us, length us, event | category | flops | bytes accessed | tf_op | source)
XLA Modules:
  0.0 189.7 jit_solution(8463550820587678251)
XLA Ops:
  0.6 2.4 %shard_map.181 = (bf16[32,64,128]{2,1,0:T(8,128)(2,1)}, s32[8,192]{1,0:T(8,128)}) custom-call(s32[2,192]{1,0:T(2,128)} %bitcast.65, f32[2,192]{1,0:T(2,128)} %bitcast.66, bf16[192,512]{1,0:T(8,128)(2,1)} %x.3, bf16[192,512]{1,0:T(8,128)(2,1)} %g.5), custom_call_target="tpu_custom_call" | custom-call | flops 1073741824 | bytes 3145728 | tf_op jit(solution)/shard_map/pallas_call | solution.py:478
  3.1 9.7 %all-to-all-start = ((bf16[32,64,128]{2,1,0:T(8,128)(2,1)}), bf16[32,64,128]{2,1,0:T(8,128)(2,1)S(1)}, u32[]{:S(2)}, u32[]{:S(2)}) async-start(bf16[32,64,128]{2,1,0:T(8,128)(2,1)} %get-tuple-element.36), calls=%async_computation | async-start | bytes 1048576 | tf_op jit(solution)/shard_map/all_to_all | solution.py:485
  16.0 3.5 %shard_map.182 = (f32[192,256]{1,0:T(8,128)}, f32[192,256]{1,0:T(8,128)}, f32[192,256]{1,0:T(8,128)}, bf16[32,96,128]{2,1,0:T(8,128)(2,1)}) custom-call(f32[192,256]{1,0:T(8,128)} %get-tuple-element.76.a_ref.a.refs_3_, f32[192,256]{1,0:T(8,128)} %get-tuple-element.67.b_ref, s32[8,192]{1,0:T(8,128)} %get-tuple-element.37.idx, f32[2,192]{1,0:T(2,128)} %bitcast.67, ...), custom_call_target="tpu_custom_call" | custom-call | flops 268435456 | bytes 2097152 | tf_op jit(solution)/shard_map/pallas_call | solution.py:510
  19.5 4.8 %all-to-all-done.refs_1_ = bf16[32,64,128]{2,1,0:T(8,128)(2,1)S(1)} async-done(((bf16[32,64,128]{2,1,0:T(8,128)(2,1)}), bf16[32,64,128]{2,1,0:T(8,128)(2,1)S(1)}, u32[]{:S(2)}, u32[]{:S(2)}) %all-to-all-start) | async-done | bytes 524320 | tf_op jit(solution)/shard_map/all_to_all | solution.py:485
  24.2 4.0 %all-to-all-start.1 = ((bf16[32,96,128]{2,1,0:T(8,128)(2,1)}), bf16[32,96,128]{2,1,0:T(8,128)(2,1)S(1)}, u32[]{:S(2)}, u32[]{:S(2)}) async-start(bf16[32,96,128]{2,1,0:T(8,128)(2,1)} %get-tuple-element.41), calls=%async_computation.1 | async-start | bytes 1572864 | tf_op jit(solution)/shard_map/all_to_all | solution.py:514
  29.5 1.5 collective-permute-start.3
  31.0 2.7 %collective-permute-start.2 = (bf16[16,64,128]{2,1,0:T(8,128)(2,1)S(1)}, bf16[16,64,128]{2,1,0:T(8,128)(2,1)}, u32[]{:S(2)}, u32[]{:S(2)}) collective-permute-start(bf16[16,64,128]{2,1,0:T(8,128)(2,1)S(1)} %get-tuple-element.73), channel_id=1, source_target_pairs={{0,3},{1,0},{2,1},{3,2},{4,7},{5,4},{6,5},{7,6},{8,11},{9,8},{10,9... | collective-permute-start | bytes 786440 | tf_op jit(solution)/shard_map/ppermute | solution.py:411
  33.7 3.5 %collective-permute-done.refs_2_ = bf16[16,64,128]{2,1,0:T(8,128)(2,1)} collective-permute-done((bf16[16,64,128]{2,1,0:T(8,128)(2,1)S(1)}, bf16[16,64,128]{2,1,0:T(8,128)(2,1)}, u32[]{:S(2)}, u32[]{:S(2)}) %collective-permute-start) | collective-permute-done | bytes 262176 | tf_op jit(solution)/shard_map/ppermute | solution.py:411
  37.2 2.7 %collective-permute-start.5 = (bf16[16,64,128]{2,1,0:T(8,128)(2,1)}, bf16[16,64,128]{2,1,0:T(8,128)(2,1)}, u32[]{:S(2)}, u32[]{:S(2)}) collective-permute-start(bf16[16,64,128]{2,1,0:T(8,128)(2,1)} %collective-permute-done.3.refs_5_), channel_id=1, source_target_pairs={{0,3},{1,0},{2,1},{3,2},{4,7},{5,4},{6,5},{7,6},{8,11},{9,8},{10,9... | collective-permute-start | bytes 786440 | tf_op jit(solution)/shard_map/ppermute | solution.py:411
  39.8 2.7 %all-to-all-done.1.refs_1_.got = bf16[32,96,128]{2,1,0:T(8,128)(2,1)S(1)} async-done(((bf16[32,96,128]{2,1,0:T(8,128)(2,1)}), bf16[32,96,128]{2,1,0:T(8,128)(2,1)S(1)}, u32[]{:S(2)}, u32[]{:S(2)}) %all-to-all-start.1) | async-done | bytes 786464 | tf_op jit(solution)/shard_map/all_to_all | solution.py:514
  43.9 1.5 collective-permute-start.9
  45.4 3.0 %collective-permute-done.4.refs_6_ = bf16[16,64,128]{2,1,0:T(8,128)(2,1)} collective-permute-done((bf16[16,64,128]{2,1,0:T(8,128)(2,1)}, bf16[16,64,128]{2,1,0:T(8,128)(2,1)}, u32[]{:S(2)}, u32[]{:S(2)}) %collective-permute-start.4) | collective-permute-done | bytes 262176 | tf_op jit(solution)/shard_map/ppermute | solution.py:411
  48.4 10.1 %shard_map.183 = (bf16[256,2048]{1,0:T(8,128)(2,1)}, bf16[256,2048]{1,0:T(8,128)(2,1)}, bf16[256,896]{1,0:T(8,128)(2,1)}, bf16[256,896]{1,0:T(8,128)(2,1)}, bf16...) custom-call(s32[1]{0:T(128)} %bitcast.refs_0_, bf16[32,64,128]{2,1,0:T(8,128)(2,1)} %copy-done.12, ...), custom_call_target="tpu_custom_call" | custom-call | flops 4697620480 | bytes 12582912 | tf_op jit(solution)/shard_map/pallas_call | solution.py:443
  58.5 11.3 %all-to-all-start.3 = ((bf16[128,32,128]{2,1,0:T(8,128)(2,1)}), bf16[128,32,128]{2,1,0:T(8,128)(2,1)S(1)}, u32[]{:S(2)}, u32[]{:S(2)}) async-start(bf16[128,32,128]{2,1,0:T(8,128)(2,1)} %bitcast.58), calls=%async_computation.3 | async-start | bytes 2097152 | tf_op jit(solution)/shard_map/all_to_all | solution.py:527
  69.8 1.4 collective-permute-start.7
  72.7 2.5 %collective-permute-start.11 = (bf16[16,80,128]{2,1,0:T(8,128)(2,1)}, bf16[16,80,128]{2,1,0:T(8,128)(2,1)S(1)}, u32[]{:S(2)}, u32[]{:S(2)}) collective-permute-start(bf16[16,80,128]{2,1,0:T(8,128)(2,1)} %collective-permute-done.9.refs_5_), channel_id=1, source_target_pairs={{0,3},{1,0},{2,1},{3,2},{4,7},{5,4},{6,5},{7,6},{8,11},{9,8},{10,9... | collective-permute-start | bytes 983048 | tf_op jit(solution)/shard_map/ppermute | solution.py:411
  75.2 15.4 %collective-permute-done.7.refs_3_ = bf16[16,80,128]{2,1,0:T(8,128)(2,1)S(1)} collective-permute-done((bf16[16,80,128]{2,1,0:T(8,128)(2,1)S(1)}, bf16[16,80,128]{2,1,0:T(8,128)(2,1)S(1)}, u32[]{:S(2)}, u32[]{:S(2)}) %collective-permute-start.7) | collective-permute-done | bytes 327712 | tf_op jit(solution)/shard_map/ppermute | solution.py:411
  90.6 7.0 %collective-permute-done.10.refs_6_ = bf16[16,80,128]{2,1,0:T(8,128)(2,1)S(1)} collective-permute-done((bf16[16,80,128]{2,1,0:T(8,128)(2,1)S(1)}, bf16[16,80,128]{2,1,0:T(8,128)(2,1)S(1)}, u32[]{:S(2)}, u32[]{:S(2)}) %collective-permute-start.10) | collective-permute-done | bytes 327712 | tf_op jit(solution)/shard_map/ppermute | solution.py:411
  99.1 12.7 %shard_map.184 = (bf16[320,2048]{1,0:T(8,128)(2,1)}, bf16[320,2048]{1,0:T(8,128)(2,1)}, bf16[320,896]{1,0:T(8,128)(2,1)}, bf16[320,896]{1,0:T(8,128)(2,1)}, bf16...) custom-call(s32[1]{0:T(128)} %bitcast.refs_0_, bf16[32,96,128]{2,1,0:T(8,128)(2,1)} %copy-done.11, ...), custom_call_target="tpu_custom_call" | custom-call | flops 5872025600 | bytes 12582912 | tf_op jit(solution)/shard_map/pallas_call | solution.py:443
  111.8 8.1 %all-to-all-start.2 = ((bf16[128,40,128]{2,1,0:T(8,128)(2,1)}), bf16[128,40,128]{2,1,0:T(8,128)(2,1)S(1)}, u32[]{:S(2)}, u32[]{:S(2)}) async-start(bf16[128,40,128]{2,1,0:T(8,128)(2,1)} %bitcast.57), calls=%async_computation.2 | async-start | bytes 2621440 | tf_op jit(solution)/shard_map/all_to_all | solution.py:529
  121.4 20.8 %all-to-all-done.2.got = bf16[128,40,128]{2,1,0:T(8,128)(2,1)S(1)} async-done(((bf16[128,40,128]{2,1,0:T(8,128)(2,1)}), bf16[128,40,128]{2,1,0:T(8,128)(2,1)S(1)}, u32[]{:S(2)}, u32[]{:S(2)}) %all-to-all-start.2) | async-done | bytes 1310752 | tf_op jit(solution)/shard_map/all_to_all | solution.py:529
  143.2 2.2 %shard_map.186 = bf16[4,192,512]{2,1,0:T(8,128)(2,1)} custom-call(bf16[128,40,128]{2,1,0:T(8,128)(2,1)S(1)} %all-to-all-done.2.got, s32[192,8]{1,0:T(8,128)S(1)} %bitcast.56, f32[192,512]{1,0:T(8,128)S(1)} %copy-done.10), custom_call_target="tpu_custom_call" | custom-call | flops 1073741824 | bytes 3145728 | tf_op jit(solution)/shard_map/pallas_call | solution.py:540
  145.4 3.7 %all-to-all-start.4 = ((bf16[4,192,512]{2,1,0:T(8,128)(2,1)}), bf16[4,192,512]{2,1,0:T(8,128)(2,1)S(1)}, u32[]{:S(2)}, u32[]{:S(2)}) async-start(bf16[4,192,512]{2,1,0:T(8,128)(2,1)} %shard_map.186), calls=%async_computation.4 | async-start | bytes 1572864 | tf_op jit(solution)/shard_map/all_to_all | solution.py:551
  149.2 2.5 %constant_dynamic-update-slice_fusion.1 = bf16[576,2048]{1,0:T(8,128)(2,1)} fusion(bf16[256,2048]{1,0:T(8,128)(2,1)} %get-tuple-element.40), kind=kLoop, calls=%fused_computation.42 | loop fusion | bytes 2097152
  151.6 2.7 %shard_map.187 = (f32[192,256]{1,0:T(8,128)}, f32[192,256]{1,0:T(8,128)}, bf16[192,256]{1,0:T(8,128)(2,1)}, f32[192,256]{1,0:T(8,128)}, f32[32,256]{1,0:T(8,128)}) custom-call(s32[1]{0:T(128)} %bitcast.14.sp_ref, bf16[32,96,128]{2,1,0:T(8,128)(2,1)} %copy-done.11, f32[192,256]{1,0:T(8,128)} %get-tuple-element.76.a_ref.a.refs_3_, ...), custom_call_target="tpu_custom_call" | custom-call | flops 268435456 | bytes 2097152 | tf_op jit(solution)/shard_map/pallas_call | solution.py:517
  154.4 4.5 %convert_bitcast_fusion = bf16[1,896,2048]{2,1,0:T(8,128)(2,1)} fusion(bf16[320,2048]{1,0:T(8,128)(2,1)S(1)} %copy-done.28, bf16[256,2048]{1,0:T(8,128)(2,1)S(1)} %copy-done.24, bf16[320,896]{1,0:T(8,128)(2,1)S(1)} %copy-done.31, bf16[256,896]{1,0:T(8,128)(2,1)S(1)} %copy-done.27), kind=kOutput, calls=%fused_computation | convolution fusion | flops 2122547200 | bytes 7061504 | tf_op jit(solution)/shard_map/dot_general | solution.py:23
  158.9 2.0 %all-to-all-done.4.full = bf16[4,192,512]{2,1,0:T(8,128)(2,1)S(1)} async-done(((bf16[4,192,512]{2,1,0:T(8,128)(2,1)}), bf16[4,192,512]{2,1,0:T(8,128)(2,1)S(1)}, u32[]{:S(2)}, u32[]{:S(2)}) %all-to-all-start.4) | async-done | bytes 786464 | tf_op jit(solution)/shard_map/all_to_all | solution.py:551
  162.2 3.9 %shard_map.188 = (f32[192,256]{1,0:T(8,128)}, f32[192,256]{1,0:T(8,128)S(1)}, bf16[32,136,128]{2,1,0:T(8,128)(2,1)}) custom-call(bf16[4,192,512]{2,1,0:T(8,128)(2,1)S(1)} %all-to-all-done.4.full, bf16[192,256]{1,0:T(8,128)(2,1)S(1)} %copy-done.8, bf16[2048,256]{1,0:T(8,128)(2,1)S(1)} %copy-done.4, f32[192,256]{1,0:T(8,128)S(1)} %copy-done.7, ...), custom_call_target="tpu_custom_call" | custom-call | flops 1073741824 | bytes 4194304 | tf_op jit(solution)/shard_map/pallas_call | solution.py:552
  166.1 4.8 %all-to-all-start.5 = ((bf16[32,136,128]{2,1,0:T(8,128)(2,1)}), bf16[32,136,128]{2,1,0:T(8,128)(2,1)S(1)}, u32[]{:S(2)}, u32[]{:S(2)}) async-start(bf16[32,136,128]{2,1,0:T(8,128)(2,1)} %get-tuple-element.58), calls=%async_computation.5 | async-start | bytes 2228224 | tf_op jit(solution)/shard_map/all_to_all | solution.py:572
  172.5 7.0 %convert_bitcast_fusion.1 = bf16[1,2048,896]{2,1,0:T(8,128)(2,1)} fusion(bf16[576,2048]{1,0:T(8,128)(2,1)} %constant_dynamic-update-slice_fusion, bf16[320,896]{1,0:T(8,128)(2,1)S(1)} %copy-done.30, bf16[256,896]{1,0:T(8,128)(2,1)S(1)} %copy-done.26), kind=kOutput, calls=%fused_computation.1 | convolution fusion | flops 2117828608 | bytes 7061504 | tf_op jit(solution)/shard_map/dot_general | solution.py:23
  179.5 4.8 %convert_bitcast_fusion.2 = bf16[1,2048,896]{2,1,0:T(8,128)(2,1)} fusion(bf16[576,2048]{1,0:T(8,128)(2,1)S(1)} %copy-done.14, bf16[320,896]{1,0:T(8,128)(2,1)S(1)} %copy-done.29, bf16[256,896]{1,0:T(8,128)(2,1)S(1)} %copy-done.25), kind=kOutput, calls=%fused_computation.2 | convolution fusion | flops 2117828608 | bytes 7061504 | tf_op jit(solution)/shard_map/dot_general | solution.py:23
  184.4 4.3 %all-to-all-done.5.got = bf16[32,136,128]{2,1,0:T(8,128)(2,1)S(1)} async-done(((bf16[32,136,128]{2,1,0:T(8,128)(2,1)}), bf16[32,136,128]{2,1,0:T(8,128)(2,1)S(1)}, u32[]{:S(2)}, u32[]{:S(2)}) %all-to-all-start.5) | async-done | bytes 1114144 | tf_op jit(solution)/shard_map/all_to_all | solution.py:572
  (91 shorter events, 15.1 us)
Async XLA Ops:
  0.6 13.1 %copy-start.15 = (bf16[192,256]{1,0:T(8,128)(2,1)S(1)}, bf16[192,256]{1,0:T(8,128)(2,1)}, u32[]{:S(2)}) copy-start(bf16[192,256]{1,0:T(8,128)(2,1)} %param.22) | copy-start | bytes 294916
  3.1 11.1 %copy-start.18 = (f32[256]{0:T(256)S(1)}, f32[256]{0:T(256)}, u32[]{:S(2)}) copy-start(f32[256]{0:T(256)} %param.26) | copy-start | bytes 3076
  3.1 11.1 %copy-start.16 = (f32[192,256]{1,0:T(8,128)S(1)}, f32[192,256]{1,0:T(8,128)}, u32[]{:S(2)}) copy-start(f32[192,256]{1,0:T(8,128)} %param.27) | copy-start | bytes 589828
  3.1 21.2 %all-to-all-start = ((bf16[32,64,128]{2,1,0:T(8,128)(2,1)}), bf16[32,64,128]{2,1,0:T(8,128)(2,1)S(1)}, u32[]{:S(2)}, u32[]{:S(2)}) async-start(bf16[32,64,128]{2,1,0:T(8,128)(2,1)} %get-tuple-element.36), calls=%async_computation | async-start | bytes 1048576 | tf_op jit(solution)/shard_map/all_to_all | solution.py:485
  24.2 24.2 %copy-start.12 = (bf16[32,64,128]{2,1,0:T(8,128)(2,1)}, bf16[32,64,128]{2,1,0:T(8,128)(2,1)S(1)}, u32[]{:S(2)}) copy-start(bf16[32,64,128]{2,1,0:T(8,128)(2,1)S(1)} %all-to-all-done.refs_1_) | copy-start | bytes 1572868
  24.2 18.3 %all-to-all-start.1 = ((bf16[32,96,128]{2,1,0:T(8,128)(2,1)}), bf16[32,96,128]{2,1,0:T(8,128)(2,1)S(1)}, u32[]{:S(2)}, u32[]{:S(2)}) async-start(bf16[32,96,128]{2,1,0:T(8,128)(2,1)} %get-tuple-element.41), calls=%async_computation.1 | async-start | bytes 1572864 | tf_op jit(solution)/shard_map/all_to_all | solution.py:514
  28.3 8.9 %collective-permute-start = (bf16[16,64,128]{2,1,0:T(8,128)(2,1)S(1)}, bf16[16,64,128]{2,1,0:T(8,128)(2,1)}, u32[]{:S(2)}, u32[]{:S(2)}) collective-permute-start(bf16[16,64,128]{2,1,0:T(8,128)(2,1)S(1)} %get-tuple-element.73), channel_id=1, source_target_pairs={{0,1},{1,2},{2,3},{3,0},{4,5},{5,6},{6,7},{7,4},{8,9},{9,10},{10,1... | collective-permute-start | bytes 786440 | tf_op jit(solution)/shard_map/ppermute | solution.py:411
  29.5 7.6 %collective-permute-start.3 = (bf16[16,64,128]{2,1,0:T(8,128)(2,1)S(1)}, bf16[16,64,128]{2,1,0:T(8,128)(2,1)}, u32[]{:S(2)}, u32[]{:S(2)}) collective-permute-start(bf16[16,64,128]{2,1,0:T(8,128)(2,1)S(1)} %get-tuple-element.72), channel_id=1, source_target_pairs={{0,3},{1,0},{2,1},{3,2},{4,7},{5,4},{6,5},{7,6},{8,11},{9,8},{10,9... | collective-permute-start | bytes 786440 | tf_op jit(solution)/shard_map/ppermute | solution.py:411
  31.0 12.9 %collective-permute-start.1 = (bf16[16,64,128]{2,1,0:T(8,128)(2,1)S(1)}, bf16[16,64,128]{2,1,0:T(8,128)(2,1)}, u32[]{:S(2)}, u32[]{:S(2)}) collective-permute-start(bf16[16,64,128]{2,1,0:T(8,128)(2,1)S(1)} %get-tuple-element.72), channel_id=1, source_target_pairs={{0,1},{1,2},{2,3},{3,0},{4,5},{5,6},{6,7},{7,4},{8,9},{9,10},{10,1... | collective-permute-start | bytes 786440 | tf_op jit(solution)/shard_map/ppermute | solution.py:411
  31.0 14.4 %collective-permute-start.2 = (bf16[16,64,128]{2,1,0:T(8,128)(2,1)S(1)}, bf16[16,64,128]{2,1,0:T(8,128)(2,1)}, u32[]{:S(2)}, u32[]{:S(2)}) collective-permute-start(bf16[16,64,128]{2,1,0:T(8,128)(2,1)S(1)} %get-tuple-element.73), channel_id=1, source_target_pairs={{0,3},{1,0},{2,1},{3,2},{4,7},{5,4},{6,5},{7,6},{8,11},{9,8},{10,9... | collective-permute-start | bytes 786440 | tf_op jit(solution)/shard_map/ppermute | solution.py:411
  37.2 11.2 %collective-permute-start.4 = (bf16[16,64,128]{2,1,0:T(8,128)(2,1)}, bf16[16,64,128]{2,1,0:T(8,128)(2,1)}, u32[]{:S(2)}, u32[]{:S(2)}) collective-permute-start(bf16[16,64,128]{2,1,0:T(8,128)(2,1)} %collective-permute-done.refs_2_), channel_id=1, source_target_pairs={{0,1},{1,2},{2,3},{3,0},{4,5},{5,6},{6,7},{7,4},{8,9},{9,10},{10,1... | collective-permute-start | bytes 786440 | tf_op jit(solution)/shard_map/ppermute | solution.py:411
  37.2 11.2 %collective-permute-start.5 = (bf16[16,64,128]{2,1,0:T(8,128)(2,1)}, bf16[16,64,128]{2,1,0:T(8,128)(2,1)}, u32[]{:S(2)}, u32[]{:S(2)}) collective-permute-start(bf16[16,64,128]{2,1,0:T(8,128)(2,1)} %collective-permute-done.3.refs_5_), channel_id=1, source_target_pairs={{0,3},{1,0},{2,1},{3,2},{4,7},{5,4},{6,5},{7,6},{8,11},{9,8},{10,9... | collective-permute-start | bytes 786440 | tf_op jit(solution)/shard_map/ppermute | solution.py:411
  42.6 15.9 %copy-start.11 = (bf16[32,96,128]{2,1,0:T(8,128)(2,1)}, bf16[32,96,128]{2,1,0:T(8,128)(2,1)S(1)}, u32[]{:S(2)}) copy-start(bf16[32,96,128]{2,1,0:T(8,128)(2,1)S(1)} %all-to-all-done.1.refs_1_.got) | copy-start | bytes 2359300
  42.6 29.9 %collective-permute-start.6 = (bf16[16,80,128]{2,1,0:T(8,128)(2,1)S(1)}, bf16[16,80,128]{2,1,0:T(8,128)(2,1)S(1)}, u32[]{:S(2)}, u32[]{:S(2)}) collective-permute-start(bf16[16,80,128]{2,1,0:T(8,128)(2,1)S(1)} %get-tuple-element.71), channel_id=1, source_target_pairs={{0,1},{1,2},{2,3},{3,0},{4,5},{5,6},{6,7},{7,4},{8,9},{9,10},{10,1... | collective-permute-start | bytes 983048 | tf_op jit(solution)/shard_map/ppermute | solution.py:411
  43.9 28.8 %collective-permute-start.9 = (bf16[16,80,128]{2,1,0:T(8,128)(2,1)S(1)}, bf16[16,80,128]{2,1,0:T(8,128)(2,1)}, u32[]{:S(2)}, u32[]{:S(2)}) collective-permute-start(bf16[16,80,128]{2,1,0:T(8,128)(2,1)S(1)} %get-tuple-element.70), channel_id=1, source_target_pairs={{0,3},{1,0},{2,1},{3,2},{4,7},{5,4},{6,5},{7,6},{8,11},{9,8},{10,9... | collective-permute-start | bytes 983048 | tf_op jit(solution)/shard_map/ppermute | solution.py:411
  58.5 53.3 %all-to-all-start.3 = ((bf16[128,32,128]{2,1,0:T(8,128)(2,1)}), bf16[128,32,128]{2,1,0:T(8,128)(2,1)S(1)}, u32[]{:S(2)}, u32[]{:S(2)}) async-start(bf16[128,32,128]{2,1,0:T(8,128)(2,1)} %bitcast.58), calls=%async_computation.3 | async-start | bytes 2097152 | tf_op jit(solution)/shard_map/all_to_all | solution.py:527
  69.8 20.8 %collective-permute-start.7 = (bf16[16,80,128]{2,1,0:T(8,128)(2,1)S(1)}, bf16[16,80,128]{2,1,0:T(8,128)(2,1)S(1)}, u32[]{:S(2)}, u32[]{:S(2)}) collective-permute-start(bf16[16,80,128]{2,1,0:T(8,128)(2,1)S(1)} %get-tuple-element.70), channel_id=1, source_target_pairs={{0,1},{1,2},{2,3},{3,0},{4,5},{5,6},{6,7},{7,4},{8,9},{9,10},{10,1... | collective-permute-start | bytes 983048 | tf_op jit(solution)/shard_map/ppermute | solution.py:411
  71.2 19.4 %collective-permute-start.8 = (bf16[16,80,128]{2,1,0:T(8,128)(2,1)S(1)}, bf16[16,80,128]{2,1,0:T(8,128)(2,1)S(1)}, u32[]{:S(2)}, u32[]{:S(2)}) collective-permute-start(bf16[16,80,128]{2,1,0:T(8,128)(2,1)S(1)} %get-tuple-element.71), channel_id=1, source_target_pairs={{0,3},{1,0},{2,1},{3,2},{4,7},{5,4},{6,5},{7,6},{8,11},{9,8},{10,9... | collective-permute-start | bytes 983048 | tf_op jit(solution)/shard_map/ppermute | solution.py:411
  72.6 25.1 %copy-start.19 = (bf16[16,80,128]{2,1,0:T(8,128)(2,1)}, bf16[16,80,128]{2,1,0:T(8,128)(2,1)S(1)}, u32[]{:S(2)}) copy-start(bf16[16,80,128]{2,1,0:T(8,128)(2,1)S(1)} %collective-permute-done.6.refs_2_) | copy-start | bytes 983044
  72.6 25.1 %collective-permute-start.10 = (bf16[16,80,128]{2,1,0:T(8,128)(2,1)S(1)}, bf16[16,80,128]{2,1,0:T(8,128)(2,1)S(1)}, u32[]{:S(2)}, u32[]{:S(2)}) collective-permute-start(bf16[16,80,128]{2,1,0:T(8,128)(2,1)S(1)} %collective-permute-done.6.refs_2_), channel_id=1, source_target_pairs={{0,1},{1,2},{2,3},{3,0},{4,5},{5,6},{6,7},{7,4},{8,9},{9,10},{10,1... | collective-permute-start | bytes 983048 | tf_op jit(solution)/shard_map/ppermute | solution.py:411
  72.7 25.0 %collective-permute-start.11 = (bf16[16,80,128]{2,1,0:T(8,128)(2,1)}, bf16[16,80,128]{2,1,0:T(8,128)(2,1)S(1)}, u32[]{:S(2)}, u32[]{:S(2)}) collective-permute-start(bf16[16,80,128]{2,1,0:T(8,128)(2,1)} %collective-permute-done.9.refs_5_), channel_id=1, source_target_pairs={{0,3},{1,0},{2,1},{3,2},{4,7},{5,4},{6,5},{7,6},{8,11},{9,8},{10,9... | collective-permute-start | bytes 983048 | tf_op jit(solution)/shard_map/ppermute | solution.py:411
  90.6 7.0 %copy-start.20 = (bf16[16,80,128]{2,1,0:T(8,128)(2,1)}, bf16[16,80,128]{2,1,0:T(8,128)(2,1)S(1)}, u32[]{:S(2)}) copy-start(bf16[16,80,128]{2,1,0:T(8,128)(2,1)S(1)} %collective-permute-done.7.refs_3_) | copy-start | bytes 983044
  90.6 7.0 %copy-start.21 = (bf16[16,80,128]{2,1,0:T(8,128)(2,1)}, bf16[16,80,128]{2,1,0:T(8,128)(2,1)S(1)}, u32[]{:S(2)}) copy-start(bf16[16,80,128]{2,1,0:T(8,128)(2,1)S(1)} %collective-permute-done.8.refs_4_) | copy-start | bytes 983044
  111.8 8.1 %copy-start.17 = (s32[8,192]{1,0:T(8,128)S(1)}, s32[8,192]{1,0:T(8,128)}, u32[]{:S(2)}) copy-start(s32[8,192]{1,0:T(8,128)} %get-tuple-element.37.idx) | copy-start | bytes 18436
  111.8 8.2 %copy-start.5 = (bf16[192,512]{1,0:T(8,128)(2,1)S(1)}, bf16[192,512]{1,0:T(8,128)(2,1)}, u32[]{:S(2)}) copy-start(bf16[192,512]{1,0:T(8,128)(2,1)} %g.5) | copy-start | bytes 589828
  111.8 30.4 %all-to-all-start.2 = ((bf16[128,40,128]{2,1,0:T(8,128)(2,1)}), bf16[128,40,128]{2,1,0:T(8,128)(2,1)S(1)}, u32[]{:S(2)}, u32[]{:S(2)}) async-start(bf16[128,40,128]{2,1,0:T(8,128)(2,1)} %bitcast.57), calls=%async_computation.2 | async-start | bytes 2621440 | tf_op jit(solution)/shard_map/all_to_all | solution.py:529
  145.4 15.5 %all-to-all-start.4 = ((bf16[4,192,512]{2,1,0:T(8,128)(2,1)}), bf16[4,192,512]{2,1,0:T(8,128)(2,1)S(1)}, u32[]{:S(2)}, u32[]{:S(2)}) async-start(bf16[4,192,512]{2,1,0:T(8,128)(2,1)} %shard_map.186), calls=%async_computation.4 | async-start | bytes 1572864 | tf_op jit(solution)/shard_map/all_to_all | solution.py:551
  162.2 8.7 %copy-start.13 = (bf16[320,2048]{1,0:T(8,128)(2,1)S(1)}, bf16[320,2048]{1,0:T(8,128)(2,1)}, u32[]{:S(2)}) copy-start(bf16[320,2048]{1,0:T(8,128)(2,1)} %get-tuple-element.42) | copy-start | bytes 3932164
  166.1 22.7 %all-to-all-start.5 = ((bf16[32,136,128]{2,1,0:T(8,128)(2,1)}), bf16[32,136,128]{2,1,0:T(8,128)(2,1)S(1)}, u32[]{:S(2)}, u32[]{:S(2)}) async-start(bf16[32,136,128]{2,1,0:T(8,128)(2,1)} %get-tuple-element.58), calls=%async_computation.5 | async-start | bytes 2228224 | tf_op jit(solution)/shard_map/all_to_all | solution.py:572
  179.5 9.2 %copy-start.1 = (f32[192,256]{1,0:T(8,128)S(1)}, f32[192,256]{1,0:T(8,128)}, u32[]{:S(2)}) copy-start(f32[192,256]{1,0:T(8,128)} %get-tuple-element.61.gain) | copy-start | bytes 589828
  179.5 9.2 %copy-start.2 = (f32[192,256]{1,0:T(8,128)S(1)}, f32[192,256]{1,0:T(8,128)}, u32[]{:S(2)}) copy-start(f32[192,256]{1,0:T(8,128)} %get-tuple-element.62.rr) | copy-start | bytes 589828
  179.5 9.2 %copy-start.3 = (f32[32,256]{1,0:T(8,128)S(1)}, f32[32,256]{1,0:T(8,128)}, u32[]{:S(2)}) copy-start(f32[32,256]{1,0:T(8,128)} %get-tuple-element.59.coef) | copy-start | bytes 98308
  (18 other events, 75.2 us)

commit v4 on v3

--- a/solution.py
+++ b/solution.py
@@ -137,7 +137,7 @@
             pltpu.make_async_copy(w.at[pl.ds(h * n, n)], v.at[pl.ds(h * n, n)], sem_w.at[2 * k + h])
             for h in range(2)
         ]
-    for copy in fetch + loads[:2]:
+    for copy in fetch:
         copy.start()
     saves = [
         pltpu.make_async_copy(v, o, sem_out.at[k])
@@ -159,6 +159,9 @@
     for source, (off, arriving) in enumerate(zip((0, 3, 1, 2), arrivals)):
         for k in arriving:
             fetch[k].wait()
+        if source == 1:
+            for load in loads[:2]:
+                load.start()
         if source == 3:
             for load in loads[2:]:
                 load.start()

time: 191 us -> 191 us (level)
  no operation moved by 1% of the time
where the time goes in v4:
time: 191 us; the launch traced here: 190 us
  waiting for transfers between devices  63.6 us (33%)
  starting transfers between devices  57.8 us (30%)
  Pallas kernels  39.5 us (21%)
  matrix products  16.7 us (9%)
  local copies, waits for them, and re-layouts  9.63 us (5%)
    ppermute x12, waiting for transfers between devices, move(): return lax.ppermute(value, 'tp', where)  28.9 us
    pallas_call x2, Pallas kernels, expert_chain(): call(body, out, len(parts) + 4, flops, 12 << 20, smem=(0,), far=range(1,...  23.2 us
    all_to_all x1, waiting for transfers between devices, per_device(): got_b = lax.all_to_all(part_b, ('sp', 'tp'), 0, 0, tiled=True)  20.8 us
    dot_general x3, matrix products, mm(): lax.dot_general(a, b, (((ca,), (cb,)), ((), ())), preferred_element_type=...  16.3 us
    ppermute x12, starting transfers between devices, move(): return lax.ppermute(value, 'tp', where)  16.3 us
    all_to_all x1, starting transfers between devices, per_device(): got_a = lax.all_to_all(part_a, ('sp', 'tp'), 0, 0, tiled=True)  11.3 us
    all_to_all x1, starting transfers between devices, per_device(): own_a = lax.all_to_all(send_a, 'sp', 0, 0, tiled=True)  9.72 us
    all_to_all x1, starting transfers between devices, per_device(): got_b = lax.all_to_all(part_b, ('sp', 'tp'), 0, 0, tiled=True)  8.07 us
  transfers between devices with their start and end apart: 18, of which 9 were waited for; matrix products, arithmetic and copies ran while one was open for 12% of the time, Pallas kernels for 16%

profile of v4, /device:TPU:1, one launch (start us, length us, event | category | flops | bytes accessed | tf_op | source)
XLA Modules:
  0.0 190.2 jit_solution(2942643975086530963)
XLA Ops:
  0.6 2.4 %shard_map.181 = (bf16[32,64,128]{2,1,0:T(8,128)(2,1)}, s32[8,192]{1,0:T(8,128)}) custom-call(s32[2,192]{1,0:T(2,128)} %bitcast.65, f32[2,192]{1,0:T(2,128)} %bitcast.66, bf16[192,512]{1,0:T(8,128)(2,1)} %x.3, bf16[192,512]{1,0:T(8,128)(2,1)} %g.5), custom_call_target="tpu_custom_call" | custom-call | flops 1073741824 | bytes 3145728 | tf_op jit(solution)/shard_map/pallas_call | solution.py:481
  3.1 9.7 %all-to-all-start = ((bf16[32,64,128]{2,1,0:T(8,128)(2,1)}), bf16[32,64,128]{2,1,0:T(8,128)(2,1)S(1)}, u32[]{:S(2)}, u32[]{:S(2)}) async-start(bf16[32,64,128]{2,1,0:T(8,128)(2,1)} %get-tuple-element.36), calls=%async_computation | async-start | bytes 1048576 | tf_op jit(solution)/shard_map/all_to_all | solution.py:488
  16.0 3.5 %shard_map.182 = (f32[192,256]{1,0:T(8,128)}, f32[192,256]{1,0:T(8,128)}, f32[192,256]{1,0:T(8,128)}, bf16[32,96,128]{2,1,0:T(8,128)(2,1)}) custom-call(f32[192,256]{1,0:T(8,128)} %get-tuple-element.76.a_ref.a.refs_3_, f32[192,256]{1,0:T(8,128)} %get-tuple-element.67.b_ref, s32[8,192]{1,0:T(8,128)} %get-tuple-element.37.idx, f32[2,192]{1,0:T(2,128)} %bitcast.67, ...), custom_call_target="tpu_custom_call" | custom-call | flops 268435456 | bytes 2097152 | tf_op jit(solution)/shard_map/pallas_call | solution.py:513
  19.5 4.8 %all-to-all-done.refs_1_ = bf16[32,64,128]{2,1,0:T(8,128)(2,1)S(1)} async-done(((bf16[32,64,128]{2,1,0:T(8,128)(2,1)}), bf16[32,64,128]{2,1,0:T(8,128)(2,1)S(1)}, u32[]{:S(2)}, u32[]{:S(2)}) %all-to-all-start) | async-done | bytes 524320 | tf_op jit(solution)/shard_map/all_to_all | solution.py:488
  24.2 4.0 %all-to-all-start.1 = ((bf16[32,96,128]{2,1,0:T(8,128)(2,1)}), bf16[32,96,128]{2,1,0:T(8,128)(2,1)S(1)}, u32[]{:S(2)}, u32[]{:S(2)}) async-start(bf16[32,96,128]{2,1,0:T(8,128)(2,1)} %get-tuple-element.41), calls=%async_computation.1 | async-start | bytes 1572864 | tf_op jit(solution)/shard_map/all_to_all | solution.py:517
  29.5 1.5 collective-permute-start.3
  31.0 2.7 %collective-permute-start.2 = (bf16[16,64,128]{2,1,0:T(8,128)(2,1)S(1)}, bf16[16,64,128]{2,1,0:T(8,128)(2,1)}, u32[]{:S(2)}, u32[]{:S(2)}) collective-permute-start(bf16[16,64,128]{2,1,0:T(8,128)(2,1)S(1)} %get-tuple-element.73), channel_id=1, source_target_pairs={{0,3},{1,0},{2,1},{3,2},{4,7},{5,4},{6,5},{7,6},{8,11},{9,8},{10,9... | collective-permute-start | bytes 786440 | tf_op jit(solution)/shard_map/ppermute | solution.py:414
  33.7 3.5 %collective-permute-done.refs_2_ = bf16[16,64,128]{2,1,0:T(8,128)(2,1)} collective-permute-done((bf16[16,64,128]{2,1,0:T(8,128)(2,1)S(1)}, bf16[16,64,128]{2,1,0:T(8,128)(2,1)}, u32[]{:S(2)}, u32[]{:S(2)}) %collective-permute-start) | collective-permute-done | bytes 262176 | tf_op jit(solution)/shard_map/ppermute | solution.py:414
  37.2 2.7 %collective-permute-start.5 = (bf16[16,64,128]{2,1,0:T(8,128)(2,1)}, bf16[16,64,128]{2,1,0:T(8,128)(2,1)}, u32[]{:S(2)}, u32[]{:S(2)}) collective-permute-start(bf16[16,64,128]{2,1,0:T(8,128)(2,1)} %collective-permute-done.3.refs_5_), channel_id=1, source_target_pairs={{0,3},{1,0},{2,1},{3,2},{4,7},{5,4},{6,5},{7,6},{8,11},{9,8},{10,9... | collective-permute-start | bytes 786440 | tf_op jit(solution)/shard_map/ppermute | solution.py:414
  39.8 2.7 %all-to-all-done.1.refs_1_.got = bf16[32,96,128]{2,1,0:T(8,128)(2,1)S(1)} async-done(((bf16[32,96,128]{2,1,0:T(8,128)(2,1)}), bf16[32,96,128]{2,1,0:T(8,128)(2,1)S(1)}, u32[]{:S(2)}, u32[]{:S(2)}) %all-to-all-start.1) | async-done | bytes 786464 | tf_op jit(solution)/shard_map/all_to_all | solution.py:517
  43.9 1.5 collective-permute-start.9
  45.4 3.0 %collective-permute-done.4.refs_6_ = bf16[16,64,128]{2,1,0:T(8,128)(2,1)} collective-permute-done((bf16[16,64,128]{2,1,0:T(8,128)(2,1)}, bf16[16,64,128]{2,1,0:T(8,128)(2,1)}, u32[]{:S(2)}, u32[]{:S(2)}) %collective-permute-start.4) | collective-permute-done | bytes 262176 | tf_op jit(solution)/shard_map/ppermute | solution.py:414
  48.4 10.5 %shard_map.183 = (bf16[256,2048]{1,0:T(8,128)(2,1)}, bf16[256,2048]{1,0:T(8,128)(2,1)}, bf16[256,896]{1,0:T(8,128)(2,1)}, bf16[256,896]{1,0:T(8,128)(2,1)}, bf16...) custom-call(s32[1]{0:T(128)} %bitcast.refs_0_, bf16[32,64,128]{2,1,0:T(8,128)(2,1)} %copy-done.12, ...), custom_call_target="tpu_custom_call" | custom-call | flops 4697620480 | bytes 12582912 | tf_op jit(solution)/shard_map/pallas_call | solution.py:446
  58.9 11.3 %all-to-all-start.3 = ((bf16[128,32,128]{2,1,0:T(8,128)(2,1)}), bf16[128,32,128]{2,1,0:T(8,128)(2,1)S(1)}, u32[]{:S(2)}, u32[]{:S(2)}) async-start(bf16[128,32,128]{2,1,0:T(8,128)(2,1)} %bitcast.58), calls=%async_computation.3 | async-start | bytes 2097152 | tf_op jit(solution)/shard_map/all_to_all | solution.py:530
  70.1 1.4 collective-permute-start.7
  73.0 2.5 %collective-permute-start.11 = (bf16[16,80,128]{2,1,0:T(8,128)(2,1)}, bf16[16,80,128]{2,1,0:T(8,128)(2,1)S(1)}, u32[]{:S(2)}, u32[]{:S(2)}) collective-permute-start(bf16[16,80,128]{2,1,0:T(8,128)(2,1)} %collective-permute-done.9.refs_5_), channel_id=1, source_target_pairs={{0,3},{1,0},{2,1},{3,2},{4,7},{5,4},{6,5},{7,6},{8,11},{9,8},{10,9... | collective-permute-start | bytes 983048 | tf_op jit(solution)/shard_map/ppermute | solution.py:414
  75.6 15.4 %collective-permute-done.7.refs_3_ = bf16[16,80,128]{2,1,0:T(8,128)(2,1)S(1)} collective-permute-done((bf16[16,80,128]{2,1,0:T(8,128)(2,1)S(1)}, bf16[16,80,128]{2,1,0:T(8,128)(2,1)S(1)}, u32[]{:S(2)}, u32[]{:S(2)}) %collective-permute-start.7) | collective-permute-done | bytes 327712 | tf_op jit(solution)/shard_map/ppermute | solution.py:414
  91.0 7.0 %collective-permute-done.10.refs_6_ = bf16[16,80,128]{2,1,0:T(8,128)(2,1)S(1)} collective-permute-done((bf16[16,80,128]{2,1,0:T(8,128)(2,1)S(1)}, bf16[16,80,128]{2,1,0:T(8,128)(2,1)S(1)}, u32[]{:S(2)}, u32[]{:S(2)}) %collective-permute-start.10) | collective-permute-done | bytes 327712 | tf_op jit(solution)/shard_map/ppermute | solution.py:414
  99.5 12.7 %shard_map.184 = (bf16[320,2048]{1,0:T(8,128)(2,1)}, bf16[320,2048]{1,0:T(8,128)(2,1)}, bf16[320,896]{1,0:T(8,128)(2,1)}, bf16[320,896]{1,0:T(8,128)(2,1)}, bf16...) custom-call(s32[1]{0:T(128)} %bitcast.refs_0_, bf16[32,96,128]{2,1,0:T(8,128)(2,1)} %copy-done.11, ...), custom_call_target="tpu_custom_call" | custom-call | flops 5872025600 | bytes 12582912 | tf_op jit(solution)/shard_map/pallas_call | solution.py:446
  112.3 8.1 %all-to-all-start.2 = ((bf16[128,40,128]{2,1,0:T(8,128)(2,1)}), bf16[128,40,128]{2,1,0:T(8,128)(2,1)S(1)}, u32[]{:S(2)}, u32[]{:S(2)}) async-start(bf16[128,40,128]{2,1,0:T(8,128)(2,1)} %bitcast.57), calls=%async_computation.2 | async-start | bytes 2621440 | tf_op jit(solution)/shard_map/all_to_all | solution.py:532
  121.9 20.8 %all-to-all-done.2.got = bf16[128,40,128]{2,1,0:T(8,128)(2,1)S(1)} async-done(((bf16[128,40,128]{2,1,0:T(8,128)(2,1)}), bf16[128,40,128]{2,1,0:T(8,128)(2,1)S(1)}, u32[]{:S(2)}, u32[]{:S(2)}) %all-to-all-start.2) | async-done | bytes 1310752 | tf_op jit(solution)/shard_map/all_to_all | solution.py:532
  143.7 2.2 %shard_map.186 = bf16[4,192,512]{2,1,0:T(8,128)(2,1)} custom-call(bf16[128,40,128]{2,1,0:T(8,128)(2,1)S(1)} %all-to-all-done.2.got, s32[192,8]{1,0:T(8,128)S(1)} %bitcast.56, f32[192,512]{1,0:T(8,128)S(1)} %copy-done.10), custom_call_target="tpu_custom_call" | custom-call | flops 1073741824 | bytes 3145728 | tf_op jit(solution)/shard_map/pallas_call | solution.py:543
  145.9 3.7 %all-to-all-start.4 = ((bf16[4,192,512]{2,1,0:T(8,128)(2,1)}), bf16[4,192,512]{2,1,0:T(8,128)(2,1)S(1)}, u32[]{:S(2)}, u32[]{:S(2)}) async-start(bf16[4,192,512]{2,1,0:T(8,128)(2,1)} %shard_map.186), calls=%async_computation.4 | async-start | bytes 1572864 | tf_op jit(solution)/shard_map/all_to_all | solution.py:554
  149.6 2.5 %constant_dynamic-update-slice_fusion.1 = bf16[576,2048]{1,0:T(8,128)(2,1)} fusion(bf16[256,2048]{1,0:T(8,128)(2,1)} %get-tuple-element.40), kind=kLoop, calls=%fused_computation.42 | loop fusion | bytes 2097152
  152.1 2.7 %shard_map.187 = (f32[192,256]{1,0:T(8,128)}, f32[192,256]{1,0:T(8,128)}, bf16[192,256]{1,0:T(8,128)(2,1)}, f32[192,256]{1,0:T(8,128)}, f32[32,256]{1,0:T(8,128)}) custom-call(s32[1]{0:T(128)} %bitcast.14.sp_ref, bf16[32,96,128]{2,1,0:T(8,128)(2,1)} %copy-done.11, f32[192,256]{1,0:T(8,128)} %get-tuple-element.76.a_ref.a.refs_3_, ...), custom_call_target="tpu_custom_call" | custom-call | flops 268435456 | bytes 2097152 | tf_op jit(solution)/shard_map/pallas_call | solution.py:520
  154.8 4.5 %convert_bitcast_fusion = bf16[1,896,2048]{2,1,0:T(8,128)(2,1)} fusion(bf16[320,2048]{1,0:T(8,128)(2,1)S(1)} %copy-done.28, bf16[256,2048]{1,0:T(8,128)(2,1)S(1)} %copy-done.24, bf16[320,896]{1,0:T(8,128)(2,1)S(1)} %copy-done.31, bf16[256,896]{1,0:T(8,128)(2,1)S(1)} %copy-done.27), kind=kOutput, calls=%fused_computation | convolution fusion | flops 2122547200 | bytes 7061504 | tf_op jit(solution)/shard_map/dot_general | solution.py:23
  159.3 2.0 %all-to-all-done.4.full = bf16[4,192,512]{2,1,0:T(8,128)(2,1)S(1)} async-done(((bf16[4,192,512]{2,1,0:T(8,128)(2,1)}), bf16[4,192,512]{2,1,0:T(8,128)(2,1)S(1)}, u32[]{:S(2)}, u32[]{:S(2)}) %all-to-all-start.4) | async-done | bytes 786464 | tf_op jit(solution)/shard_map/all_to_all | solution.py:554
  162.6 3.9 %shard_map.188 = (f32[192,256]{1,0:T(8,128)}, f32[192,256]{1,0:T(8,128)S(1)}, bf16[32,136,128]{2,1,0:T(8,128)(2,1)}) custom-call(bf16[4,192,512]{2,1,0:T(8,128)(2,1)S(1)} %all-to-all-done.4.full, bf16[192,256]{1,0:T(8,128)(2,1)S(1)} %copy-done.8, bf16[2048,256]{1,0:T(8,128)(2,1)S(1)} %copy-done.4, f32[192,256]{1,0:T(8,128)S(1)} %copy-done.7, ...), custom_call_target="tpu_custom_call" | custom-call | flops 1073741824 | bytes 4194304 | tf_op jit(solution)/shard_map/pallas_call | solution.py:555
  166.5 4.8 %all-to-all-start.5 = ((bf16[32,136,128]{2,1,0:T(8,128)(2,1)}), bf16[32,136,128]{2,1,0:T(8,128)(2,1)S(1)}, u32[]{:S(2)}, u32[]{:S(2)}) async-start(bf16[32,136,128]{2,1,0:T(8,128)(2,1)} %get-tuple-element.58), calls=%async_computation.5 | async-start | bytes 2228224 | tf_op jit(solution)/shard_map/all_to_all | solution.py:575
  172.9 7.0 %convert_bitcast_fusion.1 = bf16[1,2048,896]{2,1,0:T(8,128)(2,1)} fusion(bf16[576,2048]{1,0:T(8,128)(2,1)} %constant_dynamic-update-slice_fusion, bf16[320,896]{1,0:T(8,128)(2,1)S(1)} %copy-done.30, bf16[256,896]{1,0:T(8,128)(2,1)S(1)} %copy-done.26), kind=kOutput, calls=%fused_computation.1 | convolution fusion | flops 2117828608 | bytes 7061504 | tf_op jit(solution)/shard_map/dot_general | solution.py:23
  180.0 4.8 %convert_bitcast_fusion.2 = bf16[1,2048,896]{2,1,0:T(8,128)(2,1)} fusion(bf16[576,2048]{1,0:T(8,128)(2,1)S(1)} %copy-done.14, bf16[320,896]{1,0:T(8,128)(2,1)S(1)} %copy-done.29, bf16[256,896]{1,0:T(8,128)(2,1)S(1)} %copy-done.25), kind=kOutput, calls=%fused_computation.2 | convolution fusion | flops 2117828608 | bytes 7061504 | tf_op jit(solution)/shard_map/dot_general | solution.py:23
  184.8 4.3 %all-to-all-done.5.got = bf16[32,136,128]{2,1,0:T(8,128)(2,1)S(1)} async-done(((bf16[32,136,128]{2,1,0:T(8,128)(2,1)}), bf16[32,136,128]{2,1,0:T(8,128)(2,1)S(1)}, u32[]{:S(2)}, u32[]{:S(2)}) %all-to-all-start.5) | async-done | bytes 1114144 | tf_op jit(solution)/shard_map/all_to_all | solution.py:575
  (91 shorter events, 15.1 us)
Async XLA Ops:
  0.6 13.1 %copy-start.15 = (bf16[192,256]{1,0:T(8,128)(2,1)S(1)}, bf16[192,256]{1,0:T(8,128)(2,1)}, u32[]{:S(2)}) copy-start(bf16[192,256]{1,0:T(8,128)(2,1)} %param.22) | copy-start | bytes 294916
  3.1 11.1 %copy-start.18 = (f32[256]{0:T(256)S(1)}, f32[256]{0:T(256)}, u32[]{:S(2)}) copy-start(f32[256]{0:T(256)} %param.26) | copy-start | bytes 3076
  3.1 11.1 %copy-start.16 = (f32[192,256]{1,0:T(8,128)S(1)}, f32[192,256]{1,0:T(8,128)}, u32[]{:S(2)}) copy-start(f32[192,256]{1,0:T(8,128)} %param.27) | copy-start | bytes 589828
  3.1 21.2 %all-to-all-start = ((bf16[32,64,128]{2,1,0:T(8,128)(2,1)}), bf16[32,64,128]{2,1,0:T(8,128)(2,1)S(1)}, u32[]{:S(2)}, u32[]{:S(2)}) async-start(bf16[32,64,128]{2,1,0:T(8,128)(2,1)} %get-tuple-element.36), calls=%async_computation | async-start | bytes 1048576 | tf_op jit(solution)/shard_map/all_to_all | solution.py:488
  24.2 24.2 %copy-start.12 = (bf16[32,64,128]{2,1,0:T(8,128)(2,1)}, bf16[32,64,128]{2,1,0:T(8,128)(2,1)S(1)}, u32[]{:S(2)}) copy-start(bf16[32,64,128]{2,1,0:T(8,128)(2,1)S(1)} %all-to-all-done.refs_1_) | copy-start | bytes 1572868
  24.2 18.3 %all-to-all-start.1 = ((bf16[32,96,128]{2,1,0:T(8,128)(2,1)}), bf16[32,96,128]{2,1,0:T(8,128)(2,1)S(1)}, u32[]{:S(2)}, u32[]{:S(2)}) async-start(bf16[32,96,128]{2,1,0:T(8,128)(2,1)} %get-tuple-element.41), calls=%async_computation.1 | async-start | bytes 1572864 | tf_op jit(solution)/shard_map/all_to_all | solution.py:517
  28.3 8.9 %collective-permute-start = (bf16[16,64,128]{2,1,0:T(8,128)(2,1)S(1)}, bf16[16,64,128]{2,1,0:T(8,128)(2,1)}, u32[]{:S(2)}, u32[]{:S(2)}) collective-permute-start(bf16[16,64,128]{2,1,0:T(8,128)(2,1)S(1)} %get-tuple-element.73), channel_id=1, source_target_pairs={{0,1},{1,2},{2,3},{3,0},{4,5},{5,6},{6,7},{7,4},{8,9},{9,10},{10,1... | collective-permute-start | bytes 786440 | tf_op jit(solution)/shard_map/ppermute | solution.py:414
  29.5 7.6 %collective-permute-start.3 = (bf16[16,64,128]{2,1,0:T(8,128)(2,1)S(1)}, bf16[16,64,128]{2,1,0:T(8,128)(2,1)}, u32[]{:S(2)}, u32[]{:S(2)}) collective-permute-start(bf16[16,64,128]{2,1,0:T(8,128)(2,1)S(1)} %get-tuple-element.72), channel_id=1, source_target_pairs={{0,3},{1,0},{2,1},{3,2},{4,7},{5,4},{6,5},{7,6},{8,11},{9,8},{10,9... | collective-permute-start | bytes 786440 | tf_op jit(solution)/shard_map/ppermute | solution.py:414
  31.0 12.9 %collective-permute-start.1 = (bf16[16,64,128]{2,1,0:T(8,128)(2,1)S(1)}, bf16[16,64,128]{2,1,0:T(8,128)(2,1)}, u32[]{:S(2)}, u32[]{:S(2)}) collective-permute-start(bf16[16,64,128]{2,1,0:T(8,128)(2,1)S(1)} %get-tuple-element.72), channel_id=1, source_target_pairs={{0,1},{1,2},{2,3},{3,0},{4,5},{5,6},{6,7},{7,4},{8,9},{9,10},{10,1... | collective-permute-start | bytes 786440 | tf_op jit(solution)/shard_map/ppermute | solution.py:414
  31.0 14.4 %collective-permute-start.2 = (bf16[16,64,128]{2,1,0:T(8,128)(2,1)S(1)}, bf16[16,64,128]{2,1,0:T(8,128)(2,1)}, u32[]{:S(2)}, u32[]{:S(2)}) collective-permute-start(bf16[16,64,128]{2,1,0:T(8,128)(2,1)S(1)} %get-tuple-element.73), channel_id=1, source_target_pairs={{0,3},{1,0},{2,1},{3,2},{4,7},{5,4},{6,5},{7,6},{8,11},{9,8},{10,9... | collective-permute-start | bytes 786440 | tf_op jit(solution)/shard_map/ppermute | solution.py:414
  37.2 11.2 %collective-permute-start.4 = (bf16[16,64,128]{2,1,0:T(8,128)(2,1)}, bf16[16,64,128]{2,1,0:T(8,128)(2,1)}, u32[]{:S(2)}, u32[]{:S(2)}) collective-permute-start(bf16[16,64,128]{2,1,0:T(8,128)(2,1)} %collective-permute-done.refs_2_), channel_id=1, source_target_pairs={{0,1},{1,2},{2,3},{3,0},{4,5},{5,6},{6,7},{7,4},{8,9},{9,10},{10,1... | collective-permute-start | bytes 786440 | tf_op jit(solution)/shard_map/ppermute | solution.py:414
  37.2 11.2 %collective-permute-start.5 = (bf16[16,64,128]{2,1,0:T(8,128)(2,1)}, bf16[16,64,128]{2,1,0:T(8,128)(2,1)}, u32[]{:S(2)}, u32[]{:S(2)}) collective-permute-start(bf16[16,64,128]{2,1,0:T(8,128)(2,1)} %collective-permute-done.3.refs_5_), channel_id=1, source_target_pairs={{0,3},{1,0},{2,1},{3,2},{4,7},{5,4},{6,5},{7,6},{8,11},{9,8},{10,9... | collective-permute-start | bytes 786440 | tf_op jit(solution)/shard_map/ppermute | solution.py:414
  42.6 16.3 %copy-start.11 = (bf16[32,96,128]{2,1,0:T(8,128)(2,1)}, bf16[32,96,128]{2,1,0:T(8,128)(2,1)S(1)}, u32[]{:S(2)}) copy-start(bf16[32,96,128]{2,1,0:T(8,128)(2,1)S(1)} %all-to-all-done.1.refs_1_.got) | copy-start | bytes 2359300
  42.6 30.3 %collective-permute-start.6 = (bf16[16,80,128]{2,1,0:T(8,128)(2,1)S(1)}, bf16[16,80,128]{2,1,0:T(8,128)(2,1)S(1)}, u32[]{:S(2)}, u32[]{:S(2)}) collective-permute-start(bf16[16,80,128]{2,1,0:T(8,128)(2,1)S(1)} %get-tuple-element.71), channel_id=1, source_target_pairs={{0,1},{1,2},{2,3},{3,0},{4,5},{5,6},{6,7},{7,4},{8,9},{9,10},{10,1... | collective-permute-start | bytes 983048 | tf_op jit(solution)/shard_map/ppermute | solution.py:414
  43.9 29.1 %collective-permute-start.9 = (bf16[16,80,128]{2,1,0:T(8,128)(2,1)S(1)}, bf16[16,80,128]{2,1,0:T(8,128)(2,1)}, u32[]{:S(2)}, u32[]{:S(2)}) collective-permute-start(bf16[16,80,128]{2,1,0:T(8,128)(2,1)S(1)} %get-tuple-element.70), channel_id=1, source_target_pairs={{0,3},{1,0},{2,1},{3,2},{4,7},{5,4},{6,5},{7,6},{8,11},{9,8},{10,9... | collective-permute-start | bytes 983048 | tf_op jit(solution)/shard_map/ppermute | solution.py:414
  58.9 53.4 %all-to-all-start.3 = ((bf16[128,32,128]{2,1,0:T(8,128)(2,1)}), bf16[128,32,128]{2,1,0:T(8,128)(2,1)S(1)}, u32[]{:S(2)}, u32[]{:S(2)}) async-start(bf16[128,32,128]{2,1,0:T(8,128)(2,1)} %bitcast.58), calls=%async_computation.3 | async-start | bytes 2097152 | tf_op jit(solution)/shard_map/all_to_all | solution.py:530
  70.1 20.8 %collective-permute-start.7 = (bf16[16,80,128]{2,1,0:T(8,128)(2,1)S(1)}, bf16[16,80,128]{2,1,0:T(8,128)(2,1)S(1)}, u32[]{:S(2)}, u32[]{:S(2)}) collective-permute-start(bf16[16,80,128]{2,1,0:T(8,128)(2,1)S(1)} %get-tuple-element.70), channel_id=1, source_target_pairs={{0,1},{1,2},{2,3},{3,0},{4,5},{5,6},{6,7},{7,4},{8,9},{9,10},{10,1... | collective-permute-start | bytes 983048 | tf_op jit(solution)/shard_map/ppermute | solution.py:414
  71.6 19.4 %collective-permute-start.8 = (bf16[16,80,128]{2,1,0:T(8,128)(2,1)S(1)}, bf16[16,80,128]{2,1,0:T(8,128)(2,1)S(1)}, u32[]{:S(2)}, u32[]{:S(2)}) collective-permute-start(bf16[16,80,128]{2,1,0:T(8,128)(2,1)S(1)} %get-tuple-element.71), channel_id=1, source_target_pairs={{0,3},{1,0},{2,1},{3,2},{4,7},{5,4},{6,5},{7,6},{8,11},{9,8},{10,9... | collective-permute-start | bytes 983048 | tf_op jit(solution)/shard_map/ppermute | solution.py:414
  72.9 25.1 %copy-start.19 = (bf16[16,80,128]{2,1,0:T(8,128)(2,1)}, bf16[16,80,128]{2,1,0:T(8,128)(2,1)S(1)}, u32[]{:S(2)}) copy-start(bf16[16,80,128]{2,1,0:T(8,128)(2,1)S(1)} %collective-permute-done.6.refs_2_) | copy-start | bytes 983044
  72.9 25.1 %collective-permute-start.10 = (bf16[16,80,128]{2,1,0:T(8,128)(2,1)S(1)}, bf16[16,80,128]{2,1,0:T(8,128)(2,1)S(1)}, u32[]{:S(2)}, u32[]{:S(2)}) collective-permute-start(bf16[16,80,128]{2,1,0:T(8,128)(2,1)S(1)} %collective-permute-done.6.refs_2_), channel_id=1, source_target_pairs={{0,1},{1,2},{2,3},{3,0},{4,5},{5,6},{6,7},{7,4},{8,9},{9,10},{10,1... | collective-permute-start | bytes 983048 | tf_op jit(solution)/shard_map/ppermute | solution.py:414
  73.0 25.0 %collective-permute-start.11 = (bf16[16,80,128]{2,1,0:T(8,128)(2,1)}, bf16[16,80,128]{2,1,0:T(8,128)(2,1)S(1)}, u32[]{:S(2)}, u32[]{:S(2)}) collective-permute-start(bf16[16,80,128]{2,1,0:T(8,128)(2,1)} %collective-permute-done.9.refs_5_), channel_id=1, source_target_pairs={{0,3},{1,0},{2,1},{3,2},{4,7},{5,4},{6,5},{7,6},{8,11},{9,8},{10,9... | collective-permute-start | bytes 983048 | tf_op jit(solution)/shard_map/ppermute | solution.py:414
  91.0 7.0 %copy-start.20 = (bf16[16,80,128]{2,1,0:T(8,128)(2,1)}, bf16[16,80,128]{2,1,0:T(8,128)(2,1)S(1)}, u32[]{:S(2)}) copy-start(bf16[16,80,128]{2,1,0:T(8,128)(2,1)S(1)} %collective-permute-done.7.refs_3_) | copy-start | bytes 983044
  91.0 7.0 %copy-start.21 = (bf16[16,80,128]{2,1,0:T(8,128)(2,1)}, bf16[16,80,128]{2,1,0:T(8,128)(2,1)S(1)}, u32[]{:S(2)}) copy-start(bf16[16,80,128]{2,1,0:T(8,128)(2,1)S(1)} %collective-permute-done.8.refs_4_) | copy-start | bytes 983044
  112.2 8.1 %copy-start.17 = (s32[8,192]{1,0:T(8,128)S(1)}, s32[8,192]{1,0:T(8,128)}, u32[]{:S(2)}) copy-start(s32[8,192]{1,0:T(8,128)} %get-tuple-element.37.idx) | copy-start | bytes 18436
  112.2 8.2 %copy-start.5 = (bf16[192,512]{1,0:T(8,128)(2,1)S(1)}, bf16[192,512]{1,0:T(8,128)(2,1)}, u32[]{:S(2)}) copy-start(bf16[192,512]{1,0:T(8,128)(2,1)} %g.5) | copy-start | bytes 589828
  112.3 30.4 %all-to-all-start.2 = ((bf16[128,40,128]{2,1,0:T(8,128)(2,1)}), bf16[128,40,128]{2,1,0:T(8,128)(2,1)S(1)}, u32[]{:S(2)}, u32[]{:S(2)}) async-start(bf16[128,40,128]{2,1,0:T(8,128)(2,1)} %bitcast.57), calls=%async_computation.2 | async-start | bytes 2621440 | tf_op jit(solution)/shard_map/all_to_all | solution.py:532
  145.9 15.5 %all-to-all-start.4 = ((bf16[4,192,512]{2,1,0:T(8,128)(2,1)}), bf16[4,192,512]{2,1,0:T(8,128)(2,1)S(1)}, u32[]{:S(2)}, u32[]{:S(2)}) async-start(bf16[4,192,512]{2,1,0:T(8,128)(2,1)} %shard_map.186), calls=%async_computation.4 | async-start | bytes 1572864 | tf_op jit(solution)/shard_map/all_to_all | solution.py:554
  162.6 8.7 %copy-start.13 = (bf16[320,2048]{1,0:T(8,128)(2,1)S(1)}, bf16[320,2048]{1,0:T(8,128)(2,1)}, u32[]{:S(2)}) copy-start(bf16[320,2048]{1,0:T(8,128)(2,1)} %get-tuple-element.42) | copy-start | bytes 3932164
  166.5 22.7 %all-to-all-start.5 = ((bf16[32,136,128]{2,1,0:T(8,128)(2,1)}), bf16[32,136,128]{2,1,0:T(8,128)(2,1)S(1)}, u32[]{:S(2)}, u32[]{:S(2)}) async-start(bf16[32,136,128]{2,1,0:T(8,128)(2,1)} %get-tuple-element.58), calls=%async_computation.5 | async-start | bytes 2228224 | tf_op jit(solution)/shard_map/all_to_all | solution.py:575
  180.0 9.2 %copy-start.1 = (f32[192,256]{1,0:T(8,128)S(1)}, f32[192,256]{1,0:T(8,128)}, u32[]{:S(2)}) copy-start(f32[192,256]{1,0:T(8,128)} %get-tuple-element.61.gain) | copy-start | bytes 589828
  180.0 9.2 %copy-start.2 = (f32[192,256]{1,0:T(8,128)S(1)}, f32[192,256]{1,0:T(8,128)}, u32[]{:S(2)}) copy-start(f32[192,256]{1,0:T(8,128)} %get-tuple-element.62.rr) | copy-start | bytes 589828
  180.0 9.2 %copy-start.3 = (f32[32,256]{1,0:T(8,128)S(1)}, f32[32,256]{1,0:T(8,128)}, u32[]{:S(2)}) copy-start(f32[32,256]{1,0:T(8,128)} %get-tuple-element.59.coef) | copy-start | bytes 98308
  (18 other events, 75.3 us)
